TPU v7x, 128 devices: a whole 4x4x4 slice. The times are simulated.
128 devices in a mesh: sp: 16 (over z, x), tp: 8 (over y, core).
Axes of the slice: x: 4, y: 4, z: 4, core: 2. Of those that a mesh axis runs over, the one named last changes fastest.
Arguments:
- hidden_states: bfloat16 [12288, 4096], P('sp'), may hold values from -60 to 60
- w_conv_b: bfloat16 [4096, 2048], P(None, 'tp'), may hold values from -0.09375 to 0.09375
- w_conv_c: bfloat16 [4096, 2048], P(None, 'tp'), may hold values from -0.09375 to 0.09375
- w_conv_h: bfloat16 [4096, 2048], P(None, 'tp'), may hold values from -0.09375 to 0.09375
- conv_taps: bfloat16 [3, 2048], P(None, 'tp'), may hold values from -3.5 to 3.5
- w_query: bfloat16 [4096, 2048], P(None, 'tp'), may hold values from -0.15625 to 0.15625
- w_key: bfloat16 [4096, 2048], P(None, 'tp'), may hold values from -0.09375 to 0.09375
- w_value: bfloat16 [4096, 2048], P(None, 'tp'), may hold values from -0.09375 to 0.09375
- lambdas: float32 [16], P('tp'), may hold values from 0.3 to 0.8
- head_gain: bfloat16 [128], replicated, may hold values from 0.099609375 to 1.8984375
- w_out_conv: bfloat16 [2048, 4096], P('tp'), may hold values from -1 to 1
- w_out_attn: bfloat16 [2048, 4096], P('tp'), may hold values from -1 to 1
- out_gain: bfloat16 [4096], replicated, may hold values from 0.099609375 to 1.8984375
Outputs:
- mixed: bfloat16 [12288, 4096], P('sp', 'tp')
All inputs are finite; a program needn't handle non-finite values.
Results may differ from a plain program's by a relative error of at most 0.023.
Values may be sent and summed in bfloat16 or wider, within the bound.
No kernel may reach another device: no remote copies, remote signals or barrier semaphores. Data moves between devices by JAX's collectives and lax.ppermute only.
A program may use at most 192 MiB of HBM per device.

v0:
```python
import jax
import jax.numpy as jnp
import numpy as np
from jax import lax
from jax.experimental import pallas as pl
from jax.experimental.pallas import tpu as pltpu
from jax.sharding import Mesh
from jax.sharding import PartitionSpec as P

D = 4096
QK = 64
VD = 128
ROWS = 768
HALO = 16

CORE_OF_Z = (0, 1, 1, 0)


def forward_route(round_index):
    route = []
    for z in range(4):
        for c in range(2):
            local = round_index if z < 2 else 1 - round_index
            route.append((z * 2 + c, (2 * c + local) * 2 + CORE_OF_Z[z]))
    return route


def reverse(route):
    return [(b, a) for a, b in route]


GROUP = 64


def rotary_tables():
    inverse = 10000.0 ** (-np.arange(0, QK, 2, dtype=np.float64) / QK)
    inverse = np.tile(inverse, 128 // inverse.size)
    rows = np.arange(GROUP, dtype=np.float64)[:, None] * inverse
    starts = np.arange(0, 16 * ROWS, GROUP, dtype=np.float64)[:, None] * inverse
    tables = (np.cos(rows), np.sin(rows), np.cos(starts), np.sin(starts))
    return tuple(t.astype(np.float32) for t in tables)


CHUNK = 1024
STEPS = D // CHUNK
AHEAD = 3


def streamed_products(pairs, sem, accs):
    copies = []
    for hbm, buf, by_columns in pairs:
        slot = len(copies)

        def copy(k, hbm=hbm, buf=buf, by_columns=by_columns, slot=slot):
            at = pl.ds(k * CHUNK, CHUNK)
            source = hbm.at[:, at] if by_columns else hbm.at[at, :]
            return pltpu.make_async_copy(source, buf.at[k], sem.at[slot, k])

        copies.append(copy)
    for k in range(AHEAD):
        for copy in copies:
            copy(k).start()
    for acc, _, _ in accs:
        acc[...] = jnp.zeros(acc.shape, jnp.float32)

    def step(k, carry):
        @pl.when(k + AHEAD < STEPS)
        def _():
            for copy in copies:
                copy(k + AHEAD).start()

        for copy in copies:
            copy(k).wait()
        for acc, lhs, weights in accs:
            h = lhs[k]
            for i, w in enumerate(weights):
                acc[i] += jnp.dot(h, w[k], preferred_element_type=jnp.float32)
        return carry

    lax.fori_loop(0, STEPS, step, 0)


def qkv_kernel(
    first, h_ref, wk_ref, wv_ref, wq_ref, cr, sr, cs, ss, qa_ref, qb_ref, kva_ref, kvb_ref, acc, hb, kb, vb, qb, sem
):
    streamed_products(
        ((h_ref, hb, True), (wk_ref, kb, False), (wv_ref, vb, False), (wq_ref, qb, False)),
        sem,
        ((acc, hb, (kb, vb, qb)),),
    )
    groups = range(ROWS // GROUP)
    cosine = jnp.concatenate(
        [cs[g : g + 1] * cr[...] - ss[g : g + 1] * sr[...] for g in groups], axis=0
    )
    sine = jnp.concatenate(
        [ss[g : g + 1] * cr[...] + cs[g : g + 1] * sr[...] for g in groups], axis=0
    )
    lane = lax.broadcasted_iota(jnp.int32, (ROWS, 128), 1)
    upper = (lane % QK) < QK // 2

    def rotated(x):
        x = x.astype(jnp.bfloat16).astype(jnp.float32)
        swapped = jnp.where(upper, -pltpu.roll(x, 128 - QK // 2, 1), pltpu.roll(x, QK // 2, 1))
        return (x * cosine + swapped * sine).astype(jnp.bfloat16)

    keys = [rotated(acc[0, :, i * 128 : i * 128 + 128]) for i in range(2)]
    vals = [acc[1, :, i * 128 : i * 128 + 128].astype(jnp.bfloat16) for i in range(2)]
    queries = [rotated(acc[2, :, i * 128 : i * 128 + 128]) for i in range(2)]
    for flip, q_ref, kv_ref in ((0, qa_ref, kva_ref), (1, qb_ref, kvb_ref)):
        take = first[0] == flip
        kv_ref[:, 0:128] = jnp.where(take, keys[0], keys[1])
        kv_ref[:, 128:256] = jnp.where(take, vals[0], vals[1])
        q_ref[...] = jnp.where(take, queries[0], queries[1])


def in_hbm():
    return pl.BlockSpec(memory_space=pltpu.HBM)


def stream_buffers(weights, rim):
    rows = [pltpu.VMEM((STEPS, ROWS, CHUNK), jnp.bfloat16)]
    if rim:
        rows.append(pltpu.VMEM((STEPS, HALO, CHUNK), jnp.bfloat16))
    return (
        rows
        + [pltpu.VMEM((STEPS, CHUNK, 256), jnp.bfloat16)] * weights
        + [pltpu.SemaphoreType.DMA((weights + len(rows), STEPS))]
    )


def project_qkv(first, hidden, w_query, w_key, w_value, start_cos, start_sin):
    row_cos, row_sin, _, _ = rotary_tables()
    table = pl.BlockSpec((GROUP, 128), lambda k, *_: (0, 0))
    one = pl.BlockSpec((ROWS // GROUP, 128), lambda k, *_: (0, 0))
    return pl.pallas_call(
        qkv_kernel,
        out_shape=tuple(
            jax.ShapeDtypeStruct((ROWS, width), jnp.bfloat16) for width in (128, 128, 256, 256)
        ),
        grid_spec=pltpu.PrefetchScalarGridSpec(
            num_scalar_prefetch=1,
            grid=(1,),
            in_specs=[in_hbm(), in_hbm(), in_hbm(), in_hbm(), table, table, one, one],
            out_specs=tuple(
                pl.BlockSpec((ROWS, width), lambda k, *_: (0, 0)) for width in (128, 128, 256, 256)
            ),
            scratch_shapes=[pltpu.VMEM((3, ROWS, 256), jnp.float32), *stream_buffers(3, False)],
        ),
        compiler_params=pltpu.CompilerParams(vmem_limit_bytes=60 * 2**20),
        cost_estimate=pl.CostEstimate(
            flops=2 * ROWS * D * 768, bytes_accessed=13 * 2**20, transcendentals=0
        ),
        name="qkv",
    )(first, hidden, w_key, w_value, w_query, row_cos, row_sin, start_cos, start_sin)


def conv_kernel(
    h_ref, rim_ref, wb_ref, wc_ref, wh_ref, taps_ref, o_ref, acc, rim_acc, padded, hb, rb, b, c, h, sem
):
    streamed_products(
        (
            (h_ref, hb, True),
            (rim_ref, rb, True),
            (wb_ref, b, False),
            (wc_ref, c, False),
            (wh_ref, h, False),
        ),
        sem,
        ((acc, hb, (b, c, h)), (rim_acc, rb, (b, c, h))),
    )

    def once(x):
        return x.astype(jnp.bfloat16).astype(jnp.float32)

    padded[0:HALO] = once(rim_acc[1]) * once(rim_acc[2])
    padded[HALO:] = once(acc[1]) * once(acc[2])
    taps = taps_ref[...].astype(jnp.float32)
    conv = jnp.zeros((ROWS, 256), jnp.float32)
    for tap in range(3):
        conv = conv + taps[tap : tap + 1] * padded[HALO - 2 + tap : HALO - 2 + tap + ROWS]
    o_ref[...] = (once(acc[0]) * conv).astype(jnp.bfloat16)


def gated_conv(hidden, rim, w_b, w_c, w_h, taps):
    return pl.pallas_call(
        conv_kernel,
        out_shape=jax.ShapeDtypeStruct((ROWS, 256), jnp.bfloat16),
        grid=(1,),
        in_specs=[
            in_hbm(),
            in_hbm(),
            in_hbm(),
            in_hbm(),
            in_hbm(),
            pl.BlockSpec((3, 256), lambda k: (0, 0)),
        ],
        out_specs=pl.BlockSpec((ROWS, 256), lambda k: (0, 0)),
        scratch_shapes=[
            pltpu.VMEM((3, ROWS, 256), jnp.float32),
            pltpu.VMEM((3, HALO, 256), jnp.float32),
            pltpu.VMEM((HALO + ROWS, 256), jnp.float32),
            *stream_buffers(3, True),
        ],
        compiler_params=pltpu.CompilerParams(vmem_limit_bytes=60 * 2**20),
        cost_estimate=pl.CostEstimate(
            flops=2 * ROWS * D * 768, bytes_accessed=13 * 2**20, transcendentals=0
        ),
        name="gated_conv",
    )(hidden, rim, w_b, w_c, w_h, taps)


KEYS_AT_ONCE = 256


def split_maps(q, qz):
    lane = lax.broadcasted_iota(jnp.int32, (ROWS, 128), 1)
    q = q * jnp.bfloat16(0.125)
    qz[0] = jnp.where(lane < QK, q, jnp.zeros_like(q))
    qz[1] = jnp.where(lane >= QK, q, jnp.zeros_like(q))


def start_state(m_s, l_s, acc):
    m_s[...] = jnp.full(m_s.shape, -1e30, jnp.float32)
    l_s[...] = jnp.zeros(l_s.shape, jnp.float32)
    acc[...] = jnp.zeros(acc.shape, jnp.float32)


def attend(qz, kv_ref, m_s, l_s, acc, first_row, n, place, first_key, width, masked):
    rows = slice(first_row, first_row + n)
    keys = kv_ref[place, first_key : first_key + width, 0:128]
    vals = kv_ref[place, first_key : first_key + width, 128:256]
    s = lax.dot_general(
        qz[:, rows, :].reshape(2 * n, 128),
        keys,
        (((1,), (1,)), ((), ())),
        preferred_element_type=jnp.float32,
    ).reshape(2, n, width)
    if masked:
        r = lax.broadcasted_iota(jnp.int32, (2, n, width), 1) + first_row
        k = lax.broadcasted_iota(jnp.int32, (2, n, width), 2) + first_key
        s = jnp.where(k <= r, s, -1e30)
    m_old = m_s[:, rows, :]
    m_new = jnp.maximum(m_old, jnp.max(s, axis=2, keepdims=True))
    alpha = jnp.exp(m_old - m_new)
    p = jnp.exp(s - jnp.tile(m_new, (1, 1, width // 128)))
    part = p[:, :, 0:128]
    for w in range(1, width // 128):
        part = part + p[:, :, w * 128 : (w + 1) * 128]
    l_s[:, rows, :] = l_s[:, rows, :] * alpha + part
    m_s[:, rows, :] = m_new
    pv = jnp.dot(
        p.astype(jnp.bfloat16).reshape(2 * n, width), vals, preferred_element_type=jnp.float32
    )
    acc[:, rows, :] = acc[:, rows, :] * alpha + pv.reshape(2, n, 128)


def attend_blocks(first, count, place_of, refs):
    def block(kb):
        place = place_of(kb)
        for j in range(ROWS // KEYS_AT_ONCE):
            attend(*refs, 0, ROWS, place, j * KEYS_AT_ONCE, KEYS_AT_ONCE, False)

    def body(pair, carry):
        block(first + 2 * pair)
        block(first + 2 * pair + 1)
        return carry

    lax.fori_loop(0, count // 2, body, 0)

    @pl.when(count % 2 == 1)
    def _():
        block(first + count - 1)


def attend_diagonal(place, refs):
    for t in range(ROWS // 256):
        attend(*refs, t * 256, 256, place, 0, 256 * (t + 1), True)


def finish(lam, gain_ref, l_s, acc):
    denom = jnp.sum(l_s[...], axis=2, keepdims=True)
    diff = acc[0] / denom[0] - lam[0] * acc[1] / denom[1]
    mean_square = jnp.mean(diff * diff, axis=1, keepdims=True)
    normed = diff * lax.rsqrt(mean_square + 1e-5) * gain_ref[...].astype(jnp.float32)
    return normed.astype(jnp.bfloat16)


def low_place(kb):
    return (kb % 4) * 2 + kb // 4


def high_place(kb):
    return (kb % 4) * 2 + 3 - kb // 4


def low_kernel(own, lam, qa_ref, qb_ref, kv_ref, gain_ref, _, o_ref, m_o, l_o, a_o, qz):
    step = pl.program_id(0)
    split_maps(jnp.where(step == own[2], qa_ref[...], qb_ref[...]), qz)
    start_state(m_o, l_o, a_o)
    refs = (qz, kv_ref, m_o, l_o, a_o)
    attend_blocks(0, jnp.where(step == 0, own[0], 8), low_place, refs)

    @pl.when(step == 0)
    def _():
        attend_diagonal(low_place(own[0]), refs)
        o_ref[...] = finish(lam, gain_ref, l_o, a_o)


def high_kernel(
    own, lam, qa_ref, qb_ref, kv_ref, gain_ref, low_ref, m_i, l_i, a_i, _, oa_ref, ob_ref, qz
):
    low_first = own[2] == 0
    split_maps(jnp.where(low_first, qb_ref[...], qa_ref[...]), qz)
    refs = (qz, kv_ref, m_i, l_i, a_i)
    attend_blocks(8, own[1] - 8, high_place, refs)
    attend_diagonal(high_place(own[1]), refs)
    high = finish(lam, gain_ref, l_i, a_i)
    oa_ref[...] = jnp.where(low_first, low_ref[...], high)
    ob_ref[...] = jnp.where(low_first, high, low_ref[...])


def attention_call(kernel, steps, args, outs, unread, blocks):
    def full(shape):
        return pl.BlockSpec(shape, lambda i, *_: (0,) * len(shape))

    return pl.pallas_call(
        kernel,
        out_shape=outs,
        grid_spec=pltpu.PrefetchScalarGridSpec(
            num_scalar_prefetch=2,
            grid=(steps,),
            in_specs=[full(a.shape) for a in args[2:]] + [in_hbm() for _ in unread],
            out_specs=tuple(full(o.shape) for o in outs),
            scratch_shapes=[pltpu.VMEM((2, ROWS, 128), jnp.bfloat16)],
        ),
        compiler_params=pltpu.CompilerParams(vmem_limit_bytes=60 * 2**20),
        cost_estimate=pl.CostEstimate(
            flops=blocks * 2 * 10**9, bytes_accessed=4 * 2**20, transcendentals=0
        ),
    )(*args, *unread)


def column_kernel(wc_ref, wa_ref, o_ref, sem):
    width = o_ref.shape[3]
    copies = [
        pltpu.make_async_copy(
            w_ref.at[:, pl.ds(t * width, width)], o_ref.at[t, i], sem.at[i, t]
        )
        for i, w_ref in enumerate((wc_ref, wa_ref))
        for t in range(8)
    ]
    for copy in copies:
        copy.start()
    for copy in copies:
        copy.wait()


def column_blocks(w_conv, w_attn):
    return pl.pallas_call(
        column_kernel,
        out_shape=jax.ShapeDtypeStruct((8, 2, 256, D // 8), jnp.bfloat16),
        in_specs=[in_hbm(), in_hbm()],
        out_specs=in_hbm(),
        scratch_shapes=[pltpu.SemaphoreType.DMA((2, 8))],
        name="column_blocks",
    )(w_conv, w_attn)


def whole_conv_kernel(x_ref, w_ref, o_ref):
    left = jnp.concatenate([x_ref[t] for t in range(8)], axis=1)
    right = jnp.concatenate([w_ref[t, 0] for t in range(8)], axis=0)
    o_ref[...] = jnp.dot(left, right, preferred_element_type=jnp.float32)


def whole_last_kernel(first, x_ref, w_ref, before_ref, mix_ref, sums_ref, xb, wb, acc, sem):
    copies = []
    for t in range(8):
        copies.append(pltpu.make_async_copy(x_ref.at[t], xb.at[t], sem.at[0, t]))
        copies.append(pltpu.make_async_copy(w_ref.at[t, 1], wb.at[t], sem.at[1, t]))
    head = pltpu.make_async_copy(before_ref, acc, sem.at[2, 0])
    head.start()
    for copy in copies:
        copy.start()
    head.wait()
    for t in range(8):
        copies[2 * t].wait()
        copies[2 * t + 1].wait()
        right = jnp.concatenate(
            [
                wb[t, pl.ds(pl.multiple_of(first[0] * VD, VD), VD), :],
                wb[t, pl.ds(pl.multiple_of((1 - first[0]) * VD, VD), VD), :],
            ],
            axis=0,
        )
        acc[...] += jnp.dot(xb[t], right, preferred_element_type=jnp.float32)
    mix = acc[...].astype(jnp.bfloat16)
    mix_ref[...] = mix
    wide = mix.astype(jnp.float32)
    square = wide * wide
    high = square.astype(jnp.bfloat16)
    low = (square - high.astype(jnp.float32)).astype(jnp.bfloat16)
    ones = jnp.ones((8, mix.shape[1]), jnp.bfloat16)

    def row_sums(values):
        return lax.dot_general(
            ones, values, (((1,), (1,)), ((), ())), preferred_element_type=jnp.float32
        )[0:1]

    sums = jnp.concatenate([row_sums(mix), row_sums(high) + row_sums(low)], axis=0)
    for copy in range(8):
        sums_ref[copy] = sums


def whole_conv(gathered, weights):
    width = weights.shape[3]
    return pl.pallas_call(
        whole_conv_kernel,
        out_shape=jax.ShapeDtypeStruct((ROWS, width), jnp.float32),
        grid=(1,),
        in_specs=[
            pl.BlockSpec(gathered.shape, lambda i: (0, 0, 0)),
            pl.BlockSpec((8, 1, 256, width), lambda i: (0, 0, 0, 0)),
        ],
        out_specs=pl.BlockSpec((ROWS, width), lambda i: (0, 0)),
        compiler_params=pltpu.CompilerParams(vmem_limit_bytes=60 * 2**20),
        cost_estimate=pl.CostEstimate(
            flops=2 * ROWS * 2048 * width, bytes_accessed=7 * 2**20, transcendentals=0
        ),
        name="whole_conv",
    )(gathered, weights)


def whole_last(first, gathered, weights, before):
    width = weights.shape[3]
    return pl.pallas_call(
        whole_last_kernel,
        out_shape=(
            jax.ShapeDtypeStruct((ROWS, width), jnp.bfloat16),
            jax.ShapeDtypeStruct((8, 2, ROWS), jnp.float32),
        ),
        grid_spec=pltpu.PrefetchScalarGridSpec(
            num_scalar_prefetch=1,
            grid=(1,),
            in_specs=[in_hbm(), in_hbm(), in_hbm()],
            out_specs=(
                pl.BlockSpec((ROWS, width), lambda i, *_: (0, 0)),
                pl.BlockSpec((8, 2, ROWS), lambda i, *_: (0, 0, 0)),
            ),
            scratch_shapes=[
                pltpu.VMEM((8, ROWS, 256), jnp.bfloat16),
                pltpu.VMEM((8, 256, width), jnp.bfloat16),
                pltpu.VMEM((ROWS, width), jnp.float32),
                pltpu.SemaphoreType.DMA((3, 8)),
            ],
        ),
        compiler_params=pltpu.CompilerParams(vmem_limit_bytes=60 * 2**20),
        cost_estimate=pl.CostEstimate(
            flops=2 * ROWS * 2048 * width, bytes_accessed=7 * 2**20, transcendentals=0
        ),
        name="whole_last",
    )(first, gathered, weights, before)


def per_device(
    hidden_states,
    w_conv_b,
    w_conv_c,
    w_conv_h,
    conv_taps,
    w_query,
    w_key,
    w_value,
    lambdas,
    head_gain,
    w_out_conv,
    w_out_attn,
    out_gain,
):
    z = lax.axis_index("z")
    x = lax.axis_index("x")
    core = lax.axis_index("c")
    sp = z * 4 + x

    z_core = ("z", "c")
    rim = lax.ppermute(hidden_states[ROWS - HALO :], ("z", "x"), [(i, i + 1) for i in range(15)])
    other_lambdas = lax.ppermute(lambdas, "c", [(0, 1), (1, 0)])

    first = jnp.where(z < 2, 0, 1).astype(jnp.int32).reshape(1)
    _, _, start_cos, start_sin = rotary_tables()
    groups = ROWS // GROUP
    q_a, q_b, kv_a, kv_b = project_qkv(
        first,
        hidden_states,
        w_query,
        w_key,
        w_value,
        lax.dynamic_slice_in_dim(jnp.asarray(start_cos), sp * groups, groups, 0),
        lax.dynamic_slice_in_dim(jnp.asarray(start_sin), sp * groups, groups, 0),
    )
    route_a, route_b = forward_route(0), forward_route(1)
    kv_a = lax.ppermute(kv_a, z_core, route_a)
    kv_b = lax.ppermute(kv_b, z_core, route_b)
    q_a = lax.ppermute(q_a, z_core, route_a)
    q_b = lax.ppermute(q_b, z_core, route_b)
    even = (z % 2) == 0
    kv_low = lax.all_gather(jnp.where(even, kv_a, kv_b), ("x", "c"), axis=0)
    kv_high = lax.all_gather(jnp.where(even, kv_b, kv_a), ("x", "c"), axis=0)

    conv_out = gated_conv(hidden_states, rim, w_conv_b, w_conv_c, w_conv_h, conv_taps)
    conv_all = lax.all_gather(conv_out, ("y", "c"), axis=0)

    w_out = lax.all_to_all(
        column_blocks(w_out_conv, w_out_attn),
        ("y", "c"),
        split_axis=0,
        concat_axis=0,
        tiled=True,
    )

    plane_lambdas = jnp.where(
        core == 0,
        jnp.concatenate([lambdas, other_lambdas]),
        jnp.concatenate([other_lambdas, lambdas]),
    )
    lam = lax.dynamic_slice_in_dim(plane_lambdas, z, 1)
    low_z, high_z = jnp.where(core == 0, 0, 1), jnp.where(core == 0, 3, 2)
    own = jnp.stack([low_z * 4 + x, high_z * 4 + x, z % 2]).astype(jnp.int32)
    gain = head_gain.reshape(1, VD)
    rows = jax.ShapeDtypeStruct((ROWS, VD), jnp.bfloat16)
    state = (jax.ShapeDtypeStruct((2, ROWS, VD), jnp.float32),) * 3
    o_low, *carried = attention_call(
        low_kernel, 2, (own, lam, q_a, q_b, kv_low, gain), (rows, *state), (conv_out,), 12
    )
    o_a, o_b = attention_call(
        high_kernel,
        1,
        (own, lam, q_a, q_b, kv_high, gain, o_low, *carried),
        (rows, rows),
        (w_out,),
        6,
    )
    back_a = lax.ppermute(o_a, z_core, reverse(route_a))
    back_b = lax.ppermute(o_b, z_core, reverse(route_b))
    attn_all = lax.all_gather(jnp.concatenate([back_a, back_b], axis=1), ("y", "c"), axis=0)
    conv_part = whole_conv(conv_all, w_out)
    mix, sums = whole_last(first, attn_all, w_out, conv_part)
    everything = lax.all_to_all(sums, ("y", "c"), split_axis=0, concat_axis=0, tiled=True)
    totals = jnp.sum(everything, axis=0)
    mix_f = mix.astype(jnp.float32)
    width = mix_f.shape[1]
    mean_value = (totals[0] / D)[:, None]
    variance = (totals[1] / D)[:, None] - mean_value * mean_value
    tp = lax.axis_index("y") * 2 + core
    own_gain = lax.dynamic_slice_in_dim(out_gain.astype(jnp.float32), tp * width, width, 0)
    return ((mix_f - mean_value) * lax.rsqrt(variance + 1e-05) * own_gain[None, :]).astype(
        jnp.bfloat16
    )


def solution(mesh):
    chips = Mesh(mesh.devices.reshape(4, 4, 4, 2), ("z", "x", "y", "c"))
    sp, tp = ("z", "x"), ("y", "c")
    return jax.shard_map(
        per_device,
        mesh=chips,
        in_specs=(
            P(sp, None),
            P(None, tp),
            P(None, tp),
            P(None, tp),
            P(None, tp),
            P(None, tp),
            P(None, tp),
            P(None, tp),
            P(tp),
            P(),
            P(tp, None),
            P(tp, None),
            P(),
        ),
        out_specs=P(sp, tp),
        check_vma=False,
    )
```

profile of v0, /device:TPU:1, one launch (start us, length us, event | category | flops | bytes accessed | tf_op | source)
XLA Modules:
  0.0 319.1 jit_solution(4283507149193906920)
XLA Ops:
  6.5 0.0 all-gather.11.cloned.1.call-start
  6.5 1.3 constant_dynamic-slice_fusion
  7.9 10.1 %qkv.1 = (bf16[768,128]{1,0:T(8,128)(2,1)}, bf16[768,128]{1,0:T(8,128)(2,1)}, bf16[768,256]{1,0:T(8,128)(2,1)}, bf16[768,256]{1,0:T(8,128)(2,1)}) custom-call(s32[1]{0:T(128)} %bitcast.first, bf16[768,4096]{1,0:T(8,128)(2,1)} %h_ref.3, bf16[4096,256]{1,0:T(8,128)(2,1)} %wk_ref.1, bf16[4096,256]{1,0:T(8,128)(2,1)} %wv_ref.1, bf16[4096,256]{1,0:T(8,128)(2,1)} %wq_ref.1, ...), custom_call_target="tpu_custom_call" | custom-call | flops 4831838208 | bytes 13631488 | tf_op jit(solution)/shard_map/qkv/pallas_call | solution.py:135
  18.0 7.0 %collective-permute-start.3 = (bf16[768,256]{1,0:T(8,128)(2,1)}, bf16[768,256]{1,0:T(8,128)(2,1)S(1)}, u32[]{:S(2)}, u32[]{:S(2)}) collective-permute-start(bf16[768,256]{1,0:T(8,128)(2,1)} %get-tuple-element.19), channel_id=1, source_target_pairs={{0,32},{1,96},{32,33},{33,97},{64,1},{65,65},{96,0},{97,64},{2,34}... | collective-permute-start | bytes 1179656 | tf_op jit(solution)/shard_map/ppermute | solution.py:502
  25.0 1.9 collective-permute-start.4
  26.9 7.0 %collective-permute-done.3 = bf16[768,256]{1,0:T(8,128)(2,1)S(1)} collective-permute-done((bf16[768,256]{1,0:T(8,128)(2,1)}, bf16[768,256]{1,0:T(8,128)(2,1)S(1)}, u32[]{:S(2)}, u32[]{:S(2)}) %collective-permute-start.3) | collective-permute-done | bytes 393248 | tf_op jit(solution)/shard_map/ppermute | solution.py:502
  34.0 1.0 collective-permute-done.4
  34.9 1.0 broadcast_select_fusion
  35.9 0.0 all-gather.11.cloned.1.call-update
  35.9 0.0 all-gather.9.cloned.1.call-start
  36.0 0.7 all-gather.9.cloned.1.call-update
  36.7 0.0 all-gather.15.cloned.1.call-start
  36.7 0.9 slice.9
  37.6 3.1 collective-permute-start.5
  40.8 2.3 collective-permute-done.5.rim_ref
  43.1 0.7 copy-done.5
  43.8 10.6 %gated_conv.1._ = bf16[768,256]{1,0:T(8,128)(2,1)} custom-call(bf16[768,4096]{1,0:T(8,128)(2,1)} %h_ref.3, bf16[16,4096]{1,0:T(8,128)(2,1)} %copy-done.5, bf16[4096,256]{1,0:T(8,128)(2,1)} %wb_ref.1, bf16[4096,256]{1,0:T(8,128)(2,1)} %wc_ref.2, bf16[4096,256]{1,0:T(8,128)(2,1)} %wh_ref.1, bf16[3,256]{1,0:T(4,128)(2,1)} %taps_ref.1), custom_call_target="tpu_custom_call" | custom-call | flops 4831838208 | bytes 13631488 | tf_op jit(solution)/shard_map/gated_conv/pallas_call | solution.py:185
  54.4 0.0 all-gather.15.cloned.1.call-update
  54.4 128.3 %column_blocks.1 = bf16[8,2,256,512]{3,2,1,0:T(8,128)(2,1)} custom-call(bf16[256,4096]{1,0:T(8,128)(2,1)} %wc_ref.3, bf16[256,4096]{1,0:T(8,128)(2,1)} %wa_ref.1), custom_call_target="tpu_custom_call" | custom-call | tf_op jit(solution)/shard_map/column_blocks/pallas_call | solution.py:359
  182.8 0.0 copy-start
  182.8 6.1 %all-to-all-start = ((bf16[8,2,256,512]{3,2,1,0:T(8,128)(2,1)}), bf16[8,2,256,512]{3,2,1,0:T(8,128)(2,1)}, u32[]{:S(2)}, u32[]{:S(2)}) async-start(bf16[8,2,256,512]{3,2,1,0:T(8,128)(2,1)} %column_blocks.1), calls=%async_computation | async-start | bytes 8388608 | tf_op jit(solution)/shard_map/all_to_all | solution.py:512
  188.8 8.6 %collective-permute-start.1 = (bf16[768,128]{1,0:T(8,128)(2,1)S(1)}, bf16[768,128]{1,0:T(8,128)(2,1)S(1)}, u32[]{:S(2)}, u32[]{:S(2)}) collective-permute-start(bf16[768,128]{1,0:T(8,128)(2,1)S(1)} %copy-done.2), channel_id=1, source_target_pairs={{0,0},{1,64},{32,1},{33,65},{64,33},{65,97},{96,32},{97,96},{2,2},... | collective-permute-start | bytes 589832 | tf_op jit(solution)/shard_map/ppermute | solution.py:503
  197.5 2.1 collective-permute-start.2
  199.6 0.3 collective-permute-start
  199.9 0.6 pad_add_fusion.own
  200.5 0.5 collective-permute-done
  201.0 0.1 broadcast_select_fusion.2
  201.1 0.6 dynamic_slice.12.lam
  201.7 0.4 collective-permute-done.1.qa_ref
  202.2 3.8 %collective-permute-done.2.qb_ref = bf16[768,128]{1,0:T(8,128)(2,1)S(1)} collective-permute-done((bf16[768,128]{1,0:T(8,128)(2,1)S(1)}, bf16[768,128]{1,0:T(8,128)(2,1)S(1)}, u32[]{:S(2)}, u32[]{:S(2)}) %collective-permute-start.2) | collective-permute-done | bytes 196640 | tf_op jit(solution)/shard_map/ppermute | solution.py:504
  206.0 0.7 copy-done.4
  206.7 25.8 %shard_map.163 = (bf16[768,128]{1,0:T(8,128)(2,1)}, f32[2,768,128]{2,1,0:T(8,128)}, f32[2,768,128]{2,1,0:T(8,128)}, f32[2,768,128]{2,1,0:T(8,128)}) custom-call(s32[3]{0:T(128)} %pad_add_fusion.own, f32[1]{0:T(128)} %dynamic_slice.12.lam, bf16[768,128]{1,0:T(8,128)(2,1)} %copy-done.3, bf16[768,128]{1,0:T(8,128)(2,1)} %copy-done.4, ...), custom_call_target="tpu_custom_call" | custom-call | flops 24000000000 | bytes 4194304 | tf_op jit(solution)/shard_map/pallas_call | solution.py:326
  232.4 5.2 %all-to-all-done._.w_ref = bf16[8,2,256,512]{3,2,1,0:T(8,128)(2,1)} async-done(((bf16[8,2,256,512]{3,2,1,0:T(8,128)(2,1)}), bf16[8,2,256,512]{3,2,1,0:T(8,128)(2,1)}, u32[]{:S(2)}, u32[]{:S(2)}) %all-to-all-start) | async-done | bytes 4194336 | tf_op jit(solution)/shard_map/all_to_all | solution.py:512
  237.6 7.0 %shard_map.164 = (bf16[768,128]{1,0:T(8,128)(2,1)}, bf16[768,128]{1,0:T(8,128)(2,1)}) custom-call(s32[3]{0:T(128)} %pad_add_fusion.own, f32[1]{0:T(128)} %dynamic_slice.12.lam, bf16[768,128]{1,0:T(8,128)(2,1)} %copy-done.3, bf16[768,128]{1,0:T(8,128)(2,1)} %copy-done.4, bf16[8,768,256]{2,1,0:T(8,128)(2,1)} %bitcast.11, bf16[1,128]{1,0:T(2,128)(2,1)} %bitcast.14, ...), custom_call_target="tpu_custom_call" | custom-call | flops 12000000000 | bytes 4194304 | tf_op jit(solution)/shard_map/pallas_call | solution.py:326
  244.7 13.2 %collective-permute-start.6 = (bf16[768,128]{1,0:T(8,128)(2,1)}, bf16[768,128]{1,0:T(8,128)(2,1)S(1)}, u32[]{:S(2)}, u32[]{:S(2)}) collective-permute-start(bf16[768,128]{1,0:T(8,128)(2,1)} %get-tuple-element.25), channel_id=1, source_target_pairs={{0,0},{64,1},{1,32},{65,33},{33,64},{97,65},{32,96},{96,97},{2,2},... | collective-permute-start | bytes 589832 | tf_op jit(solution)/shard_map/ppermute | solution.py:542
  257.9 4.3 %collective-permute-start.7 = (bf16[768,128]{1,0:T(8,128)(2,1)}, bf16[768,128]{1,0:T(8,128)(2,1)S(1)}, u32[]{:S(2)}, u32[]{:S(2)}) collective-permute-start(bf16[768,128]{1,0:T(8,128)(2,1)} %get-tuple-element.26), channel_id=1, source_target_pairs={{32,0},{96,1},{33,32},{97,33},{1,64},{65,65},{0,96},{64,97},{34,2}... | collective-permute-start | bytes 589832 | tf_op jit(solution)/shard_map/ppermute | solution.py:543
  262.2 1.6 collective-permute-done.6
  263.8 2.5 collective-permute-done.7
  266.3 0.8 pad_maximum_fusion
  267.1 0.0 all-gather.13.cloned.1.call-update
  267.1 0.0 all-gather.15.cloned.1.call-done
  267.2 5.6 %whole_conv.1.before_ref = f32[768,512]{1,0:T(8,128)} custom-call(bf16[8,768,256]{2,1,0:T(8,128)(2,1)} %bitcast.9, bf16[8,2,256,512]{3,2,1,0:T(8,128)(2,1)} %all-to-all-done._.w_ref), custom_call_target="tpu_custom_call" | custom-call | flops 1610612736 | bytes 7340032 | tf_op jit(solution)/shard_map/whole_conv/pallas_call | solution.py:416
  272.7 23.8 %all-gather.13.cloned.1.call-done = bf16[6144,256]{1,0:T(8,128)(2,1)} async-done(((bf16[768,256]{1,0:T(8,128)(2,1)}), bf16[6144,256]{1,0:T(8,128)(2,1)}) %all-gather.13.cloned.1.call-update) | async-done | bytes 3145744 | tf_op jit(solution)/shard_map/all_gather | solution.py:544
  296.5 5.3 %whole_last.1 = (bf16[768,512]{1,0:T(8,128)(2,1)}, f32[8,2,768]{2,1,0:T(2,128)}) custom-call(s32[1]{0:T(128)} %bitcast.first, bf16[8,768,256]{2,1,0:T(8,128)(2,1)} %bitcast.10, bf16[8,2,256,512]{3,2,1,0:T(8,128)(2,1)} %all-to-all-done._.w_ref, f32[768,512]{1,0:T(8,128)} %whole_conv.1.before_ref), custom_call_target="tpu_custom_call" | custom-call | flops 1610612736 | bytes 7340032 | tf_op jit(solution)/shard_map/whole_last/pallas_call | solution.py:435
  301.8 3.5 %all-to-all-start.1 = ((f32[8,2,768]{2,1,0:T(2,128)}), f32[8,2,768]{2,1,0:T(2,128)S(1)}, u32[]{:S(2)}, u32[]{:S(2)}) async-start(f32[8,2,768]{2,1,0:T(2,128)} %get-tuple-element.28), calls=%async_computation.1 | async-start | bytes 98304 | tf_op jit(solution)/shard_map/all_to_all | solution.py:547
  305.3 0.8 dynamic-slice_convert_fusion
  306.1 4.0 %all-to-all-done.1 = f32[8,2,768]{2,1,0:T(2,128)S(1)} async-done(((f32[8,2,768]{2,1,0:T(2,128)}), f32[8,2,768]{2,1,0:T(2,128)S(1)}, u32[]{:S(2)}, u32[]{:S(2)}) %all-to-all-start.1) | async-done | bytes 49184 | tf_op jit(solution)/shard_map/all_to_all | solution.py:547
  310.2 2.4 multiply_convert_fusion
  (15 shorter events, 0.1 us)
Async XLA Ops:
  6.5 199.5 %all-gather.11.cloned.1.call-start = ((), (), s32[]{:S(2)}) async-start(), calls=%async_computation.3 | async-start | bytes 3538944 | tf_op jit(solution)/shard_map/all_gather | solution.py:506
  18.0 16.0 %collective-permute-start.3 = (bf16[768,256]{1,0:T(8,128)(2,1)}, bf16[768,256]{1,0:T(8,128)(2,1)S(1)}, u32[]{:S(2)}, u32[]{:S(2)}) collective-permute-start(bf16[768,256]{1,0:T(8,128)(2,1)} %get-tuple-element.19), channel_id=1, source_target_pairs={{0,32},{1,96},{32,33},{33,97},{64,1},{65,65},{96,0},{97,64},{2,34}... | collective-permute-start | bytes 1179656 | tf_op jit(solution)/shard_map/ppermute | solution.py:502
  25.0 9.9 %collective-permute-start.4 = (bf16[768,256]{1,0:T(8,128)(2,1)}, bf16[768,256]{1,0:T(8,128)(2,1)S(1)}, u32[]{:S(2)}, u32[]{:S(2)}) collective-permute-start(bf16[768,256]{1,0:T(8,128)(2,1)} %get-tuple-element.20), channel_id=1, source_target_pairs={{0,0},{1,64},{32,1},{33,65},{64,33},{65,97},{96,32},{97,96},{2,2},... | collective-permute-start | bytes 1179656 | tf_op jit(solution)/shard_map/ppermute | solution.py:501
  35.9 201.7 %all-gather.9.cloned.1.call-start = ((), (), s32[]{:S(2)}) async-start(), calls=%async_computation.2 | async-start | bytes 3538944 | tf_op jit(solution)/shard_map/all_gather | solution.py:507
  36.7 230.5 %all-gather.15.cloned.1.call-start = ((), (), s32[]{:S(2)}) async-start(), calls=%async_computation.5 | async-start | bytes 3538944 | tf_op jit(solution)/shard_map/all_gather | solution.py:510
  37.6 5.5 %collective-permute-start.5 = (bf16[16,4096]{1,0:T(8,128)(2,1)S(1)}, bf16[16,4096]{1,0:T(8,128)(2,1)S(1)}, u32[]{:S(2)}, u32[]{:S(2)}) collective-permute-start(bf16[16,4096]{1,0:T(8,128)(2,1)S(1)} %slice.9), channel_id=1, source_target_pairs={{0,8},{8,16},{16,24},{24,32},{32,40},{40,48},{48,56},{56,64},{64,7... | collective-permute-start | bytes 393224 | tf_op jit(solution)/shard_map/ppermute | solution.py:485
  43.1 0.7 copy-start.5
  182.7 6.1 %copy-start.2 = (bf16[768,128]{1,0:T(8,128)(2,1)S(1)}, bf16[768,128]{1,0:T(8,128)(2,1)}, u32[]{:S(2)}) copy-start(bf16[768,128]{1,0:T(8,128)(2,1)} %get-tuple-element.17) | copy-start | bytes 589828
  182.7 14.8 %copy-start.1 = (bf16[768,128]{1,0:T(8,128)(2,1)S(1)}, bf16[768,128]{1,0:T(8,128)(2,1)}, u32[]{:S(2)}) copy-start(bf16[768,128]{1,0:T(8,128)(2,1)} %get-tuple-element.18) | copy-start | bytes 589828
  182.8 16.8 %copy-start = (f32[2]{0:T(128)S(1)}, f32[2]{0:T(128)}, u32[]{:S(2)}) copy-start(f32[2]{0:T(128)} %param.25) | copy-start | bytes 28
  182.8 54.8 %all-to-all-start = ((bf16[8,2,256,512]{3,2,1,0:T(8,128)(2,1)}), bf16[8,2,256,512]{3,2,1,0:T(8,128)(2,1)}, u32[]{:S(2)}, u32[]{:S(2)}) async-start(bf16[8,2,256,512]{3,2,1,0:T(8,128)(2,1)} %column_blocks.1), calls=%async_computation | async-start | bytes 8388608 | tf_op jit(solution)/shard_map/all_to_all | solution.py:512
  188.8 107.7 %all-gather.13.cloned.1.call-start = ((), (), s32[]{:S(2)}) async-start(), calls=%async_computation.4 | async-start | bytes 3538944 | tf_op jit(solution)/shard_map/all_gather | solution.py:544
  188.8 13.3 %collective-permute-start.1 = (bf16[768,128]{1,0:T(8,128)(2,1)S(1)}, bf16[768,128]{1,0:T(8,128)(2,1)S(1)}, u32[]{:S(2)}, u32[]{:S(2)}) collective-permute-start(bf16[768,128]{1,0:T(8,128)(2,1)S(1)} %copy-done.2), channel_id=1, source_target_pairs={{0,0},{1,64},{32,1},{33,65},{64,33},{65,97},{96,32},{97,96},{2,2},... | collective-permute-start | bytes 589832 | tf_op jit(solution)/shard_map/ppermute | solution.py:503
  197.5 8.5 %collective-permute-start.2 = (bf16[768,128]{1,0:T(8,128)(2,1)S(1)}, bf16[768,128]{1,0:T(8,128)(2,1)S(1)}, u32[]{:S(2)}, u32[]{:S(2)}) collective-permute-start(bf16[768,128]{1,0:T(8,128)(2,1)S(1)} %copy-done.1), channel_id=1, source_target_pairs={{0,32},{1,96},{32,33},{33,97},{64,1},{65,65},{96,0},{97,64},{2,34}... | collective-permute-start | bytes 589832 | tf_op jit(solution)/shard_map/ppermute | solution.py:504
  199.6 1.4 collective-permute-start
  202.2 3.8 %copy-start.3 = (bf16[768,128]{1,0:T(8,128)(2,1)}, bf16[768,128]{1,0:T(8,128)(2,1)S(1)}, u32[]{:S(2)}) copy-start(bf16[768,128]{1,0:T(8,128)(2,1)S(1)} %collective-permute-done.1.qa_ref) | copy-start | bytes 589828
  206.0 0.7 copy-start.4
  244.7 19.2 %collective-permute-start.6 = (bf16[768,128]{1,0:T(8,128)(2,1)}, bf16[768,128]{1,0:T(8,128)(2,1)S(1)}, u32[]{:S(2)}, u32[]{:S(2)}) collective-permute-start(bf16[768,128]{1,0:T(8,128)(2,1)} %get-tuple-element.25), channel_id=1, source_target_pairs={{0,0},{64,1},{1,32},{65,33},{33,64},{97,65},{32,96},{96,97},{2,2},... | collective-permute-start | bytes 589832 | tf_op jit(solution)/shard_map/ppermute | solution.py:542
  257.9 8.4 %collective-permute-start.7 = (bf16[768,128]{1,0:T(8,128)(2,1)}, bf16[768,128]{1,0:T(8,128)(2,1)S(1)}, u32[]{:S(2)}, u32[]{:S(2)}) collective-permute-start(bf16[768,128]{1,0:T(8,128)(2,1)} %get-tuple-element.26), channel_id=1, source_target_pairs={{32,0},{96,1},{33,32},{97,33},{1,64},{65,65},{0,96},{64,97},{34,2}... | collective-permute-start | bytes 589832 | tf_op jit(solution)/shard_map/ppermute | solution.py:543
  301.8 8.3 %all-to-all-start.1 = ((f32[8,2,768]{2,1,0:T(2,128)}), f32[8,2,768]{2,1,0:T(2,128)S(1)}, u32[]{:S(2)}, u32[]{:S(2)}) async-start(f32[8,2,768]{2,1,0:T(2,128)} %get-tuple-element.28), calls=%async_computation.1 | async-start | bytes 98304 | tf_op jit(solution)/shard_map/all_to_all | solution.py:547
Sparse Core Ops, SparseCore 0:
  36.0 29.6 all-gather.10
  67.4 27.5 all-gather.8
  96.8 27.6 all-gather.14
  267.2 29.2 all-gather.12
where the time goes:
time: 320 us; the launch traced here: 319 us
  Pallas kernels  193 us (60%)
  waiting for transfers between devices  53 us (17%)
  starting transfers between devices  50.3 us (16%)
  between operations  13.3 us (4%)
  other arithmetic  5.6 us (2%)
  local copies, waits for them, and re-layouts  4.24 us (1%)
    pallas_call x1, Pallas kernels, column_blocks(): pl.pallas_call(column_kernel, out_shape=jax.ShapeDtypeStruct((8, 2, 256,...  128 us
    pallas_call x2, Pallas kernels, attention_call(): pl.pallas_call(kernel, out_shape=outs, grid_spec=pltpu.PrefetchScalarGrid...  32.8 us
    all_gather x1, waiting for transfers between devices, per_device(): lax.all_gather(jnp.concatenate([back_a, back_b], axis=1), ('y', 'c'), axi...  23.8 us
    ppermute x1, starting transfers between devices, per_device(): back_a = lax.ppermute(o_a, z_core, reverse(route_a))  13.2 us
    pallas_call x1, Pallas kernels, gated_conv(): pl.pallas_call(conv_kernel, out_shape=jax.ShapeDtypeStruct((ROWS, 256), j...  10.6 us
    pallas_call x1, Pallas kernels, project_qkv(): pl.pallas_call(qkv_kernel, out_shape=tuple((jax.ShapeDtypeStruct((ROWS, w...  10.1 us
    ppermute x1, starting transfers between devices, per_device(): q_a = lax.ppermute(q_a, z_core, route_a)  8.65 us
    ppermute x1, starting transfers between devices, per_device(): kv_b = lax.ppermute(kv_b, z_core, route_b)  7.04 us
  transfers between devices with their start and end apart: 14, of which 11 were waited for; matrix products, arithmetic and copies ran while one was open for 1% of the time, Pallas kernels for 56%

commit v1 on v0

--- a/solution.py
+++ b/solution.py
@@ -12,6 +12,7 @@
 VD = 128
 ROWS = 768
 HALO = 16
+LOG2E = 1.4426950408889634
 
 CORE_OF_Z = (0, 1, 1, 0)
 
@@ -29,7 +30,7 @@
     return [(b, a) for a, b in route]
 
 
-GROUP = 64
+GROUP = 96
 
 
 def rotary_tables():
@@ -80,14 +81,7 @@
     lax.fori_loop(0, STEPS, step, 0)
 
 
-def qkv_kernel(
-    first, h_ref, wk_ref, wv_ref, wq_ref, cr, sr, cs, ss, qa_ref, qb_ref, kva_ref, kvb_ref, acc, hb, kb, vb, qb, sem
-):
-    streamed_products(
-        ((h_ref, hb, True), (wk_ref, kb, False), (wv_ref, vb, False), (wq_ref, qb, False)),
-        sem,
-        ((acc, hb, (kb, vb, qb)),),
-    )
+def rotation(cr, sr, cs, ss):
     groups = range(ROWS // GROUP)
     cosine = jnp.concatenate(
         [cs[g : g + 1] * cr[...] - ss[g : g + 1] * sr[...] for g in groups], axis=0
@@ -101,16 +95,37 @@
     def rotated(x):
         x = x.astype(jnp.bfloat16).astype(jnp.float32)
         swapped = jnp.where(upper, -pltpu.roll(x, 128 - QK // 2, 1), pltpu.roll(x, QK // 2, 1))
-        return (x * cosine + swapped * sine).astype(jnp.bfloat16)
-
-    keys = [rotated(acc[0, :, i * 128 : i * 128 + 128]) for i in range(2)]
+        return x * cosine + swapped * sine
+
+    return rotated
+
+
+def kv_kernel(
+    where, h_ref, wk_ref, wv_ref, cr, sr, cs, ss, kva_ref, kvb_ref, acc, hb, kb, vb, sem
+):
+    streamed_products(
+        ((h_ref, hb, True), (wk_ref, kb, False), (wv_ref, vb, False)),
+        sem,
+        ((acc, hb, (kb, vb)),),
+    )
+    rotated = rotation(cr, sr, cs, ss)
+    keys = [rotated(acc[0, :, i * 128 : i * 128 + 128]).astype(jnp.bfloat16) for i in range(2)]
     vals = [acc[1, :, i * 128 : i * 128 + 128].astype(jnp.bfloat16) for i in range(2)]
-    queries = [rotated(acc[2, :, i * 128 : i * 128 + 128]) for i in range(2)]
-    for flip, q_ref, kv_ref in ((0, qa_ref, kva_ref), (1, qb_ref, kvb_ref)):
-        take = first[0] == flip
+    for flip, kv_ref in ((0, kva_ref), (1, kvb_ref)):
+        take = where[1] == flip
         kv_ref[:, 0:128] = jnp.where(take, keys[0], keys[1])
         kv_ref[:, 128:256] = jnp.where(take, vals[0], vals[1])
-        q_ref[...] = jnp.where(take, queries[0], queries[1])
+
+
+def q_kernel(where, h_ref, wq_ref, cr, sr, cs, ss, _, qa_ref, qb_ref, acc, hb, qb, sem):
+    streamed_products(((h_ref, hb, True), (wq_ref, qb, False)), sem, ((acc, hb, (qb,)),))
+    rotated = rotation(cr, sr, cs, ss)
+    queries = [
+        (rotated(acc[0, :, i * 128 : i * 128 + 128]) * (LOG2E / 8)).astype(jnp.bfloat16)
+        for i in range(2)
+    ]
+    for flip, q_ref in ((0, qa_ref), (1, qb_ref)):
+        q_ref[...] = jnp.where(where[1] == flip, queries[0], queries[1])
 
 
 def in_hbm():
@@ -128,30 +143,34 @@
     )
 
 
-def project_qkv(first, hidden, w_query, w_key, w_value, start_cos, start_sin):
-    row_cos, row_sin, _, _ = rotary_tables()
+def project(kernel, width, where, hidden, weights, unread=()):
+    row_cos, row_sin, start_cos, start_sin = rotary_tables()
     table = pl.BlockSpec((GROUP, 128), lambda k, *_: (0, 0))
-    one = pl.BlockSpec((ROWS // GROUP, 128), lambda k, *_: (0, 0))
+    starts = pl.BlockSpec((ROWS // GROUP, 128), lambda k, where: (where[0], 0))
+    out = jax.ShapeDtypeStruct((ROWS, width), jnp.bfloat16)
+    count = len(weights)
     return pl.pallas_call(
-        qkv_kernel,
-        out_shape=tuple(
-            jax.ShapeDtypeStruct((ROWS, width), jnp.bfloat16) for width in (128, 128, 256, 256)
-        ),
+        kernel,
+        out_shape=(out, out),
         grid_spec=pltpu.PrefetchScalarGridSpec(
             num_scalar_prefetch=1,
             grid=(1,),
-            in_specs=[in_hbm(), in_hbm(), in_hbm(), in_hbm(), table, table, one, one],
-            out_specs=tuple(
-                pl.BlockSpec((ROWS, width), lambda k, *_: (0, 0)) for width in (128, 128, 256, 256)
-            ),
-            scratch_shapes=[pltpu.VMEM((3, ROWS, 256), jnp.float32), *stream_buffers(3, False)],
+            in_specs=[in_hbm()] * (1 + count)
+            + [table, table, starts, starts]
+            + [in_hbm()] * len(unread),
+            out_specs=(pl.BlockSpec((ROWS, width), lambda k, *_: (0, 0)),) * 2,
+            scratch_shapes=[
+                pltpu.VMEM((count, ROWS, 256), jnp.float32),
+                *stream_buffers(count, False),
+            ],
         ),
         compiler_params=pltpu.CompilerParams(vmem_limit_bytes=60 * 2**20),
         cost_estimate=pl.CostEstimate(
-            flops=2 * ROWS * D * 768, bytes_accessed=13 * 2**20, transcendentals=0
-        ),
-        name="qkv",
-    )(first, hidden, w_key, w_value, w_query, row_cos, row_sin, start_cos, start_sin)
+            flops=2 * ROWS * D * 256 * count,
+            bytes_accessed=(6 + 2 * count) * 2**20,
+            transcendentals=0,
+        ),
+    )(where, hidden, *weights, row_cos, row_sin, start_cos, start_sin, *unread)
 
 
 def conv_kernel(
@@ -214,7 +233,6 @@
 
 def split_maps(q, qz):
     lane = lax.broadcasted_iota(jnp.int32, (ROWS, 128), 1)
-    q = q * jnp.bfloat16(0.125)
     qz[0] = jnp.where(lane < QK, q, jnp.zeros_like(q))
     qz[1] = jnp.where(lane >= QK, q, jnp.zeros_like(q))
 
@@ -241,8 +259,8 @@
         s = jnp.where(k <= r, s, -1e30)
     m_old = m_s[:, rows, :]
     m_new = jnp.maximum(m_old, jnp.max(s, axis=2, keepdims=True))
-    alpha = jnp.exp(m_old - m_new)
-    p = jnp.exp(s - jnp.tile(m_new, (1, 1, width // 128)))
+    alpha = jnp.exp2(m_old - m_new)
+    p = jnp.exp2(s - jnp.tile(m_new, (1, 1, width // 128)))
     part = p[:, :, 0:128]
     for w in range(1, width // 128):
         part = part + p[:, :, w * 128 : (w + 1) * 128]
@@ -340,19 +358,26 @@
     )(*args, *unread)
 
 
-def column_kernel(wc_ref, wa_ref, o_ref, sem):
+def column_kernel(wc_ref, wa_ref, o_ref, buf, sem):
     width = o_ref.shape[3]
-    copies = [
-        pltpu.make_async_copy(
-            w_ref.at[:, pl.ds(t * width, width)], o_ref.at[t, i], sem.at[i, t]
-        )
+    loads = [
+        pltpu.make_async_copy(w_ref, buf.at[i], sem.at[i, 8])
         for i, w_ref in enumerate((wc_ref, wa_ref))
-        for t in range(8)
     ]
-    for copy in copies:
-        copy.start()
-    for copy in copies:
-        copy.wait()
+    for load in loads:
+        load.start()
+    stores = []
+    for i in range(2):
+        loads[i].wait()
+        for t in range(8):
+            stores.append(
+                pltpu.make_async_copy(
+                    buf.at[i, :, pl.ds(t * width, width)], o_ref.at[t, i], sem.at[i, t]
+                )
+            )
+            stores[-1].start()
+    for store in stores:
+        store.wait()
 
 
 def column_blocks(w_conv, w_attn):
@@ -361,7 +386,11 @@
         out_shape=jax.ShapeDtypeStruct((8, 2, 256, D // 8), jnp.bfloat16),
         in_specs=[in_hbm(), in_hbm()],
         out_specs=in_hbm(),
-        scratch_shapes=[pltpu.SemaphoreType.DMA((2, 8))],
+        scratch_shapes=[pltpu.VMEM((2, 256, D), jnp.bfloat16), pltpu.SemaphoreType.DMA((2, 9))],
+        compiler_params=pltpu.CompilerParams(vmem_limit_bytes=60 * 2**20),
+        cost_estimate=pl.CostEstimate(
+            flops=3 * 10**9, bytes_accessed=9 * 2**20, transcendentals=0
+        ),
         name="column_blocks",
     )(w_conv, w_attn)
 
@@ -404,9 +433,11 @@
     def row_sums(values):
         return lax.dot_general(
             ones, values, (((1,), (1,)), ((), ())), preferred_element_type=jnp.float32
-        )[0:1]
-
-    sums = jnp.concatenate([row_sums(mix), row_sums(high) + row_sums(low)], axis=0)
+        )
+
+    row = lax.broadcasted_iota(jnp.int32, (8, ROWS), 0)
+    squares = jnp.where(row == 1, row_sums(high) + row_sums(low), 0.0)
+    sums = jnp.where(row == 0, row_sums(mix), squares)
     for copy in range(8):
         sums_ref[copy] = sums
 
@@ -436,7 +467,7 @@
         whole_last_kernel,
         out_shape=(
             jax.ShapeDtypeStruct((ROWS, width), jnp.bfloat16),
-            jax.ShapeDtypeStruct((8, 2, ROWS), jnp.float32),
+            jax.ShapeDtypeStruct((8, 8, ROWS), jnp.float32),
         ),
         grid_spec=pltpu.PrefetchScalarGridSpec(
             num_scalar_prefetch=1,
@@ -444,7 +475,7 @@
             in_specs=[in_hbm(), in_hbm(), in_hbm()],
             out_specs=(
                 pl.BlockSpec((ROWS, width), lambda i, *_: (0, 0)),
-                pl.BlockSpec((8, 2, ROWS), lambda i, *_: (0, 0, 0)),
+                pl.BlockSpec((8, 8, ROWS), lambda i, *_: (0, 0, 0)),
             ),
             scratch_shapes=[
                 pltpu.VMEM((8, ROWS, 256), jnp.bfloat16),
@@ -459,6 +490,50 @@
         ),
         name="whole_last",
     )(first, gathered, weights, before)
+
+
+def norm_kernel(own, mix_ref, sums_ref, gain_ref, o_ref):
+    sums = sums_ref[...].reshape(64, ROWS)
+    row = lax.broadcasted_iota(jnp.int32, (64, 128), 0) % 8
+
+    def column(which):
+        total = lax.dot_general(
+            sums,
+            jnp.where(row == which, 1.0, 0.0),
+            (((0,), (0,)), ((), ())),
+            preferred_element_type=jnp.float32,
+            precision=lax.Precision.HIGHEST,
+        )
+        return total * (1.0 / D)
+
+    mean = column(0)
+    variance = column(1) - mean * mean
+    scale = lax.rsqrt(variance + 1e-5)
+    gain = gain_ref[...].astype(jnp.float32)
+    for at in range(0, mix_ref.shape[1], 128):
+        mix = mix_ref[:, at : at + 128].astype(jnp.float32)
+        o_ref[:, at : at + 128] = ((mix - mean) * scale * gain[:, at : at + 128]).astype(
+            jnp.bfloat16
+        )
+
+
+def layer_norm(own, mix, sums, gain):
+    width = mix.shape[1]
+    return pl.pallas_call(
+        norm_kernel,
+        out_shape=jax.ShapeDtypeStruct(mix.shape, jnp.bfloat16),
+        grid_spec=pltpu.PrefetchScalarGridSpec(
+            num_scalar_prefetch=1,
+            grid=(1,),
+            in_specs=[
+                pl.BlockSpec(mix.shape, lambda i, *_: (0, 0)),
+                pl.BlockSpec(sums.shape, lambda i, *_: (0, 0, 0)),
+                pl.BlockSpec((1, width), lambda i, own: (0, own[0])),
+            ],
+            out_specs=pl.BlockSpec(mix.shape, lambda i, *_: (0, 0)),
+        ),
+        name="norm",
+    )(own, mix, sums, gain)
 
 
 def per_device(
@@ -486,31 +561,25 @@
     other_lambdas = lax.ppermute(lambdas, "c", [(0, 1), (1, 0)])
 
     first = jnp.where(z < 2, 0, 1).astype(jnp.int32).reshape(1)
-    _, _, start_cos, start_sin = rotary_tables()
-    groups = ROWS // GROUP
-    q_a, q_b, kv_a, kv_b = project_qkv(
-        first,
-        hidden_states,
-        w_query,
-        w_key,
-        w_value,
-        lax.dynamic_slice_in_dim(jnp.asarray(start_cos), sp * groups, groups, 0),
-        lax.dynamic_slice_in_dim(jnp.asarray(start_sin), sp * groups, groups, 0),
-    )
+    where = jnp.stack([sp, jnp.where(z < 2, 0, 1)]).astype(jnp.int32)
     route_a, route_b = forward_route(0), forward_route(1)
+    kv_a, kv_b = project(kv_kernel, 256, where, hidden_states, (w_key, w_value))
+    blocks = column_blocks(w_out_conv, w_out_attn)
+    q_a, q_b = project(q_kernel, 128, where, hidden_states, (w_query,), (kv_a,))
     kv_a = lax.ppermute(kv_a, z_core, route_a)
     kv_b = lax.ppermute(kv_b, z_core, route_b)
     q_a = lax.ppermute(q_a, z_core, route_a)
     q_b = lax.ppermute(q_b, z_core, route_b)
     even = (z % 2) == 0
-    kv_low = lax.all_gather(jnp.where(even, kv_a, kv_b), ("x", "c"), axis=0)
-    kv_high = lax.all_gather(jnp.where(even, kv_b, kv_a), ("x", "c"), axis=0)
+    kv_low, kv_high = jnp.where(even, kv_a, kv_b), jnp.where(even, kv_b, kv_a)
+    kv_low = lax.all_gather(kv_low, ("x", "c"), axis=0)
+    kv_high = lax.all_gather(kv_high, ("x", "c"), axis=0)
 
     conv_out = gated_conv(hidden_states, rim, w_conv_b, w_conv_c, w_conv_h, conv_taps)
     conv_all = lax.all_gather(conv_out, ("y", "c"), axis=0)
 
     w_out = lax.all_to_all(
-        column_blocks(w_out_conv, w_out_attn),
+        blocks,
         ("y", "c"),
         split_axis=0,
         concat_axis=0,
@@ -545,16 +614,8 @@
     conv_part = whole_conv(conv_all, w_out)
     mix, sums = whole_last(first, attn_all, w_out, conv_part)
     everything = lax.all_to_all(sums, ("y", "c"), split_axis=0, concat_axis=0, tiled=True)
-    totals = jnp.sum(everything, axis=0)
-    mix_f = mix.astype(jnp.float32)
-    width = mix_f.shape[1]
-    mean_value = (totals[0] / D)[:, None]
-    variance = (totals[1] / D)[:, None] - mean_value * mean_value
-    tp = lax.axis_index("y") * 2 + core
-    own_gain = lax.dynamic_slice_in_dim(out_gain.astype(jnp.float32), tp * width, width, 0)
-    return ((mix_f - mean_value) * lax.rsqrt(variance + 1e-05) * own_gain[None, :]).astype(
-        jnp.bfloat16
-    )
+    tp = (lax.axis_index("y") * 2 + core).astype(jnp.int32).reshape(1)
+    return layer_norm(tp, mix, everything, out_gain.reshape(1, D))
 
 
 def solution(mesh):

time: 320 us -> 201 us (0.63)
  Pallas kernels: 193 us -> 75.1 us
    pallas_call x1, Pallas kernels: 128 us -> 3.82 us  [column_blocks(): pl.pallas_call(column_kernel, out_shape=jax.ShapeDtypeStruct((8, 2, 256,...]
    ppermute x1, starting transfers between devices: 13.2 us -> 4.14 us  [per_device(): back_a = lax.ppermute(o_a, z_core, reverse(route_a))]
    pallas_call x1 -> x3, Pallas kernels: 10.1 us -> 18.5 us  [the longest x2 15.3 us: project(): pl.pallas_call(kernel, out_shape=(out, out), grid_spec=pltpu.PrefetchScal...]
    ppermute x1, starting transfers between devices: 4.32 us -> 11.9 us  [per_device(): back_b = lax.ppermute(o_b, z_core, reverse(route_b))]
    ppermute x1, waiting for transfers between devices: 0.96 us -> 6.04 us  [per_device(): kv_a = lax.ppermute(kv_a, z_core, route_a)]
    ppermute x1, starting transfers between devices: 1.92 us -> 6.88 us  [per_device(): kv_a = lax.ppermute(kv_a, z_core, route_a)]
    ppermute x1, starting transfers between devices: 7.04 us -> 2.62 us  [per_device(): kv_b = lax.ppermute(kv_b, z_core, route_b)]
    ppermute x1, waiting for transfers between devices: 2.46 us -> 6.66 us  [per_device(): back_b = lax.ppermute(o_b, z_core, reverse(route_b))]
  transfers between devices with their start and end apart: 14 -> 14, of which waited for: 11 -> 8; matrix products, arithmetic and copies ran while one was open for 1% -> 2% of each run, Pallas kernels for 56% -> 29%
where the time goes in v1:
time: 201 us; the launch traced here: 200 us
  Pallas kernels  75.1 us (37%)
  waiting for transfers between devices  55 us (27%)
  starting transfers between devices  49.5 us (25%)
  between operations  13.3 us (7%)
  local copies, waits for them, and re-layouts  4.17 us (2%)
  other arithmetic  2.93 us (1%)
    pallas_call x2, Pallas kernels, attention_call(): pl.pallas_call(kernel, out_shape=outs, grid_spec=pltpu.PrefetchScalarGrid...  31.3 us
    all_gather x1, waiting for transfers between devices, per_device(): lax.all_gather(jnp.concatenate([back_a, back_b], axis=1), ('y', 'c'), axi...  22.5 us
    pallas_call x2, Pallas kernels, project(): pl.pallas_call(kernel, out_shape=(out, out), grid_spec=pltpu.PrefetchScal...  15.3 us
    ppermute x1, starting transfers between devices, per_device(): back_b = lax.ppermute(o_b, z_core, reverse(route_b))  11.9 us
    pallas_call x1, Pallas kernels, gated_conv(): pl.pallas_call(conv_kernel, out_shape=jax.ShapeDtypeStruct((ROWS, 256), j...  10.6 us
    all_to_all x1, starting transfers between devices, per_device(): lax.all_to_all(blocks, ('y', 'c'), split_axis=0, concat_axis=0, tiled=True)  7.02 us
    ppermute x1, starting transfers between devices, per_device(): kv_a = lax.ppermute(kv_a, z_core, route_a)  6.88 us
    ppermute x1, waiting for transfers between devices, per_device(): back_b = lax.ppermute(o_b, z_core, reverse(route_b))  6.66 us
  transfers between devices with their start and end apart: 14, of which 8 were waited for; matrix products, arithmetic and copies ran while one was open for 2% of the time, Pallas kernels for 29%

profile of v1, /device:TPU:1, one launch (start us, length us, event | category | flops | bytes accessed | tf_op | source)
XLA Modules:
  0.0 200.0 jit_solution(2318255081514432609)
XLA Ops:
  6.5 0.6 pad_add_fusion.1.where
  7.1 8.6 %shard_map.199 = (bf16[768,256]{1,0:T(8,128)(2,1)}, bf16[768,256]{1,0:T(8,128)(2,1)}) custom-call(s32[2]{0:T(128)} %pad_add_fusion.1.where, bf16[768,4096]{1,0:T(8,128)(2,1)} %h_ref.5, bf16[4096,256]{1,0:T(8,128)(2,1)} %wk_ref.1, bf16[4096,256]{1,0:T(8,128)(2,1)} %wv_ref.1, f32[96,128]{1,0:T(8,128)} %constant.44.clone.cr, f32[96,128]{1,0:T(8,128)} %constant.45.clone.sr, ...), custom_call_target="tpu_custom_call" | custom-call | flops 3221225472 | bytes 10485760 | tf_op jit(solution)/shard_map/pallas_call | solution.py:152
  15.7 6.9 %collective-permute-start.4 = (bf16[768,256]{1,0:T(8,128)(2,1)}, bf16[768,256]{1,0:T(8,128)(2,1)S(1)}, u32[]{:S(2)}, u32[]{:S(2)}) collective-permute-start(bf16[768,256]{1,0:T(8,128)(2,1)} %get-tuple-element.17._), channel_id=1, source_target_pairs={{0,0},{1,64},{32,1},{33,65},{64,33},{65,97},{96,32},{97,96},{2,2},... | collective-permute-start | bytes 1179656 | tf_op jit(solution)/shard_map/ppermute | solution.py:569
  22.6 2.6 %collective-permute-start.3 = (bf16[768,256]{1,0:T(8,128)(2,1)}, bf16[768,256]{1,0:T(8,128)(2,1)S(1)}, u32[]{:S(2)}, u32[]{:S(2)}) collective-permute-start(bf16[768,256]{1,0:T(8,128)(2,1)} %get-tuple-element.20), channel_id=1, source_target_pairs={{0,32},{1,96},{32,33},{33,97},{64,1},{65,65},{96,0},{97,64},{2,34}... | collective-permute-start | bytes 1179656 | tf_op jit(solution)/shard_map/ppermute | solution.py:570
  25.2 6.0 %collective-permute-done.4 = bf16[768,256]{1,0:T(8,128)(2,1)S(1)} collective-permute-done((bf16[768,256]{1,0:T(8,128)(2,1)}, bf16[768,256]{1,0:T(8,128)(2,1)S(1)}, u32[]{:S(2)}, u32[]{:S(2)}) %collective-permute-start.4) | collective-permute-done | bytes 393248 | tf_op jit(solution)/shard_map/ppermute | solution.py:569
  31.3 3.0 %collective-permute-done.3 = bf16[768,256]{1,0:T(8,128)(2,1)S(1)} collective-permute-done((bf16[768,256]{1,0:T(8,128)(2,1)}, bf16[768,256]{1,0:T(8,128)(2,1)S(1)}, u32[]{:S(2)}, u32[]{:S(2)}) %collective-permute-start.3) | collective-permute-done | bytes 393248 | tf_op jit(solution)/shard_map/ppermute | solution.py:570
  34.3 0.9 broadcast_select_fusion
  35.2 0.0 all-gather.11.cloned.1.call-update
  35.3 0.0 all-gather.9.cloned.1.call-start
  35.3 0.7 all-gather.9.cloned.1.call-update
  36.0 0.0 all-gather.15.cloned.1.call-start
  36.1 0.9 slice.3
  37.0 3.1 %collective-permute-start.5 = (bf16[16,4096]{1,0:T(8,128)(2,1)S(1)}, bf16[16,4096]{1,0:T(8,128)(2,1)S(1)}, u32[]{:S(2)}, u32[]{:S(2)}) collective-permute-start(bf16[16,4096]{1,0:T(8,128)(2,1)S(1)} %slice.3), channel_id=1, source_target_pairs={{0,8},{8,16},{16,24},{24,32},{32,40},{40,48},{48,56},{56,64},{64,7... | collective-permute-start | bytes 393224 | tf_op jit(solution)/shard_map/ppermute | solution.py:560
  40.1 1.9 collective-permute-done.5.rim_ref
  42.0 0.6 copy-done.5
  42.7 10.6 %gated_conv.1._ = bf16[768,256]{1,0:T(8,128)(2,1)} custom-call(bf16[768,4096]{1,0:T(8,128)(2,1)} %h_ref.5, bf16[16,4096]{1,0:T(8,128)(2,1)} %copy-done.5, bf16[4096,256]{1,0:T(8,128)(2,1)} %wb_ref.1, bf16[4096,256]{1,0:T(8,128)(2,1)} %wc_ref.2, bf16[4096,256]{1,0:T(8,128)(2,1)} %wh_ref.1, bf16[3,256]{1,0:T(4,128)(2,1)} %taps_ref.1), custom_call_target="tpu_custom_call" | custom-call | flops 4831838208 | bytes 13631488 | tf_op jit(solution)/shard_map/gated_conv/pallas_call | solution.py:204
  53.3 0.0 all-gather.15.cloned.1.call-update
  53.3 3.8 %column_blocks.1 = bf16[8,2,256,512]{3,2,1,0:T(8,128)(2,1)} custom-call(bf16[256,4096]{1,0:T(8,128)(2,1)} %wc_ref.3, bf16[256,4096]{1,0:T(8,128)(2,1)} %wa_ref.1), custom_call_target="tpu_custom_call" | custom-call | flops 3000000000 | bytes 9437184 | tf_op jit(solution)/shard_map/column_blocks/pallas_call | solution.py:384
  57.1 0.0 copy-start.2
  57.2 7.0 %all-to-all-start = ((bf16[8,2,256,512]{3,2,1,0:T(8,128)(2,1)}), bf16[8,2,256,512]{3,2,1,0:T(8,128)(2,1)}, u32[]{:S(2)}, u32[]{:S(2)}) async-start(bf16[8,2,256,512]{3,2,1,0:T(8,128)(2,1)} %column_blocks.1), calls=%async_computation | async-start | bytes 8388608 | tf_op jit(solution)/shard_map/all_to_all | solution.py:581
  64.2 0.2 collective-permute-start
  64.3 6.7 %shard_map.200 = (bf16[768,128]{1,0:T(8,128)(2,1)}, bf16[768,128]{1,0:T(8,128)(2,1)}) custom-call(s32[2]{0:T(128)} %pad_add_fusion.1.where, bf16[768,4096]{1,0:T(8,128)(2,1)} %h_ref.5, bf16[4096,256]{1,0:T(8,128)(2,1)} %wq_ref.1, f32[96,128]{1,0:T(8,128)} %constant.44.clone.cr, f32[96,128]{1,0:T(8,128)} %constant.45.clone.sr, f32[128,128]{1,0:T(8,128)} %constant.46.clone.cs, ...), custom_call_target="tpu_custom_call" | custom-call | flops 1610612736 | bytes 8388608 | tf_op jit(solution)/shard_map/pallas_call | solution.py:152
  71.1 4.8 %collective-permute-start.1 = (bf16[768,128]{1,0:T(8,128)(2,1)}, bf16[768,128]{1,0:T(8,128)(2,1)S(1)}, u32[]{:S(2)}, u32[]{:S(2)}) collective-permute-start(bf16[768,128]{1,0:T(8,128)(2,1)} %get-tuple-element.18), channel_id=1, source_target_pairs={{0,0},{1,64},{32,1},{33,65},{64,33},{65,97},{96,32},{97,96},{2,2},... | collective-permute-start | bytes 589832 | tf_op jit(solution)/shard_map/ppermute | solution.py:571
  75.9 5.1 %collective-permute-start.2 = (bf16[768,128]{1,0:T(8,128)(2,1)}, bf16[768,128]{1,0:T(8,128)(2,1)S(1)}, u32[]{:S(2)}, u32[]{:S(2)}) collective-permute-start(bf16[768,128]{1,0:T(8,128)(2,1)} %get-tuple-element.19), channel_id=1, source_target_pairs={{0,32},{1,96},{32,33},{33,97},{64,1},{65,65},{96,0},{97,64},{2,34}... | collective-permute-start | bytes 589832 | tf_op jit(solution)/shard_map/ppermute | solution.py:572
  81.0 0.6 pad_add_fusion.own
  81.6 0.0 collective-permute-done
  81.6 0.1 broadcast_select_fusion.2
  81.7 0.6 dynamic_slice.3.lam
  82.3 0.0 collective-permute-done.1.qa_ref
  82.3 3.5 %collective-permute-done.2.qb_ref = bf16[768,128]{1,0:T(8,128)(2,1)S(1)} collective-permute-done((bf16[768,128]{1,0:T(8,128)(2,1)}, bf16[768,128]{1,0:T(8,128)(2,1)S(1)}, u32[]{:S(2)}, u32[]{:S(2)}) %collective-permute-start.2) | collective-permute-done | bytes 196640 | tf_op jit(solution)/shard_map/ppermute | solution.py:572
  85.8 0.7 copy-done.4
  86.4 24.2 %shard_map.201 = (bf16[768,128]{1,0:T(8,128)(2,1)}, f32[2,768,128]{2,1,0:T(8,128)}, f32[2,768,128]{2,1,0:T(8,128)}, f32[2,768,128]{2,1,0:T(8,128)}) custom-call(s32[3]{0:T(128)} %pad_add_fusion.own, f32[1]{0:T(128)} %dynamic_slice.3.lam, bf16[768,128]{1,0:T(8,128)(2,1)} %copy-done.3, bf16[768,128]{1,0:T(8,128)(2,1)} %copy-done.4, ...), custom_call_target="tpu_custom_call" | custom-call | flops 24000000000 | bytes 4194304 | tf_op jit(solution)/shard_map/pallas_call | solution.py:344
  110.6 5.4 %all-to-all-done._.w_ref = bf16[8,2,256,512]{3,2,1,0:T(8,128)(2,1)} async-done(((bf16[8,2,256,512]{3,2,1,0:T(8,128)(2,1)}), bf16[8,2,256,512]{3,2,1,0:T(8,128)(2,1)}, u32[]{:S(2)}, u32[]{:S(2)}) %all-to-all-start) | async-done | bytes 4194336 | tf_op jit(solution)/shard_map/all_to_all | solution.py:581
  116.0 7.0 %shard_map.202 = (bf16[768,128]{1,0:T(8,128)(2,1)}, bf16[768,128]{1,0:T(8,128)(2,1)}) custom-call(s32[3]{0:T(128)} %pad_add_fusion.own, f32[1]{0:T(128)} %dynamic_slice.3.lam, bf16[768,128]{1,0:T(8,128)(2,1)} %copy-done.3, bf16[768,128]{1,0:T(8,128)(2,1)} %copy-done.4, bf16[8,768,256]{2,1,0:T(8,128)(2,1)} %bitcast.13, bf16[1,128]{1,0:T(2,128)(2,1)} %bitcast.16, ...), custom_call_target="tpu_custom_call" | custom-call | flops 12000000000 | bytes 4194304 | tf_op jit(solution)/shard_map/pallas_call | solution.py:344
  123.1 11.9 %collective-permute-start.7 = (bf16[768,128]{1,0:T(8,128)(2,1)}, bf16[768,128]{1,0:T(8,128)(2,1)S(1)}, u32[]{:S(2)}, u32[]{:S(2)}) collective-permute-start(bf16[768,128]{1,0:T(8,128)(2,1)} %get-tuple-element.26), channel_id=1, source_target_pairs={{32,0},{96,1},{33,32},{97,33},{1,64},{65,65},{0,96},{64,97},{34,2}... | collective-permute-start | bytes 589832 | tf_op jit(solution)/shard_map/ppermute | solution.py:612
  135.0 4.1 %collective-permute-start.6 = (bf16[768,128]{1,0:T(8,128)(2,1)}, bf16[768,128]{1,0:T(8,128)(2,1)S(1)}, u32[]{:S(2)}, u32[]{:S(2)}) collective-permute-start(bf16[768,128]{1,0:T(8,128)(2,1)} %get-tuple-element.25), channel_id=1, source_target_pairs={{0,0},{64,1},{1,32},{65,33},{33,64},{97,65},{32,96},{96,97},{2,2},... | collective-permute-start | bytes 589832 | tf_op jit(solution)/shard_map/ppermute | solution.py:611
  139.2 6.7 %collective-permute-done.7 = bf16[768,128]{1,0:T(8,128)(2,1)S(1)} collective-permute-done((bf16[768,128]{1,0:T(8,128)(2,1)}, bf16[768,128]{1,0:T(8,128)(2,1)S(1)}, u32[]{:S(2)}, u32[]{:S(2)}) %collective-permute-start.7) | collective-permute-done | bytes 196640 | tf_op jit(solution)/shard_map/ppermute | solution.py:612
  145.8 0.8 pad_maximum_fusion
  146.6 0.0 all-gather.13.cloned.1.call-update
  146.6 0.0 all-gather.15.cloned.1.call-done
  146.7 5.6 %whole_conv.1.before_ref = f32[768,512]{1,0:T(8,128)} custom-call(bf16[8,768,256]{2,1,0:T(8,128)(2,1)} %bitcast.11, bf16[8,2,256,512]{3,2,1,0:T(8,128)(2,1)} %all-to-all-done._.w_ref), custom_call_target="tpu_custom_call" | custom-call | flops 1610612736 | bytes 7340032 | tf_op jit(solution)/shard_map/whole_conv/pallas_call | solution.py:447
  152.2 22.5 %all-gather.13.cloned.1.call-done = bf16[6144,256]{1,0:T(8,128)(2,1)} async-done(((bf16[768,256]{1,0:T(8,128)(2,1)}), bf16[6144,256]{1,0:T(8,128)(2,1)}) %all-gather.13.cloned.1.call-update) | async-done | bytes 3145744 | tf_op jit(solution)/shard_map/all_gather | solution.py:613
  174.7 5.3 %whole_last.1 = (bf16[768,512]{1,0:T(8,128)(2,1)}, f32[8,8,768]{2,1,0:T(8,128)}) custom-call(s32[1]{0:T(128)} %bitcast.1.first, bf16[8,768,256]{2,1,0:T(8,128)(2,1)} %bitcast.12, bf16[8,2,256,512]{3,2,1,0:T(8,128)(2,1)} %all-to-all-done._.w_ref, f32[768,512]{1,0:T(8,128)} %whole_conv.1.before_ref), custom_call_target="tpu_custom_call" | custom-call | flops 1610612736 | bytes 7340032 | tf_op jit(solution)/shard_map/whole_last/pallas_call | solution.py:466
  180.1 3.6 %all-to-all-start.1 = ((f32[8,8,768]{2,1,0:T(8,128)}), f32[8,8,768]{2,1,0:T(8,128)S(1)}, u32[]{:S(2)}, u32[]{:S(2)}) async-start(f32[8,8,768]{2,1,0:T(8,128)} %get-tuple-element.28), calls=%async_computation.1 | async-start | bytes 393216 | tf_op jit(solution)/shard_map/all_to_all | solution.py:616
  183.6 0.6 reshape.15.gain_ref
  184.3 5.3 %all-to-all-done.1.sums_ref = f32[8,8,768]{2,1,0:T(8,128)S(1)} async-done(((f32[8,8,768]{2,1,0:T(8,128)}), f32[8,8,768]{2,1,0:T(8,128)S(1)}, u32[]{:S(2)}, u32[]{:S(2)}) %all-to-all-start.1) | async-done | bytes 196640 | tf_op jit(solution)/shard_map/all_to_all | solution.py:616
  189.5 0.7 copy-done
  190.2 3.2 %norm.1 = bf16[768,512]{1,0:T(8,128)(2,1)} custom-call(s32[1]{0:T(128)} %bitcast.own, bf16[768,512]{1,0:T(8,128)(2,1)} %get-tuple-element.27.mix_ref, f32[8,8,768]{2,1,0:T(8,128)} %copy-done, bf16[1,4096]{1,0:T(2,128)(2,1)} %reshape.15.gain_ref), custom_call_target="tpu_custom_call" | custom-call | tf_op jit(solution)/shard_map/norm/pallas_call | solution.py:522
  (13 shorter events, 0.0 us)
Async XLA Ops:
  6.5 79.2 %all-gather.11.cloned.1.call-start = ((), (), s32[]{:S(2)}) async-start(), calls=%async_computation.3 | async-start | bytes 3538944 | tf_op jit(solution)/shard_map/all_gather | solution.py:575
  15.7 15.6 %collective-permute-start.4 = (bf16[768,256]{1,0:T(8,128)(2,1)}, bf16[768,256]{1,0:T(8,128)(2,1)S(1)}, u32[]{:S(2)}, u32[]{:S(2)}) collective-permute-start(bf16[768,256]{1,0:T(8,128)(2,1)} %get-tuple-element.17._), channel_id=1, source_target_pairs={{0,0},{1,64},{32,1},{33,65},{64,33},{65,97},{96,32},{97,96},{2,2},... | collective-permute-start | bytes 1179656 | tf_op jit(solution)/shard_map/ppermute | solution.py:569
  22.6 11.7 %collective-permute-start.3 = (bf16[768,256]{1,0:T(8,128)(2,1)}, bf16[768,256]{1,0:T(8,128)(2,1)S(1)}, u32[]{:S(2)}, u32[]{:S(2)}) collective-permute-start(bf16[768,256]{1,0:T(8,128)(2,1)} %get-tuple-element.20), channel_id=1, source_target_pairs={{0,32},{1,96},{32,33},{33,97},{64,1},{65,65},{96,0},{97,64},{2,34}... | collective-permute-start | bytes 1179656 | tf_op jit(solution)/shard_map/ppermute | solution.py:570
  35.3 80.8 %all-gather.9.cloned.1.call-start = ((), (), s32[]{:S(2)}) async-start(), calls=%async_computation.2 | async-start | bytes 3538944 | tf_op jit(solution)/shard_map/all_gather | solution.py:576
  36.0 110.6 %all-gather.15.cloned.1.call-start = ((), (), s32[]{:S(2)}) async-start(), calls=%async_computation.5 | async-start | bytes 3538944 | tf_op jit(solution)/shard_map/all_gather | solution.py:579
  37.0 5.1 %collective-permute-start.5 = (bf16[16,4096]{1,0:T(8,128)(2,1)S(1)}, bf16[16,4096]{1,0:T(8,128)(2,1)S(1)}, u32[]{:S(2)}, u32[]{:S(2)}) collective-permute-start(bf16[16,4096]{1,0:T(8,128)(2,1)S(1)} %slice.3), channel_id=1, source_target_pairs={{0,8},{8,16},{16,24},{24,32},{32,40},{40,48},{48,56},{56,64},{64,7... | collective-permute-start | bytes 393224 | tf_op jit(solution)/shard_map/ppermute | solution.py:560
  42.0 0.7 copy-start.5
  57.1 7.0 %copy-start.2 = (f32[2]{0:T(128)S(1)}, f32[2]{0:T(128)}, u32[]{:S(2)}) copy-start(f32[2]{0:T(128)} %param.29) | copy-start | bytes 28
  57.2 58.8 %all-to-all-start = ((bf16[8,2,256,512]{3,2,1,0:T(8,128)(2,1)}), bf16[8,2,256,512]{3,2,1,0:T(8,128)(2,1)}, u32[]{:S(2)}, u32[]{:S(2)}) async-start(bf16[8,2,256,512]{3,2,1,0:T(8,128)(2,1)} %column_blocks.1), calls=%async_computation | async-start | bytes 8388608 | tf_op jit(solution)/shard_map/all_to_all | solution.py:581
  64.2 110.5 %all-gather.13.cloned.1.call-start = ((), (), s32[]{:S(2)}) async-start(), calls=%async_computation.4 | async-start | bytes 3538944 | tf_op jit(solution)/shard_map/all_gather | solution.py:613
  64.2 17.4 %collective-permute-start = (f32[2]{0:T(128)S(1)}, f32[2]{0:T(128)S(1)}, u32[]{:S(2)}, u32[]{:S(2)}) collective-permute-start(f32[2]{0:T(128)S(1)} %copy-done.2), channel_id=1, source_target_pairs={{0,1},{1,0},{2,3},{3,2},{4,5},{5,4},{6,7},{7,6},{8,9},{9,8},{10,11... | collective-permute-start | bytes 32 | tf_op jit(solution)/shard_map/ppermute | solution.py:561
  71.1 11.2 %collective-permute-start.1 = (bf16[768,128]{1,0:T(8,128)(2,1)}, bf16[768,128]{1,0:T(8,128)(2,1)S(1)}, u32[]{:S(2)}, u32[]{:S(2)}) collective-permute-start(bf16[768,128]{1,0:T(8,128)(2,1)} %get-tuple-element.18), channel_id=1, source_target_pairs={{0,0},{1,64},{32,1},{33,65},{64,33},{65,97},{96,32},{97,96},{2,2},... | collective-permute-start | bytes 589832 | tf_op jit(solution)/shard_map/ppermute | solution.py:571
  75.9 9.9 %collective-permute-start.2 = (bf16[768,128]{1,0:T(8,128)(2,1)}, bf16[768,128]{1,0:T(8,128)(2,1)S(1)}, u32[]{:S(2)}, u32[]{:S(2)}) collective-permute-start(bf16[768,128]{1,0:T(8,128)(2,1)} %get-tuple-element.19), channel_id=1, source_target_pairs={{0,32},{1,96},{32,33},{33,97},{64,1},{65,65},{96,0},{97,64},{2,34}... | collective-permute-start | bytes 589832 | tf_op jit(solution)/shard_map/ppermute | solution.py:572
  82.3 3.5 %copy-start.3 = (bf16[768,128]{1,0:T(8,128)(2,1)}, bf16[768,128]{1,0:T(8,128)(2,1)S(1)}, u32[]{:S(2)}) copy-start(bf16[768,128]{1,0:T(8,128)(2,1)S(1)} %collective-permute-done.1.qa_ref) | copy-start | bytes 589828
  85.7 0.7 copy-start.4
  123.1 22.8 %collective-permute-start.7 = (bf16[768,128]{1,0:T(8,128)(2,1)}, bf16[768,128]{1,0:T(8,128)(2,1)S(1)}, u32[]{:S(2)}, u32[]{:S(2)}) collective-permute-start(bf16[768,128]{1,0:T(8,128)(2,1)} %get-tuple-element.26), channel_id=1, source_target_pairs={{32,0},{96,1},{33,32},{97,33},{1,64},{65,65},{0,96},{64,97},{34,2}... | collective-permute-start | bytes 589832 | tf_op jit(solution)/shard_map/ppermute | solution.py:612
  135.0 10.8 %collective-permute-start.6 = (bf16[768,128]{1,0:T(8,128)(2,1)}, bf16[768,128]{1,0:T(8,128)(2,1)S(1)}, u32[]{:S(2)}, u32[]{:S(2)}) collective-permute-start(bf16[768,128]{1,0:T(8,128)(2,1)} %get-tuple-element.25), channel_id=1, source_target_pairs={{0,0},{64,1},{1,32},{65,33},{33,64},{97,65},{32,96},{96,97},{2,2},... | collective-permute-start | bytes 589832 | tf_op jit(solution)/shard_map/ppermute | solution.py:611
  174.7 8.9 %copy-start.1 = (bf16[4096]{0:T(1024)(128)(2,1)S(1)}, bf16[4096]{0:T(1024)(128)(2,1)}, u32[]{:S(2)}) copy-start(bf16[4096]{0:T(1024)(128)(2,1)} %param.33) | copy-start | bytes 24580
  180.1 9.5 %all-to-all-start.1 = ((f32[8,8,768]{2,1,0:T(8,128)}), f32[8,8,768]{2,1,0:T(8,128)S(1)}, u32[]{:S(2)}, u32[]{:S(2)}) async-start(f32[8,8,768]{2,1,0:T(8,128)} %get-tuple-element.28), calls=%async_computation.1 | async-start | bytes 393216 | tf_op jit(solution)/shard_map/all_to_all | solution.py:616
  189.5 0.7 copy-start
Sparse Core Ops, SparseCore 0:
  35.4 29.6 all-gather.10
  66.8 27.6 all-gather.8
  96.1 31.5 all-gather.14
  146.8 27.9 all-gather.12

commit v2 on v1

--- a/solution.py
+++ b/solution.py
@@ -100,32 +100,28 @@
     return rotated
 
 
-def kv_kernel(
-    where, h_ref, wk_ref, wv_ref, cr, sr, cs, ss, kva_ref, kvb_ref, acc, hb, kb, vb, sem
+def qkv_kernel(
+    where, h_ref, wk_ref, wv_ref, wq_ref, cr, sr, cs, ss, a_ref, b_ref, rim_ref, acc, hb, kb, vb, qb, sem
 ):
     streamed_products(
-        ((h_ref, hb, True), (wk_ref, kb, False), (wv_ref, vb, False)),
+        ((h_ref, hb, True), (wk_ref, kb, False), (wv_ref, vb, False), (wq_ref, qb, False)),
         sem,
-        ((acc, hb, (kb, vb)),),
-    )
+        ((acc, hb, (kb, vb, qb)),),
+    )
+    for k in range(STEPS):
+        rim_ref[:, k * CHUNK : (k + 1) * CHUNK] = hb[k, ROWS - HALO :, :]
     rotated = rotation(cr, sr, cs, ss)
-    keys = [rotated(acc[0, :, i * 128 : i * 128 + 128]).astype(jnp.bfloat16) for i in range(2)]
-    vals = [acc[1, :, i * 128 : i * 128 + 128].astype(jnp.bfloat16) for i in range(2)]
-    for flip, kv_ref in ((0, kva_ref), (1, kvb_ref)):
-        take = where[1] == flip
-        kv_ref[:, 0:128] = jnp.where(take, keys[0], keys[1])
-        kv_ref[:, 128:256] = jnp.where(take, vals[0], vals[1])
-
-
-def q_kernel(where, h_ref, wq_ref, cr, sr, cs, ss, _, qa_ref, qb_ref, acc, hb, qb, sem):
-    streamed_products(((h_ref, hb, True), (wq_ref, qb, False)), sem, ((acc, hb, (qb,)),))
-    rotated = rotation(cr, sr, cs, ss)
-    queries = [
-        (rotated(acc[0, :, i * 128 : i * 128 + 128]) * (LOG2E / 8)).astype(jnp.bfloat16)
-        for i in range(2)
-    ]
-    for flip, q_ref in ((0, qa_ref), (1, qb_ref)):
-        q_ref[...] = jnp.where(where[1] == flip, queries[0], queries[1])
+    heads = []
+    for i in range(2):
+        cols = slice(i * 128, i * 128 + 128)
+        query = rotated(acc[2, :, cols]) * (LOG2E / 8)
+        parts = (rotated(acc[0, :, cols]), acc[1, :, cols], query)
+        heads.append([part.astype(jnp.bfloat16) for part in parts])
+    for flip, o_ref in ((0, a_ref), (1, b_ref)):
+        for i in range(3):
+            o_ref[:, i * 128 : i * 128 + 128] = jnp.where(
+                where[1] == flip, heads[0][i], heads[1][i]
+            )
 
 
 def in_hbm():
@@ -143,39 +139,42 @@
     )
 
 
-def project(kernel, width, where, hidden, weights, unread=()):
+def project(where, hidden, w_key, w_value, w_query):
     row_cos, row_sin, start_cos, start_sin = rotary_tables()
     table = pl.BlockSpec((GROUP, 128), lambda k, *_: (0, 0))
     starts = pl.BlockSpec((ROWS // GROUP, 128), lambda k, where: (where[0], 0))
-    out = jax.ShapeDtypeStruct((ROWS, width), jnp.bfloat16)
-    count = len(weights)
+    shapes = ((ROWS, 384), (ROWS, 384), (HALO, D))
     return pl.pallas_call(
-        kernel,
-        out_shape=(out, out),
+        qkv_kernel,
+        out_shape=tuple(jax.ShapeDtypeStruct(shape, jnp.bfloat16) for shape in shapes),
         grid_spec=pltpu.PrefetchScalarGridSpec(
             num_scalar_prefetch=1,
             grid=(1,),
-            in_specs=[in_hbm()] * (1 + count)
-            + [table, table, starts, starts]
-            + [in_hbm()] * len(unread),
-            out_specs=(pl.BlockSpec((ROWS, width), lambda k, *_: (0, 0)),) * 2,
-            scratch_shapes=[
-                pltpu.VMEM((count, ROWS, 256), jnp.float32),
-                *stream_buffers(count, False),
-            ],
+            in_specs=[in_hbm()] * 4 + [table, table, starts, starts],
+            out_specs=tuple(pl.BlockSpec(shape, lambda k, *_: (0, 0)) for shape in shapes),
+            scratch_shapes=[pltpu.VMEM((3, ROWS, 256), jnp.float32), *stream_buffers(3, False)],
         ),
         compiler_params=pltpu.CompilerParams(vmem_limit_bytes=60 * 2**20),
         cost_estimate=pl.CostEstimate(
-            flops=2 * ROWS * D * 256 * count,
-            bytes_accessed=(6 + 2 * count) * 2**20,
-            transcendentals=0,
-        ),
-    )(where, hidden, *weights, row_cos, row_sin, start_cos, start_sin, *unread)
+            flops=2 * ROWS * D * 768, bytes_accessed=13 * 2**20, transcendentals=0
+        ),
+        name="qkv",
+    )(where, hidden, w_key, w_value, w_query, row_cos, row_sin, start_cos, start_sin)
+
+
+PARCEL = ROWS + 4 * 256
 
 
 def conv_kernel(
-    h_ref, rim_ref, wb_ref, wc_ref, wh_ref, taps_ref, o_ref, acc, rim_acc, padded, hb, rb, b, c, h, sem
+    h_ref, rim_ref, wb_ref, wc_ref, wh_ref, oc_ref, oa_ref, taps_ref, parcel_ref,
+    acc, rim_acc, padded, staged, out_w, load_sem, store_sem, hb, rb, b, c, h, sem
 ):
+    loads = [
+        pltpu.make_async_copy(w_ref, out_w.at[i], load_sem.at[i])
+        for i, w_ref in enumerate((oc_ref, oa_ref))
+    ]
+    for load in loads:
+        load.start()
     streamed_products(
         (
             (h_ref, hb, True),
@@ -187,6 +186,23 @@
         sem,
         ((acc, hb, (b, c, h)), (rim_acc, rb, (b, c, h))),
     )
+    stores = []
+
+    def store(source, t, part, first_row, count):
+        stores.append(
+            pltpu.make_async_copy(
+                source, parcel_ref.at[t, pl.ds(first_row, count)], store_sem.at[t, part]
+            )
+        )
+        stores[-1].start()
+
+    for i in range(2):
+        loads[i].wait()
+        for t in range(8):
+            for half in range(2):
+                part = 2 * i + half
+                column = pl.ds((2 * t + half) * 256, 256)
+                store(out_w.at[i, :, column], t, part, ROWS + part * 256, 256)
 
     def once(x):
         return x.astype(jnp.bfloat16).astype(jnp.float32)
@@ -197,35 +213,36 @@
     conv = jnp.zeros((ROWS, 256), jnp.float32)
     for tap in range(3):
         conv = conv + taps[tap : tap + 1] * padded[HALO - 2 + tap : HALO - 2 + tap + ROWS]
-    o_ref[...] = (once(acc[0]) * conv).astype(jnp.bfloat16)
-
-
-def gated_conv(hidden, rim, w_b, w_c, w_h, taps):
+    staged[...] = (once(acc[0]) * conv).astype(jnp.bfloat16)
+    for t in range(8):
+        store(staged, t, 4, 0, ROWS)
+    for copy in stores:
+        copy.wait()
+
+
+def gated_conv(hidden, rim, w_b, w_c, w_h, w_out_conv, w_out_attn, taps):
     return pl.pallas_call(
         conv_kernel,
-        out_shape=jax.ShapeDtypeStruct((ROWS, 256), jnp.bfloat16),
+        out_shape=jax.ShapeDtypeStruct((8, PARCEL, 256), jnp.bfloat16),
         grid=(1,),
-        in_specs=[
-            in_hbm(),
-            in_hbm(),
-            in_hbm(),
-            in_hbm(),
-            in_hbm(),
-            pl.BlockSpec((3, 256), lambda k: (0, 0)),
-        ],
-        out_specs=pl.BlockSpec((ROWS, 256), lambda k: (0, 0)),
+        in_specs=[in_hbm()] * 7 + [pl.BlockSpec((3, 256), lambda k: (0, 0))],
+        out_specs=in_hbm(),
         scratch_shapes=[
             pltpu.VMEM((3, ROWS, 256), jnp.float32),
             pltpu.VMEM((3, HALO, 256), jnp.float32),
             pltpu.VMEM((HALO + ROWS, 256), jnp.float32),
+            pltpu.VMEM((ROWS, 256), jnp.bfloat16),
+            pltpu.VMEM((2, 256, D), jnp.bfloat16),
+            pltpu.SemaphoreType.DMA((2,)),
+            pltpu.SemaphoreType.DMA((8, 5)),
             *stream_buffers(3, True),
         ],
         compiler_params=pltpu.CompilerParams(vmem_limit_bytes=60 * 2**20),
         cost_estimate=pl.CostEstimate(
-            flops=2 * ROWS * D * 768, bytes_accessed=13 * 2**20, transcendentals=0
+            flops=2 * ROWS * D * 768, bytes_accessed=24 * 2**20, transcendentals=0
         ),
         name="gated_conv",
-    )(hidden, rim, w_b, w_c, w_h, taps)
+    )(hidden, rim, w_b, w_c, w_h, w_out_conv, w_out_attn, taps)
 
 
 KEYS_AT_ONCE = 256
@@ -311,9 +328,9 @@
     return (kb % 4) * 2 + 3 - kb // 4
 
 
-def low_kernel(own, lam, qa_ref, qb_ref, kv_ref, gain_ref, _, o_ref, m_o, l_o, a_o, qz):
+def low_kernel(own, lam, ql_ref, qh_ref, kv_ref, gain_ref, o_ref, m_o, l_o, a_o, qz):
     step = pl.program_id(0)
-    split_maps(jnp.where(step == own[2], qa_ref[...], qb_ref[...]), qz)
+    split_maps(jnp.where(step == 0, ql_ref[...], qh_ref[...]), qz)
     start_state(m_o, l_o, a_o)
     refs = (qz, kv_ref, m_o, l_o, a_o)
     attend_blocks(0, jnp.where(step == 0, own[0], 8), low_place, refs)
@@ -325,10 +342,10 @@
 
 
 def high_kernel(
-    own, lam, qa_ref, qb_ref, kv_ref, gain_ref, low_ref, m_i, l_i, a_i, _, oa_ref, ob_ref, qz
+    own, lam, qh_ref, kv_ref, gain_ref, low_ref, m_i, l_i, a_i, oa_ref, ob_ref, qz
 ):
     low_first = own[2] == 0
-    split_maps(jnp.where(low_first, qb_ref[...], qa_ref[...]), qz)
+    split_maps(qh_ref[...], qz)
     refs = (qz, kv_ref, m_i, l_i, a_i)
     attend_blocks(8, own[1] - 8, high_place, refs)
     attend_diagonal(high_place(own[1]), refs)
@@ -358,54 +375,22 @@
     )(*args, *unread)
 
 
-def column_kernel(wc_ref, wa_ref, o_ref, buf, sem):
-    width = o_ref.shape[3]
-    loads = [
-        pltpu.make_async_copy(w_ref, buf.at[i], sem.at[i, 8])
-        for i, w_ref in enumerate((wc_ref, wa_ref))
-    ]
-    for load in loads:
-        load.start()
-    stores = []
-    for i in range(2):
-        loads[i].wait()
-        for t in range(8):
-            stores.append(
-                pltpu.make_async_copy(
-                    buf.at[i, :, pl.ds(t * width, width)], o_ref.at[t, i], sem.at[i, t]
-                )
-            )
-            stores[-1].start()
-    for store in stores:
-        store.wait()
-
-
-def column_blocks(w_conv, w_attn):
-    return pl.pallas_call(
-        column_kernel,
-        out_shape=jax.ShapeDtypeStruct((8, 2, 256, D // 8), jnp.bfloat16),
-        in_specs=[in_hbm(), in_hbm()],
-        out_specs=in_hbm(),
-        scratch_shapes=[pltpu.VMEM((2, 256, D), jnp.bfloat16), pltpu.SemaphoreType.DMA((2, 9))],
-        compiler_params=pltpu.CompilerParams(vmem_limit_bytes=60 * 2**20),
-        cost_estimate=pl.CostEstimate(
-            flops=3 * 10**9, bytes_accessed=9 * 2**20, transcendentals=0
-        ),
-        name="column_blocks",
-    )(w_conv, w_attn)
-
-
-def whole_conv_kernel(x_ref, w_ref, o_ref):
-    left = jnp.concatenate([x_ref[t] for t in range(8)], axis=1)
-    right = jnp.concatenate([w_ref[t, 0] for t in range(8)], axis=0)
-    o_ref[...] = jnp.dot(left, right, preferred_element_type=jnp.float32)
-
-
-def whole_last_kernel(first, x_ref, w_ref, before_ref, mix_ref, sums_ref, xb, wb, acc, sem):
+def whole_conv_kernel(parcel_ref, o_ref):
+    left = jnp.concatenate([parcel_ref[t, 0:ROWS] for t in range(8)], axis=1)
+    for half in range(2):
+        at = ROWS + half * 256
+        right = jnp.concatenate([parcel_ref[t, at : at + 256] for t in range(8)], axis=0)
+        o_ref[:, half * 256 : half * 256 + 256] = jnp.dot(
+            left, right, preferred_element_type=jnp.float32
+        )
+
+
+def whole_last_kernel(first, x_ref, parcel_ref, before_ref, mix_ref, sums_ref, xb, wb, acc, sem):
     copies = []
     for t in range(8):
+        source = parcel_ref.at[t, pl.ds(ROWS + 512, 512)]
         copies.append(pltpu.make_async_copy(x_ref.at[t], xb.at[t], sem.at[0, t]))
-        copies.append(pltpu.make_async_copy(w_ref.at[t, 1], wb.at[t], sem.at[1, t]))
+        copies.append(pltpu.make_async_copy(source, wb.at[t], sem.at[1, t]))
     head = pltpu.make_async_copy(before_ref, acc, sem.at[2, 0])
     head.start()
     for copy in copies:
@@ -414,14 +399,17 @@
     for t in range(8):
         copies[2 * t].wait()
         copies[2 * t + 1].wait()
-        right = jnp.concatenate(
-            [
-                wb[t, pl.ds(pl.multiple_of(first[0] * VD, VD), VD), :],
-                wb[t, pl.ds(pl.multiple_of((1 - first[0]) * VD, VD), VD), :],
-            ],
-            axis=0,
-        )
-        acc[...] += jnp.dot(xb[t], right, preferred_element_type=jnp.float32)
+        for half in range(2):
+            right = jnp.concatenate(
+                [
+                    wb[t, pl.ds(pl.multiple_of(half * 256 + first[0] * VD, VD), VD), :],
+                    wb[t, pl.ds(pl.multiple_of(half * 256 + (1 - first[0]) * VD, VD), VD), :],
+                ],
+                axis=0,
+            )
+            acc[:, half * 256 : half * 256 + 256] += jnp.dot(
+                xb[t], right, preferred_element_type=jnp.float32
+            )
     mix = acc[...].astype(jnp.bfloat16)
     mix_ref[...] = mix
     wide = mix.astype(jnp.float32)
@@ -435,39 +423,34 @@
             ones, values, (((1,), (1,)), ((), ())), preferred_element_type=jnp.float32
         )
 
-    row = lax.broadcasted_iota(jnp.int32, (8, ROWS), 0)
-    squares = jnp.where(row == 1, row_sums(high) + row_sums(low), 0.0)
-    sums = jnp.where(row == 0, row_sums(mix), squares)
+    squares = row_sums(high) + row_sums(low)
+    sums = jnp.concatenate([row_sums(mix)[0:1], squares[0:1]], axis=0)
     for copy in range(8):
         sums_ref[copy] = sums
 
 
-def whole_conv(gathered, weights):
-    width = weights.shape[3]
+def whole_conv(parcels):
     return pl.pallas_call(
         whole_conv_kernel,
-        out_shape=jax.ShapeDtypeStruct((ROWS, width), jnp.float32),
+        out_shape=jax.ShapeDtypeStruct((ROWS, D // 8), jnp.float32),
         grid=(1,),
-        in_specs=[
-            pl.BlockSpec(gathered.shape, lambda i: (0, 0, 0)),
-            pl.BlockSpec((8, 1, 256, width), lambda i: (0, 0, 0, 0)),
-        ],
-        out_specs=pl.BlockSpec((ROWS, width), lambda i: (0, 0)),
+        in_specs=[pl.BlockSpec((8, ROWS + 512, 256), lambda i: (0, 0, 0))],
+        out_specs=pl.BlockSpec((ROWS, D // 8), lambda i: (0, 0)),
         compiler_params=pltpu.CompilerParams(vmem_limit_bytes=60 * 2**20),
         cost_estimate=pl.CostEstimate(
-            flops=2 * ROWS * 2048 * width, bytes_accessed=7 * 2**20, transcendentals=0
+            flops=2 * ROWS * 2048 * D // 8, bytes_accessed=7 * 2**20, transcendentals=0
         ),
         name="whole_conv",
-    )(gathered, weights)
-
-
-def whole_last(first, gathered, weights, before):
-    width = weights.shape[3]
+    )(parcels)
+
+
+def whole_last(first, gathered, parcels, before):
+    width = D // 8
     return pl.pallas_call(
         whole_last_kernel,
         out_shape=(
             jax.ShapeDtypeStruct((ROWS, width), jnp.bfloat16),
-            jax.ShapeDtypeStruct((8, 8, ROWS), jnp.float32),
+            jax.ShapeDtypeStruct((8, 2, ROWS), jnp.float32),
         ),
         grid_spec=pltpu.PrefetchScalarGridSpec(
             num_scalar_prefetch=1,
@@ -475,11 +458,11 @@
             in_specs=[in_hbm(), in_hbm(), in_hbm()],
             out_specs=(
                 pl.BlockSpec((ROWS, width), lambda i, *_: (0, 0)),
-                pl.BlockSpec((8, 8, ROWS), lambda i, *_: (0, 0, 0)),
+                pl.BlockSpec((8, 2, ROWS), lambda i, *_: (0, 0, 0)),
             ),
             scratch_shapes=[
                 pltpu.VMEM((8, ROWS, 256), jnp.bfloat16),
-                pltpu.VMEM((8, 256, width), jnp.bfloat16),
+                pltpu.VMEM((8, 512, 256), jnp.bfloat16),
                 pltpu.VMEM((ROWS, width), jnp.float32),
                 pltpu.SemaphoreType.DMA((3, 8)),
             ],
@@ -489,17 +472,16 @@
             flops=2 * ROWS * 2048 * width, bytes_accessed=7 * 2**20, transcendentals=0
         ),
         name="whole_last",
-    )(first, gathered, weights, before)
+    )(first, gathered, parcels, before)
 
 
 def norm_kernel(own, mix_ref, sums_ref, gain_ref, o_ref):
-    sums = sums_ref[...].reshape(64, ROWS)
-    row = lax.broadcasted_iota(jnp.int32, (64, 128), 0) % 8
+    ones = jnp.ones((8, 128), jnp.float32)
 
     def column(which):
         total = lax.dot_general(
-            sums,
-            jnp.where(row == which, 1.0, 0.0),
+            sums_ref[:, which, :],
+            ones,
             (((0,), (0,)), ((), ())),
             preferred_element_type=jnp.float32,
             precision=lax.Precision.HIGHEST,
@@ -557,34 +539,34 @@
     sp = z * 4 + x
 
     z_core = ("z", "c")
-    rim = lax.ppermute(hidden_states[ROWS - HALO :], ("z", "x"), [(i, i + 1) for i in range(15)])
     other_lambdas = lax.ppermute(lambdas, "c", [(0, 1), (1, 0)])
 
     first = jnp.where(z < 2, 0, 1).astype(jnp.int32).reshape(1)
     where = jnp.stack([sp, jnp.where(z < 2, 0, 1)]).astype(jnp.int32)
     route_a, route_b = forward_route(0), forward_route(1)
-    kv_a, kv_b = project(kv_kernel, 256, where, hidden_states, (w_key, w_value))
-    blocks = column_blocks(w_out_conv, w_out_attn)
-    q_a, q_b = project(q_kernel, 128, where, hidden_states, (w_query,), (kv_a,))
-    kv_a = lax.ppermute(kv_a, z_core, route_a)
-    kv_b = lax.ppermute(kv_b, z_core, route_b)
-    q_a = lax.ppermute(q_a, z_core, route_a)
-    q_b = lax.ppermute(q_b, z_core, route_b)
+    head_a, head_b, last_rows = project(where, hidden_states, w_key, w_value, w_query)
+    rim = lax.ppermute(last_rows, ("z", "x"), [(i, i + 1) for i in range(15)])
+    head_a = lax.ppermute(head_a, z_core, route_a)
+    head_b = lax.ppermute(head_b, z_core, route_b)
+    parcels = gated_conv(
+        hidden_states,
+        rim,
+        w_conv_b,
+        w_conv_c,
+        w_conv_h,
+        w_out_conv,
+        w_out_attn,
+        conv_taps,
+    )
+    parcels = lax.all_to_all(parcels, ("y", "c"), split_axis=0, concat_axis=0, tiled=True)
     even = (z % 2) == 0
-    kv_low, kv_high = jnp.where(even, kv_a, kv_b), jnp.where(even, kv_b, kv_a)
+    kv, q = slice(0, 256), slice(256, 384)
+    kv_low = jnp.where(even, head_a[:, kv], head_b[:, kv])
+    kv_high = jnp.where(even, head_b[:, kv], head_a[:, kv])
+    q_low = jnp.where(even, head_a[:, q], head_b[:, q])
+    q_high = jnp.where(even, head_b[:, q], head_a[:, q])
     kv_low = lax.all_gather(kv_low, ("x", "c"), axis=0)
     kv_high = lax.all_gather(kv_high, ("x", "c"), axis=0)
-
-    conv_out = gated_conv(hidden_states, rim, w_conv_b, w_conv_c, w_conv_h, conv_taps)
-    conv_all = lax.all_gather(conv_out, ("y", "c"), axis=0)
-
-    w_out = lax.all_to_all(
-        blocks,
-        ("y", "c"),
-        split_axis=0,
-        concat_axis=0,
-        tiled=True,
-    )
 
     plane_lambdas = jnp.where(
         core == 0,
@@ -598,21 +580,16 @@
     rows = jax.ShapeDtypeStruct((ROWS, VD), jnp.bfloat16)
     state = (jax.ShapeDtypeStruct((2, ROWS, VD), jnp.float32),) * 3
     o_low, *carried = attention_call(
-        low_kernel, 2, (own, lam, q_a, q_b, kv_low, gain), (rows, *state), (conv_out,), 12
+        low_kernel, 2, (own, lam, q_low, q_high, kv_low, gain), (rows, *state), (), 12
     )
     o_a, o_b = attention_call(
-        high_kernel,
-        1,
-        (own, lam, q_a, q_b, kv_high, gain, o_low, *carried),
-        (rows, rows),
-        (w_out,),
-        6,
+        high_kernel, 1, (own, lam, q_high, kv_high, gain, o_low, *carried), (rows, rows), (), 6
     )
     back_a = lax.ppermute(o_a, z_core, reverse(route_a))
     back_b = lax.ppermute(o_b, z_core, reverse(route_b))
     attn_all = lax.all_gather(jnp.concatenate([back_a, back_b], axis=1), ("y", "c"), axis=0)
-    conv_part = whole_conv(conv_all, w_out)
-    mix, sums = whole_last(first, attn_all, w_out, conv_part)
+    conv_part = whole_conv(parcels)
+    mix, sums = whole_last(first, attn_all, parcels, conv_part)
     everything = lax.all_to_all(sums, ("y", "c"), split_axis=0, concat_axis=0, tiled=True)
     tp = (lax.axis_index("y") * 2 + core).astype(jnp.int32).reshape(1)
     return layer_norm(tp, mix, everything, out_gain.reshape(1, D))

time: 201 us -> 195 us (0.970); the launches traced: 200 us -> 191 us
  starting transfers between devices: 49.5 us -> 36.4 us
  waiting for transfers between devices: 55 us -> 66.5 us
  Pallas kernels: 75.1 us -> 68.7 us
    all_to_all x1, waiting for transfers between devices: 5.36 us -> 31.6 us  [per_device(): lax.all_to_all(parcels, ('y', 'c'), split_axis=0, concat_axis=0, tiled=True)]
    all_gather x1, waiting for transfers between devices: 22.5 us -> 1.28 us  [per_device(): lax.all_gather(jnp.concatenate([back_a, back_b], axis=1), ('y', 'c'), axi...]
    ppermute x5 -> x3, starting transfers between devices: 22.5 us -> 12.7 us  [the longest x1 7.01 us: per_device(): head_a = lax.ppermute(head_a, z_core, route_a)]
    pallas_call x5 -> x3, Pallas kernels: 35.3 us -> 29.3 us  [the longest x1 12.8 us: gated_conv(): pl.pallas_call(conv_kernel, out_shape=jax.ShapeDtypeStruct((8, PARCEL, 25...]
    all_gather x1, waiting for transfers between devices: 0.01 us -> 5.13 us  [per_device(): kv_high = lax.all_gather(kv_high, ('x', 'c'), axis=0)]
    ppermute x1, waiting for transfers between devices: 0.01 us -> 4.96 us  [per_device(): back_a = lax.ppermute(o_a, z_core, reverse(route_a))]
    ppermute x1, waiting for transfers between devices: 6.66 us -> 1.82 us  [per_device(): back_b = lax.ppermute(o_b, z_core, reverse(route_b))]
    ppermute x1, starting transfers between devices: 4.14 us -> 1.92 us  [per_device(): back_a = lax.ppermute(o_a, z_core, reverse(route_a))]
  transfers between devices with their start and end apart: 14 -> 11, of which waited for: 8 -> 10; matrix products, arithmetic and copies ran while one was open for 2% -> 2% of each run, Pallas kernels for 29% -> 26%
where the time goes in v2:
time: 195 us; the launch traced here: 191 us
  Pallas kernels  68.7 us (35%)
  waiting for transfers between devices  66.5 us (34%)
  starting transfers between devices  36.4 us (19%)
  between operations  13.2 us (7%)
  other arithmetic  3.88 us (2%)
  local copies, waits for them, and re-layouts  2.46 us (1%)
    all_to_all x1, waiting for transfers between devices, per_device(): lax.all_to_all(parcels, ('y', 'c'), split_axis=0, concat_axis=0, tiled=True)  31.6 us
    pallas_call x2, Pallas kernels, attention_call(): pl.pallas_call(kernel, out_shape=outs, grid_spec=pltpu.PrefetchScalarGrid...  30.9 us
    pallas_call x1, Pallas kernels, gated_conv(): pl.pallas_call(conv_kernel, out_shape=jax.ShapeDtypeStruct((8, PARCEL, 25...  12.8 us
    pallas_call x1, Pallas kernels, project(): pl.pallas_call(qkv_kernel, out_shape=tuple((jax.ShapeDtypeStruct(shape, j...  10.9 us
    ppermute x1, starting transfers between devices, per_device(): back_b = lax.ppermute(o_b, z_core, reverse(route_b))  10.6 us
    ppermute x1, waiting for transfers between devices, per_device(): head_a = lax.ppermute(head_a, z_core, route_a)  10.3 us
    ppermute x1, starting transfers between devices, per_device(): head_a = lax.ppermute(head_a, z_core, route_a)  7.01 us
    all_to_all x1, starting transfers between devices, per_device(): lax.all_to_all(parcels, ('y', 'c'), split_axis=0, concat_axis=0, tiled=True)  5.59 us
  transfers between devices with their start and end apart: 11, of which 10 were waited for; matrix products, arithmetic and copies ran while one was open for 2% of the time, Pallas kernels for 26%

profile of v2, /device:TPU:1, one launch (start us, length us, event | category | flops | bytes accessed | tf_op | source)
XLA Modules:
  0.0 191.3 jit_solution(8742911759095426894)
XLA Ops:
  6.5 0.0 all-gather.9.cloned.1.call-start
  6.5 0.6 pad_add_fusion.1.where
  7.2 10.9 %qkv.1 = (bf16[768,384]{1,0:T(8,128)(2,1)}, bf16[768,384]{1,0:T(8,128)(2,1)}, bf16[16,4096]{1,0:T(8,128)(2,1)}) custom-call(s32[2]{0:T(128)} %pad_add_fusion.1.where, bf16[768,4096]{1,0:T(8,128)(2,1)} %h_ref.3, bf16[4096,256]{1,0:T(8,128)(2,1)} %wk_ref.1, bf16[4096,256]{1,0:T(8,128)(2,1)} %wv_ref.1, bf16[4096,256]{1,0:T(8,128)(2,1)} %wq_ref.1, ...), custom_call_target="tpu_custom_call" | custom-call | flops 4831838208 | bytes 13631488 | tf_op jit(solution)/shard_map/qkv/pallas_call | solution.py:147
  18.1 0.0 copy-start.3
  18.1 0.0 copy-start.4
  18.1 7.0 %collective-permute-start.2 = (bf16[768,384]{1,0:T(8,128)(2,1)}, bf16[768,384]{1,0:T(8,128)(2,1)S(1)}, u32[]{:S(2)}, u32[]{:S(2)}) collective-permute-start(bf16[768,384]{1,0:T(8,128)(2,1)} %get-tuple-element.17), channel_id=1, source_target_pairs={{0,0},{1,64},{32,1},{33,65},{64,33},{65,97},{96,32},{97,96},{2,2},... | collective-permute-start | bytes 1769480 | tf_op jit(solution)/shard_map/ppermute | solution.py:549
  25.1 2.6 %collective-permute-start.1 = (bf16[768,384]{1,0:T(8,128)(2,1)}, bf16[768,384]{1,0:T(8,128)(2,1)S(1)}, u32[]{:S(2)}, u32[]{:S(2)}) collective-permute-start(bf16[768,384]{1,0:T(8,128)(2,1)} %get-tuple-element.16), channel_id=1, source_target_pairs={{0,32},{1,96},{32,33},{33,97},{64,1},{65,65},{96,0},{97,64},{2,34}... | collective-permute-start | bytes 1769480 | tf_op jit(solution)/shard_map/ppermute | solution.py:550
  27.8 10.3 %collective-permute-done.2 = bf16[768,384]{1,0:T(8,128)(2,1)S(1)} collective-permute-done((bf16[768,384]{1,0:T(8,128)(2,1)}, bf16[768,384]{1,0:T(8,128)(2,1)S(1)}, u32[]{:S(2)}, u32[]{:S(2)}) %collective-permute-start.2) | collective-permute-done | bytes 589856 | tf_op jit(solution)/shard_map/ppermute | solution.py:549
  38.0 3.1 %collective-permute-done.1 = bf16[768,384]{1,0:T(8,128)(2,1)S(1)} collective-permute-done((bf16[768,384]{1,0:T(8,128)(2,1)}, bf16[768,384]{1,0:T(8,128)(2,1)S(1)}, u32[]{:S(2)}, u32[]{:S(2)}) %collective-permute-start.1) | collective-permute-done | bytes 589856 | tf_op jit(solution)/shard_map/ppermute | solution.py:550
  41.1 1.0 broadcast_select_fusion
  42.1 0.0 all-gather.9.cloned.1.call-update
  42.1 0.0 all-gather.7.cloned.1.call-start
  42.2 0.7 all-gather.7.cloned.1.call-update
  42.9 0.0 copy-done.3
  42.9 1.5 collective-permute-start
  44.4 0.0 copy-done.4
  44.4 3.1 %collective-permute-start.5 = (bf16[16,4096]{1,0:T(8,128)(2,1)S(1)}, bf16[16,4096]{1,0:T(8,128)(2,1)S(1)}, u32[]{:S(2)}, u32[]{:S(2)}) collective-permute-start(bf16[16,4096]{1,0:T(8,128)(2,1)S(1)} %copy-done.4), channel_id=1, source_target_pairs={{0,8},{8,16},{16,24},{24,32},{32,40},{40,48},{48,56},{56,64},{64,7... | collective-permute-start | bytes 393224 | tf_op jit(solution)/shard_map/ppermute | solution.py:548
  47.5 0.6 pad_add_fusion.own
  48.1 0.0 collective-permute-done
  48.1 0.1 broadcast_select_fusion.4
  48.2 0.6 dynamic_slice.3.lam
  48.8 1.5 collective-permute-done.5.rim_ref
  50.3 0.0 copy-start.1
  50.3 0.7 copy-done.1
  51.0 12.8 %gated_conv.1 = bf16[8,1792,256]{2,1,0:T(8,128)(2,1)} custom-call(bf16[768,4096]{1,0:T(8,128)(2,1)} %h_ref.3, bf16[16,4096]{1,0:T(8,128)(2,1)} %copy-done.1, bf16[4096,256]{1,0:T(8,128)(2,1)} %wb_ref.1, bf16[4096,256]{1,0:T(8,128)(2,1)} %wc_ref.1, bf16[4096,256]{1,0:T(8,128)(2,1)} %wh_ref.1, bf16[256,4096]{1,0:T(8,128)(2,1)} %oc_ref.1, ...), custom_call_target="tpu_custom_call" | custom-call | flops 4831838208 | bytes 25165824 | tf_op jit(solution)/shard_map/gated_conv/pallas_call | solution.py:224
  63.8 5.6 %all-to-all-start = ((bf16[8,1792,256]{2,1,0:T(8,128)(2,1)}), bf16[8,1792,256]{2,1,0:T(8,128)(2,1)}, u32[]{:S(2)}, u32[]{:S(2)}) async-start(bf16[8,1792,256]{2,1,0:T(8,128)(2,1)} %gated_conv.1), calls=%async_computation | async-start | bytes 14680064 | tf_op jit(solution)/shard_map/all_to_all | solution.py:561
  69.4 0.0 all-gather.11.cloned.1.call-start
  69.4 0.8 broadcast_select_fusion.2
  70.2 1.9 all-gather.9.cloned.1.call-done
  72.1 24.1 %shard_map.163 = (bf16[768,128]{1,0:T(8,128)(2,1)}, f32[2,768,128]{2,1,0:T(8,128)}, f32[2,768,128]{2,1,0:T(8,128)}, f32[2,768,128]{2,1,0:T(8,128)}) custom-call(s32[3]{0:T(128)} %pad_add_fusion.own, f32[1]{0:T(128)} %dynamic_slice.3.lam, bf16[768,128]{1,0:T(8,128)(2,1)} %get-tuple-element.29.ql_ref, bf16[768,128]{1,0:T(8,128)(2,1)} %get-tuple-element.30.qh_ref, ...), custom_call_target="tpu_custom_call" | custom-call | flops 24000000000 | bytes 4194304 | tf_op jit(solution)/shard_map/pallas_call | solution.py:361
  96.2 5.1 %all-gather.7.cloned.1.call-done = bf16[6144,256]{1,0:T(8,128)(2,1)} async-done(((bf16[768,256]{1,0:T(8,128)(2,1)}), bf16[6144,256]{1,0:T(8,128)(2,1)}) %all-gather.7.cloned.1.call-update) | async-done | bytes 3145744 | tf_op jit(solution)/shard_map/all_gather | solution.py:569
  101.4 6.8 %shard_map.164 = (bf16[768,128]{1,0:T(8,128)(2,1)}, bf16[768,128]{1,0:T(8,128)(2,1)}) custom-call(s32[3]{0:T(128)} %pad_add_fusion.own, f32[1]{0:T(128)} %dynamic_slice.3.lam, bf16[768,128]{1,0:T(8,128)(2,1)} %get-tuple-element.30.qh_ref, bf16[8,768,256]{2,1,0:T(8,128)(2,1)} %bitcast.12, bf16[1,128]{1,0:T(2,128)(2,1)} %bitcast.14, ...), custom_call_target="tpu_custom_call" | custom-call | flops 12000000000 | bytes 4194304 | tf_op jit(solution)/shard_map/pallas_call | solution.py:361
  108.1 10.6 %collective-permute-start.4 = (bf16[768,128]{1,0:T(8,128)(2,1)}, bf16[768,128]{1,0:T(8,128)(2,1)S(1)}, u32[]{:S(2)}, u32[]{:S(2)}) collective-permute-start(bf16[768,128]{1,0:T(8,128)(2,1)} %get-tuple-element.23), channel_id=1, source_target_pairs={{32,0},{96,1},{33,32},{97,33},{1,64},{65,65},{0,96},{64,97},{34,2}... | collective-permute-start | bytes 589832 | tf_op jit(solution)/shard_map/ppermute | solution.py:589
  118.7 1.9 %collective-permute-start.3 = (bf16[768,128]{1,0:T(8,128)(2,1)}, bf16[768,128]{1,0:T(8,128)(2,1)S(1)}, u32[]{:S(2)}, u32[]{:S(2)}) collective-permute-start(bf16[768,128]{1,0:T(8,128)(2,1)} %get-tuple-element.22), channel_id=1, source_target_pairs={{0,0},{64,1},{1,32},{65,33},{33,64},{97,65},{32,96},{96,97},{2,2},... | collective-permute-start | bytes 589832 | tf_op jit(solution)/shard_map/ppermute | solution.py:588
  120.7 1.8 collective-permute-done.4
  122.5 5.0 %collective-permute-done.3 = bf16[768,128]{1,0:T(8,128)(2,1)S(1)} collective-permute-done((bf16[768,128]{1,0:T(8,128)(2,1)}, bf16[768,128]{1,0:T(8,128)(2,1)S(1)}, u32[]{:S(2)}, u32[]{:S(2)}) %collective-permute-start.3) | collective-permute-done | bytes 196640 | tf_op jit(solution)/shard_map/ppermute | solution.py:588
  127.4 0.8 pad_maximum_fusion
  128.2 0.0 all-gather.11.cloned.1.call-update
  128.3 31.6 %all-to-all-done.parcel_ref = bf16[8,1792,256]{2,1,0:T(8,128)(2,1)} async-done(((bf16[8,1792,256]{2,1,0:T(8,128)(2,1)}), bf16[8,1792,256]{2,1,0:T(8,128)(2,1)}, u32[]{:S(2)}, u32[]{:S(2)}) %all-to-all-start) | async-done | bytes 7340064 | tf_op jit(solution)/shard_map/all_to_all | solution.py:561
  159.9 5.6 %whole_conv.1.before_ref = f32[768,512]{1,0:T(8,128)} custom-call(bf16[8,1792,256]{2,1,0:T(8,128)(2,1)} %all-to-all-done.parcel_ref), custom_call_target="tpu_custom_call" | custom-call | flops 1610612736 | bytes 7340032 | tf_op jit(solution)/shard_map/whole_conv/pallas_call | solution.py:433
  165.4 1.3 all-gather.11.cloned.1.call-done
  166.7 5.3 %whole_last.1 = (bf16[768,512]{1,0:T(8,128)(2,1)}, f32[8,2,768]{2,1,0:T(2,128)}) custom-call(s32[1]{0:T(128)} %bitcast.1.first, bf16[8,768,256]{2,1,0:T(8,128)(2,1)} %bitcast.10, bf16[8,1792,256]{2,1,0:T(8,128)(2,1)} %all-to-all-done.parcel_ref, f32[768,512]{1,0:T(8,128)} %whole_conv.1.before_ref), custom_call_target="tpu_custom_call" | custom-call | flops 1610612736 | bytes 7340032 | tf_op jit(solution)/shard_map/whole_last/pallas_call | solution.py:449
  172.0 4.1 %all-to-all-start.1 = ((f32[8,2,768]{2,1,0:T(2,128)}), f32[8,2,768]{2,1,0:T(2,128)S(1)}, u32[]{:S(2)}, u32[]{:S(2)}) async-start(f32[8,2,768]{2,1,0:T(2,128)} %get-tuple-element.26), calls=%async_computation.1 | async-start | bytes 98304 | tf_op jit(solution)/shard_map/all_to_all | solution.py:593
  176.1 0.0 copy-done.2
  176.1 0.6 reshape.15.gain_ref
  176.7 4.2 %all-to-all-done.1.sums_ref = f32[8,2,768]{2,1,0:T(2,128)S(1)} async-done(((f32[8,2,768]{2,1,0:T(2,128)}), f32[8,2,768]{2,1,0:T(2,128)S(1)}, u32[]{:S(2)}, u32[]{:S(2)}) %all-to-all-start.1) | async-done | bytes 49184 | tf_op jit(solution)/shard_map/all_to_all | solution.py:593
  180.9 0.6 copy-done
  181.5 3.2 %norm.1 = bf16[768,512]{1,0:T(8,128)(2,1)} custom-call(s32[1]{0:T(128)} %bitcast.own, bf16[768,512]{1,0:T(8,128)(2,1)} %get-tuple-element.25.mix_ref, f32[8,2,768]{2,1,0:T(2,128)} %copy-done, bf16[1,4096]{1,0:T(2,128)(2,1)} %reshape.15.gain_ref), custom_call_target="tpu_custom_call" | custom-call | tf_op jit(solution)/shard_map/norm/pallas_call | solution.py:504
  (2 shorter events, 0.0 us)
Async XLA Ops:
  6.5 65.6 %all-gather.9.cloned.1.call-start = ((), (), s32[]{:S(2)}) async-start(), calls=%async_computation.3 | async-start | bytes 3538944 | tf_op jit(solution)/shard_map/all_gather | solution.py:568
  18.1 24.8 %copy-start.3 = (f32[2]{0:T(128)S(1)}, f32[2]{0:T(128)}, u32[]{:S(2)}) copy-start(f32[2]{0:T(128)} %param.25) | copy-start | bytes 28
  18.1 26.3 %copy-start.4 = (bf16[16,4096]{1,0:T(8,128)(2,1)S(1)}, bf16[16,4096]{1,0:T(8,128)(2,1)}, u32[]{:S(2)}) copy-start(bf16[16,4096]{1,0:T(8,128)(2,1)} %get-tuple-element.24) | copy-start | bytes 393220
  18.1 19.9 %collective-permute-start.2 = (bf16[768,384]{1,0:T(8,128)(2,1)}, bf16[768,384]{1,0:T(8,128)(2,1)S(1)}, u32[]{:S(2)}, u32[]{:S(2)}) collective-permute-start(bf16[768,384]{1,0:T(8,128)(2,1)} %get-tuple-element.17), channel_id=1, source_target_pairs={{0,0},{1,64},{32,1},{33,65},{64,33},{65,97},{96,32},{97,96},{2,2},... | collective-permute-start | bytes 1769480 | tf_op jit(solution)/shard_map/ppermute | solution.py:549
  25.1 16.0 %collective-permute-start.1 = (bf16[768,384]{1,0:T(8,128)(2,1)}, bf16[768,384]{1,0:T(8,128)(2,1)S(1)}, u32[]{:S(2)}, u32[]{:S(2)}) collective-permute-start(bf16[768,384]{1,0:T(8,128)(2,1)} %get-tuple-element.16), channel_id=1, source_target_pairs={{0,32},{1,96},{32,33},{33,97},{64,1},{65,65},{96,0},{97,64},{2,34}... | collective-permute-start | bytes 1769480 | tf_op jit(solution)/shard_map/ppermute | solution.py:550
  42.1 59.2 %all-gather.7.cloned.1.call-start = ((), (), s32[]{:S(2)}) async-start(), calls=%async_computation.2 | async-start | bytes 3538944 | tf_op jit(solution)/shard_map/all_gather | solution.py:569
  42.9 5.2 %collective-permute-start = (f32[2]{0:T(128)S(1)}, f32[2]{0:T(128)S(1)}, u32[]{:S(2)}, u32[]{:S(2)}) collective-permute-start(f32[2]{0:T(128)S(1)} %copy-done.3), channel_id=1, source_target_pairs={{0,1},{1,0},{2,3},{3,2},{4,5},{5,4},{6,7},{7,6},{8,9},{9,8},{10,11... | collective-permute-start | bytes 32 | tf_op jit(solution)/shard_map/ppermute | solution.py:542
  44.4 5.9 %collective-permute-start.5 = (bf16[16,4096]{1,0:T(8,128)(2,1)S(1)}, bf16[16,4096]{1,0:T(8,128)(2,1)S(1)}, u32[]{:S(2)}, u32[]{:S(2)}) collective-permute-start(bf16[16,4096]{1,0:T(8,128)(2,1)S(1)} %copy-done.4), channel_id=1, source_target_pairs={{0,8},{8,16},{16,24},{24,32},{32,40},{40,48},{48,56},{56,64},{64,7... | collective-permute-start | bytes 393224 | tf_op jit(solution)/shard_map/ppermute | solution.py:548
  50.3 0.7 copy-start.1
  63.8 96.1 %all-to-all-start = ((bf16[8,1792,256]{2,1,0:T(8,128)(2,1)}), bf16[8,1792,256]{2,1,0:T(8,128)(2,1)}, u32[]{:S(2)}, u32[]{:S(2)}) async-start(bf16[8,1792,256]{2,1,0:T(8,128)(2,1)} %gated_conv.1), calls=%async_computation | async-start | bytes 14680064 | tf_op jit(solution)/shard_map/all_to_all | solution.py:561
  69.4 97.3 %all-gather.11.cloned.1.call-start = ((), (), s32[]{:S(2)}) async-start(), calls=%async_computation.4 | async-start | bytes 3538944 | tf_op jit(solution)/shard_map/all_gather | solution.py:590
  108.1 14.3 %collective-permute-start.4 = (bf16[768,128]{1,0:T(8,128)(2,1)}, bf16[768,128]{1,0:T(8,128)(2,1)S(1)}, u32[]{:S(2)}, u32[]{:S(2)}) collective-permute-start(bf16[768,128]{1,0:T(8,128)(2,1)} %get-tuple-element.23), channel_id=1, source_target_pairs={{32,0},{96,1},{33,32},{97,33},{1,64},{65,65},{0,96},{64,97},{34,2}... | collective-permute-start | bytes 589832 | tf_op jit(solution)/shard_map/ppermute | solution.py:589
  118.7 8.7 %collective-permute-start.3 = (bf16[768,128]{1,0:T(8,128)(2,1)}, bf16[768,128]{1,0:T(8,128)(2,1)S(1)}, u32[]{:S(2)}, u32[]{:S(2)}) collective-permute-start(bf16[768,128]{1,0:T(8,128)(2,1)} %get-tuple-element.22), channel_id=1, source_target_pairs={{0,0},{64,1},{1,32},{65,33},{33,64},{97,65},{32,96},{96,97},{2,2},... | collective-permute-start | bytes 589832 | tf_op jit(solution)/shard_map/ppermute | solution.py:588
  166.7 9.4 %copy-start.2 = (bf16[4096]{0:T(1024)(128)(2,1)S(1)}, bf16[4096]{0:T(1024)(128)(2,1)}, u32[]{:S(2)}) copy-start(bf16[4096]{0:T(1024)(128)(2,1)} %param.29) | copy-start | bytes 24580
  172.0 8.9 %all-to-all-start.1 = ((f32[8,2,768]{2,1,0:T(2,128)}), f32[8,2,768]{2,1,0:T(2,128)S(1)}, u32[]{:S(2)}, u32[]{:S(2)}) async-start(f32[8,2,768]{2,1,0:T(2,128)} %get-tuple-element.26), calls=%async_computation.1 | async-start | bytes 98304 | tf_op jit(solution)/shard_map/all_to_all | solution.py:593
  180.9 0.6 copy-start
Sparse Core Ops, SparseCore 0:
  42.2 29.7 all-gather.8
  73.8 27.5 all-gather.6
  128.4 38.2 all-gather.10

commit v3 on v1

--- a/solution.py
+++ b/solution.py
@@ -100,32 +100,28 @@
     return rotated
 
 
-def kv_kernel(
-    where, h_ref, wk_ref, wv_ref, cr, sr, cs, ss, kva_ref, kvb_ref, acc, hb, kb, vb, sem
+def qkv_kernel(
+    where, h_ref, wk_ref, wv_ref, wq_ref, cr, sr, cs, ss, a_ref, b_ref, rim_ref, acc, hb, kb, vb, qb, sem
 ):
     streamed_products(
-        ((h_ref, hb, True), (wk_ref, kb, False), (wv_ref, vb, False)),
+        ((h_ref, hb, True), (wk_ref, kb, False), (wv_ref, vb, False), (wq_ref, qb, False)),
         sem,
-        ((acc, hb, (kb, vb)),),
-    )
+        ((acc, hb, (kb, vb, qb)),),
+    )
+    for k in range(STEPS):
+        rim_ref[:, k * CHUNK : (k + 1) * CHUNK] = hb[k, ROWS - HALO :, :]
     rotated = rotation(cr, sr, cs, ss)
-    keys = [rotated(acc[0, :, i * 128 : i * 128 + 128]).astype(jnp.bfloat16) for i in range(2)]
-    vals = [acc[1, :, i * 128 : i * 128 + 128].astype(jnp.bfloat16) for i in range(2)]
-    for flip, kv_ref in ((0, kva_ref), (1, kvb_ref)):
-        take = where[1] == flip
-        kv_ref[:, 0:128] = jnp.where(take, keys[0], keys[1])
-        kv_ref[:, 128:256] = jnp.where(take, vals[0], vals[1])
-
-
-def q_kernel(where, h_ref, wq_ref, cr, sr, cs, ss, _, qa_ref, qb_ref, acc, hb, qb, sem):
-    streamed_products(((h_ref, hb, True), (wq_ref, qb, False)), sem, ((acc, hb, (qb,)),))
-    rotated = rotation(cr, sr, cs, ss)
-    queries = [
-        (rotated(acc[0, :, i * 128 : i * 128 + 128]) * (LOG2E / 8)).astype(jnp.bfloat16)
-        for i in range(2)
-    ]
-    for flip, q_ref in ((0, qa_ref), (1, qb_ref)):
-        q_ref[...] = jnp.where(where[1] == flip, queries[0], queries[1])
+    heads = []
+    for i in range(2):
+        cols = slice(i * 128, i * 128 + 128)
+        query = rotated(acc[2, :, cols]) * (LOG2E / 8)
+        parts = (rotated(acc[0, :, cols]), acc[1, :, cols], query)
+        heads.append([part.astype(jnp.bfloat16) for part in parts])
+    for flip, o_ref in ((0, a_ref), (1, b_ref)):
+        for i in range(3):
+            o_ref[:, i * 128 : i * 128 + 128] = jnp.where(
+                where[1] == flip, heads[0][i], heads[1][i]
+            )
 
 
 def in_hbm():
@@ -143,34 +139,27 @@
     )
 
 
-def project(kernel, width, where, hidden, weights, unread=()):
+def project(where, hidden, w_key, w_value, w_query):
     row_cos, row_sin, start_cos, start_sin = rotary_tables()
     table = pl.BlockSpec((GROUP, 128), lambda k, *_: (0, 0))
     starts = pl.BlockSpec((ROWS // GROUP, 128), lambda k, where: (where[0], 0))
-    out = jax.ShapeDtypeStruct((ROWS, width), jnp.bfloat16)
-    count = len(weights)
+    shapes = ((ROWS, 384), (ROWS, 384), (HALO, D))
     return pl.pallas_call(
-        kernel,
-        out_shape=(out, out),
+        qkv_kernel,
+        out_shape=tuple(jax.ShapeDtypeStruct(shape, jnp.bfloat16) for shape in shapes),
         grid_spec=pltpu.PrefetchScalarGridSpec(
             num_scalar_prefetch=1,
             grid=(1,),
-            in_specs=[in_hbm()] * (1 + count)
-            + [table, table, starts, starts]
-            + [in_hbm()] * len(unread),
-            out_specs=(pl.BlockSpec((ROWS, width), lambda k, *_: (0, 0)),) * 2,
-            scratch_shapes=[
-                pltpu.VMEM((count, ROWS, 256), jnp.float32),
-                *stream_buffers(count, False),
-            ],
+            in_specs=[in_hbm()] * 4 + [table, table, starts, starts],
+            out_specs=tuple(pl.BlockSpec(shape, lambda k, *_: (0, 0)) for shape in shapes),
+            scratch_shapes=[pltpu.VMEM((3, ROWS, 256), jnp.float32), *stream_buffers(3, False)],
         ),
         compiler_params=pltpu.CompilerParams(vmem_limit_bytes=60 * 2**20),
         cost_estimate=pl.CostEstimate(
-            flops=2 * ROWS * D * 256 * count,
-            bytes_accessed=(6 + 2 * count) * 2**20,
-            transcendentals=0,
-        ),
-    )(where, hidden, *weights, row_cos, row_sin, start_cos, start_sin, *unread)
+            flops=2 * ROWS * D * 768, bytes_accessed=13 * 2**20, transcendentals=0
+        ),
+        name="qkv",
+    )(where, hidden, w_key, w_value, w_query, row_cos, row_sin, start_cos, start_sin)
 
 
 def conv_kernel(
@@ -272,21 +261,24 @@
     acc[:, rows, :] = acc[:, rows, :] * alpha + pv.reshape(2, n, 128)
 
 
-def attend_blocks(first, count, place_of, refs):
+def attend_blocks(first, count, slot_of, ready, refs):
     def block(kb):
-        place = place_of(kb)
         for j in range(ROWS // KEYS_AT_ONCE):
-            attend(*refs, 0, ROWS, place, j * KEYS_AT_ONCE, KEYS_AT_ONCE, False)
+            attend(*refs, 0, ROWS, slot_of(kb), j * KEYS_AT_ONCE, KEYS_AT_ONCE, False)
 
     def body(pair, carry):
-        block(first + 2 * pair)
-        block(first + 2 * pair + 1)
+        kb = first + 2 * pair
+        ready(kb)
+        ready(kb + 1)
+        block(kb)
+        block(kb + 1)
         return carry
 
     lax.fori_loop(0, count // 2, body, 0)
 
     @pl.when(count % 2 == 1)
     def _():
+        ready(first + count - 1)
         block(first + count - 1)
 
 
@@ -311,28 +303,54 @@
     return (kb % 4) * 2 + 3 - kb // 4
 
 
-def low_kernel(own, lam, qa_ref, qb_ref, kv_ref, gain_ref, _, o_ref, m_o, l_o, a_o, qz):
+def low_kernel(own, lam, ql_ref, qh_ref, gain_ref, kv_hbm, _, o_ref, m_o, l_o, a_o, qz, kv_ref, sem):
     step = pl.program_id(0)
-    split_maps(jnp.where(step == own[2], qa_ref[...], qb_ref[...]), qz)
+
+    def load(kb):
+        return pltpu.make_async_copy(kv_hbm.at[low_place(kb)], kv_ref.at[kb], sem.at[kb])
+
+    @pl.when(step == 0)
+    def _():
+        for kb in range(8):
+            load(kb).start()
+
+    def ready(kb):
+        @pl.when(jnp.logical_or(step == 0, kb > own[0]))
+        def _():
+            load(kb).wait()
+
+    split_maps(jnp.where(step == 0, ql_ref[...], qh_ref[...]), qz)
     start_state(m_o, l_o, a_o)
     refs = (qz, kv_ref, m_o, l_o, a_o)
-    attend_blocks(0, jnp.where(step == 0, own[0], 8), low_place, refs)
+    attend_blocks(0, jnp.where(step == 0, own[0], 8), lambda kb: kb, ready, refs)
 
     @pl.when(step == 0)
     def _():
-        attend_diagonal(low_place(own[0]), refs)
+        load(own[0]).wait()
+        attend_diagonal(own[0], refs)
         o_ref[...] = finish(lam, gain_ref, l_o, a_o)
 
 
 def high_kernel(
-    own, lam, qa_ref, qb_ref, kv_ref, gain_ref, low_ref, m_i, l_i, a_i, _, oa_ref, ob_ref, qz
+    own, lam, qh_ref, gain_ref, low_ref, m_i, l_i, a_i, kv_hbm, oa_ref, ob_ref, qz, kv_ref, sem
 ):
+    def load(kb):
+        slot = kb - 8
+        return pltpu.make_async_copy(kv_hbm.at[high_place(kb)], kv_ref.at[slot], sem.at[slot])
+
+    for kb in range(8, 16):
+
+        @pl.when(kb <= own[1])
+        def _(kb=kb):
+            load(kb).start()
+
+    split_maps(qh_ref[...], qz)
+    refs = (qz, kv_ref, m_i, l_i, a_i)
+    attend_blocks(8, own[1] - 8, lambda kb: kb - 8, lambda kb: load(kb).wait(), refs)
+    load(own[1]).wait()
+    attend_diagonal(own[1] - 8, refs)
+    high = finish(lam, gain_ref, l_i, a_i)
     low_first = own[2] == 0
-    split_maps(jnp.where(low_first, qb_ref[...], qa_ref[...]), qz)
-    refs = (qz, kv_ref, m_i, l_i, a_i)
-    attend_blocks(8, own[1] - 8, high_place, refs)
-    attend_diagonal(high_place(own[1]), refs)
-    high = finish(lam, gain_ref, l_i, a_i)
     oa_ref[...] = jnp.where(low_first, low_ref[...], high)
     ob_ref[...] = jnp.where(low_first, high, low_ref[...])
 
@@ -349,7 +367,11 @@
             grid=(steps,),
             in_specs=[full(a.shape) for a in args[2:]] + [in_hbm() for _ in unread],
             out_specs=tuple(full(o.shape) for o in outs),
-            scratch_shapes=[pltpu.VMEM((2, ROWS, 128), jnp.bfloat16)],
+            scratch_shapes=[
+                pltpu.VMEM((2, ROWS, 128), jnp.bfloat16),
+                pltpu.VMEM((8, ROWS, 256), jnp.bfloat16),
+                pltpu.SemaphoreType.DMA((8,)),
+            ],
         ),
         compiler_params=pltpu.CompilerParams(vmem_limit_bytes=60 * 2**20),
         cost_estimate=pl.CostEstimate(
@@ -435,9 +457,8 @@
             ones, values, (((1,), (1,)), ((), ())), preferred_element_type=jnp.float32
         )
 
-    row = lax.broadcasted_iota(jnp.int32, (8, ROWS), 0)
-    squares = jnp.where(row == 1, row_sums(high) + row_sums(low), 0.0)
-    sums = jnp.where(row == 0, row_sums(mix), squares)
+    squares = row_sums(high) + row_sums(low)
+    sums = jnp.concatenate([row_sums(mix)[0:1], squares[0:1]], axis=0)
     for copy in range(8):
         sums_ref[copy] = sums
 
@@ -467,7 +488,7 @@
         whole_last_kernel,
         out_shape=(
             jax.ShapeDtypeStruct((ROWS, width), jnp.bfloat16),
-            jax.ShapeDtypeStruct((8, 8, ROWS), jnp.float32),
+            jax.ShapeDtypeStruct((8, 2, ROWS), jnp.float32),
         ),
         grid_spec=pltpu.PrefetchScalarGridSpec(
             num_scalar_prefetch=1,
@@ -475,7 +496,7 @@
             in_specs=[in_hbm(), in_hbm(), in_hbm()],
             out_specs=(
                 pl.BlockSpec((ROWS, width), lambda i, *_: (0, 0)),
-                pl.BlockSpec((8, 8, ROWS), lambda i, *_: (0, 0, 0)),
+                pl.BlockSpec((8, 2, ROWS), lambda i, *_: (0, 0, 0)),
             ),
             scratch_shapes=[
                 pltpu.VMEM((8, ROWS, 256), jnp.bfloat16),
@@ -493,13 +514,12 @@
 
 
 def norm_kernel(own, mix_ref, sums_ref, gain_ref, o_ref):
-    sums = sums_ref[...].reshape(64, ROWS)
-    row = lax.broadcasted_iota(jnp.int32, (64, 128), 0) % 8
+    ones = jnp.ones((8, 128), jnp.float32)
 
     def column(which):
         total = lax.dot_general(
-            sums,
-            jnp.where(row == which, 1.0, 0.0),
+            sums_ref[:, which, :],
+            ones,
             (((0,), (0,)), ((), ())),
             preferred_element_type=jnp.float32,
             precision=lax.Precision.HIGHEST,
@@ -557,34 +577,28 @@
     sp = z * 4 + x
 
     z_core = ("z", "c")
-    rim = lax.ppermute(hidden_states[ROWS - HALO :], ("z", "x"), [(i, i + 1) for i in range(15)])
     other_lambdas = lax.ppermute(lambdas, "c", [(0, 1), (1, 0)])
 
     first = jnp.where(z < 2, 0, 1).astype(jnp.int32).reshape(1)
     where = jnp.stack([sp, jnp.where(z < 2, 0, 1)]).astype(jnp.int32)
     route_a, route_b = forward_route(0), forward_route(1)
-    kv_a, kv_b = project(kv_kernel, 256, where, hidden_states, (w_key, w_value))
+    head_a, head_b, last_rows = project(where, hidden_states, w_key, w_value, w_query)
+    rim = lax.ppermute(last_rows, ("z", "x"), [(i, i + 1) for i in range(15)])
+    head_a = lax.ppermute(head_a, z_core, route_a)
+    head_b = lax.ppermute(head_b, z_core, route_b)
     blocks = column_blocks(w_out_conv, w_out_attn)
-    q_a, q_b = project(q_kernel, 128, where, hidden_states, (w_query,), (kv_a,))
-    kv_a = lax.ppermute(kv_a, z_core, route_a)
-    kv_b = lax.ppermute(kv_b, z_core, route_b)
-    q_a = lax.ppermute(q_a, z_core, route_a)
-    q_b = lax.ppermute(q_b, z_core, route_b)
+    w_out = lax.all_to_all(blocks, ("y", "c"), split_axis=0, concat_axis=0, tiled=True)
     even = (z % 2) == 0
-    kv_low, kv_high = jnp.where(even, kv_a, kv_b), jnp.where(even, kv_b, kv_a)
+    kv, q = slice(0, 256), slice(256, 384)
+    kv_low = jnp.where(even, head_a[:, kv], head_b[:, kv])
+    kv_high = jnp.where(even, head_b[:, kv], head_a[:, kv])
+    q_low = jnp.where(even, head_a[:, q], head_b[:, q])
+    q_high = jnp.where(even, head_b[:, q], head_a[:, q])
     kv_low = lax.all_gather(kv_low, ("x", "c"), axis=0)
     kv_high = lax.all_gather(kv_high, ("x", "c"), axis=0)
 
     conv_out = gated_conv(hidden_states, rim, w_conv_b, w_conv_c, w_conv_h, conv_taps)
     conv_all = lax.all_gather(conv_out, ("y", "c"), axis=0)
-
-    w_out = lax.all_to_all(
-        blocks,
-        ("y", "c"),
-        split_axis=0,
-        concat_axis=0,
-        tiled=True,
-    )
 
     plane_lambdas = jnp.where(
         core == 0,
@@ -598,15 +612,10 @@
     rows = jax.ShapeDtypeStruct((ROWS, VD), jnp.bfloat16)
     state = (jax.ShapeDtypeStruct((2, ROWS, VD), jnp.float32),) * 3
     o_low, *carried = attention_call(
-        low_kernel, 2, (own, lam, q_a, q_b, kv_low, gain), (rows, *state), (conv_out,), 12
+        low_kernel, 2, (own, lam, q_low, q_high, gain), (rows, *state), (kv_low, conv_out), 12
     )
     o_a, o_b = attention_call(
-        high_kernel,
-        1,
-        (own, lam, q_a, q_b, kv_high, gain, o_low, *carried),
-        (rows, rows),
-        (w_out,),
-        6,
+        high_kernel, 1, (own, lam, q_high, gain, o_low, *carried), (rows, rows), (kv_high,), 6
     )
     back_a = lax.ppermute(o_a, z_core, reverse(route_a))
     back_b = lax.ppermute(o_b, z_core, reverse(route_b))

time: 201 us -> 232 us (1.15); the launches traced: 200 us -> 228 us
  blocking collectives: 0 us -> 65.7 us
  starting transfers between devices: 49.5 us -> 32.6 us
  waiting for transfers between devices: 55 us -> 40.4 us
  Pallas kernels: 75.1 us -> 70.1 us
    all_to_all x0 -> x1, blocking collectives: none -> 65.7 us  [per_device(): lax.all_to_all(blocks, ('y', 'c'), split_axis=0, concat_axis=0, tiled=True)]
    all_gather x1, waiting for transfers between devices: 22.5 us -> 0.01 us  [per_device(): lax.all_gather(jnp.concatenate([back_a, back_b], axis=1), ('y', 'c'), axi...]
    ppermute x5 -> x3, starting transfers between devices: 22.5 us -> 12.8 us  [the longest x1 7.01 us: per_device(): head_a = lax.ppermute(head_a, z_core, route_a)]
    all_gather x1, waiting for transfers between devices: 0.01 us -> 7.75 us  [per_device(): kv_low = lax.all_gather(kv_low, ('x', 'c'), axis=0)]
    all_to_all x1 -> x0, starting transfers between devices: 7.02 us -> none  [per_device(): lax.all_to_all(blocks, ('y', 'c'), split_axis=0, concat_axis=0, tiled=True)]
    all_to_all x1 -> x0, waiting for transfers between devices: 5.36 us -> none  [per_device(): lax.all_to_all(blocks, ('y', 'c'), split_axis=0, concat_axis=0, tiled=True)]
    all_gather x1, waiting for transfers between devices: 0.01 us -> 5.35 us  [per_device(): kv_high = lax.all_gather(kv_high, ('x', 'c'), axis=0)]
    ppermute x1, waiting for transfers between devices: 0.01 us -> 5.01 us  [per_device(): back_a = lax.ppermute(o_a, z_core, reverse(route_a))]
  transfers between devices with their start and end apart: 14 -> 11, of which waited for: 8 -> 9; matrix products, arithmetic and copies ran while one was open for 2% -> 2% of each run, Pallas kernels for 29% -> 22%
where the time goes in v3:
time: 232 us; the launch traced here: 228 us
  Pallas kernels  70.1 us (30%)
  blocking collectives  65.7 us (28%)
  waiting for transfers between devices  40.4 us (17%)
  starting transfers between devices  32.6 us (14%)
  between operations  13.3 us (6%)
  other arithmetic  3.8 us (2%)
  local copies, waits for them, and re-layouts  2.51 us (1%)
    all_to_all x1, blocking collectives, per_device(): lax.all_to_all(blocks, ('y', 'c'), split_axis=0, concat_axis=0, tiled=True)  65.7 us
    pallas_call x2, Pallas kernels, attention_call(): pl.pallas_call(kernel, out_shape=outs, grid_spec=pltpu.PrefetchScalarGrid...  30.7 us
    ppermute x1, starting transfers between devices, per_device(): back_b = lax.ppermute(o_b, z_core, reverse(route_b))  10.9 us
    pallas_call x1, Pallas kernels, project(): pl.pallas_call(qkv_kernel, out_shape=tuple((jax.ShapeDtypeStruct(shape, j...  10.9 us
    pallas_call x1, Pallas kernels, gated_conv(): pl.pallas_call(conv_kernel, out_shape=jax.ShapeDtypeStruct((ROWS, 256), j...  10.6 us
    ppermute x1, waiting for transfers between devices, per_device(): head_a = lax.ppermute(head_a, z_core, route_a)  10.3 us
    all_gather x1, waiting for transfers between devices, per_device(): kv_low = lax.all_gather(kv_low, ('x', 'c'), axis=0)  7.75 us
    ppermute x1, starting transfers between devices, per_device(): head_a = lax.ppermute(head_a, z_core, route_a)  7.01 us
  transfers between devices with their start and end apart: 11, of which 9 were waited for; matrix products, arithmetic and copies ran while one was open for 2% of the time, Pallas kernels for 22%

profile of v3, /device:TPU:1, one launch (start us, length us, event | category | flops | bytes accessed | tf_op | source)
XLA Modules:
  0.0 228.4 jit_solution(9818313575448469131)
XLA Ops:
  6.5 0.0 all-gather.9.cloned.1.call-start
  6.5 0.6 pad_add_fusion.1.where
  7.2 10.9 %qkv.1 = (bf16[768,384]{1,0:T(8,128)(2,1)}, bf16[768,384]{1,0:T(8,128)(2,1)}, bf16[16,4096]{1,0:T(8,128)(2,1)}) custom-call(s32[2]{0:T(128)} %pad_add_fusion.1.where, bf16[768,4096]{1,0:T(8,128)(2,1)} %h_ref.3, bf16[4096,256]{1,0:T(8,128)(2,1)} %wk_ref.1, bf16[4096,256]{1,0:T(8,128)(2,1)} %wv_ref.1, bf16[4096,256]{1,0:T(8,128)(2,1)} %wq_ref.1, ...), custom_call_target="tpu_custom_call" | custom-call | flops 4831838208 | bytes 13631488 | tf_op jit(solution)/shard_map/qkv/pallas_call | solution.py:147
  18.1 0.0 copy-start.3
  18.1 7.0 %collective-permute-start.2 = (bf16[768,384]{1,0:T(8,128)(2,1)}, bf16[768,384]{1,0:T(8,128)(2,1)S(1)}, u32[]{:S(2)}, u32[]{:S(2)}) collective-permute-start(bf16[768,384]{1,0:T(8,128)(2,1)} %get-tuple-element.17), channel_id=1, source_target_pairs={{0,0},{1,64},{32,1},{33,65},{64,33},{65,97},{96,32},{97,96},{2,2},... | collective-permute-start | bytes 1769480 | tf_op jit(solution)/shard_map/ppermute | solution.py:587
  25.1 2.6 %collective-permute-start.1 = (bf16[768,384]{1,0:T(8,128)(2,1)}, bf16[768,384]{1,0:T(8,128)(2,1)S(1)}, u32[]{:S(2)}, u32[]{:S(2)}) collective-permute-start(bf16[768,384]{1,0:T(8,128)(2,1)} %get-tuple-element.16), channel_id=1, source_target_pairs={{0,32},{1,96},{32,33},{33,97},{64,1},{65,65},{96,0},{97,64},{2,34}... | collective-permute-start | bytes 1769480 | tf_op jit(solution)/shard_map/ppermute | solution.py:588
  27.8 10.3 %collective-permute-done.2 = bf16[768,384]{1,0:T(8,128)(2,1)S(1)} collective-permute-done((bf16[768,384]{1,0:T(8,128)(2,1)}, bf16[768,384]{1,0:T(8,128)(2,1)S(1)}, u32[]{:S(2)}, u32[]{:S(2)}) %collective-permute-start.2) | collective-permute-done | bytes 589856 | tf_op jit(solution)/shard_map/ppermute | solution.py:587
  38.0 3.1 %collective-permute-done.1 = bf16[768,384]{1,0:T(8,128)(2,1)S(1)} collective-permute-done((bf16[768,384]{1,0:T(8,128)(2,1)}, bf16[768,384]{1,0:T(8,128)(2,1)S(1)}, u32[]{:S(2)}, u32[]{:S(2)}) %collective-permute-start.1) | collective-permute-done | bytes 589856 | tf_op jit(solution)/shard_map/ppermute | solution.py:588
  41.1 0.9 broadcast_select_fusion
  42.1 0.0 all-gather.9.cloned.1.call-update
  42.1 0.0 all-gather.11.cloned.1.call-start
  42.1 0.7 all-gather.11.cloned.1.call-update
  42.8 0.0 all-gather.15.cloned.1.call-start
  42.9 0.0 copy-done.3
  42.9 0.0 copy-start.2
  42.9 3.1 %collective-permute-start.3 = (bf16[16,4096]{1,0:T(8,128)(2,1)S(1)}, bf16[16,4096]{1,0:T(8,128)(2,1)S(1)}, u32[]{:S(2)}, u32[]{:S(2)}) collective-permute-start(bf16[16,4096]{1,0:T(8,128)(2,1)S(1)} %copy-done.3), channel_id=1, source_target_pairs={{0,8},{8,16},{16,24},{24,32},{32,40},{40,48},{48,56},{56,64},{64,7... | collective-permute-start | bytes 393224 | tf_op jit(solution)/shard_map/ppermute | solution.py:586
  46.0 1.9 collective-permute-done.3.rim_ref
  48.0 0.7 copy-done.4
  48.6 10.6 %gated_conv.1._ = bf16[768,256]{1,0:T(8,128)(2,1)} custom-call(bf16[768,4096]{1,0:T(8,128)(2,1)} %h_ref.3, bf16[16,4096]{1,0:T(8,128)(2,1)} %copy-done.4, bf16[4096,256]{1,0:T(8,128)(2,1)} %wb_ref.1, bf16[4096,256]{1,0:T(8,128)(2,1)} %wc_ref.2, bf16[4096,256]{1,0:T(8,128)(2,1)} %wh_ref.1, bf16[3,256]{1,0:T(4,128)(2,1)} %taps_ref.1), custom_call_target="tpu_custom_call" | custom-call | flops 4831838208 | bytes 13631488 | tf_op jit(solution)/shard_map/gated_conv/pallas_call | solution.py:193
  59.3 0.0 all-gather.15.cloned.1.call-update
  59.3 0.0 all-gather.13.cloned.1.call-start
  59.3 0.0 copy-done.2
  59.3 2.6 %collective-permute-start = (f32[2]{0:T(128)S(1)}, f32[2]{0:T(128)S(1)}, u32[]{:S(2)}, u32[]{:S(2)}) collective-permute-start(f32[2]{0:T(128)S(1)} %copy-done.2), channel_id=1, source_target_pairs={{0,1},{1,0},{2,3},{3,2},{4,5},{5,4},{6,7},{7,6},{8,9},{9,8},{10,11... | collective-permute-start | bytes 32 | tf_op jit(solution)/shard_map/ppermute | solution.py:580
  61.9 0.6 pad_add_fusion.own
  62.5 0.2 collective-permute-done
  62.7 0.1 broadcast_select_fusion.4
  62.8 0.6 dynamic_slice.3.lam
  63.4 0.8 broadcast_select_fusion.2
  64.2 7.7 %all-gather.9.cloned.1.call-done = bf16[6144,256]{1,0:T(8,128)(2,1)} async-done(((bf16[768,256]{1,0:T(8,128)(2,1)}), bf16[6144,256]{1,0:T(8,128)(2,1)}) %all-gather.9.cloned.1.call-update) | async-done | bytes 3145744 | tf_op jit(solution)/shard_map/all_gather | solution.py:597
  71.9 24.0 %shard_map.163 = (bf16[768,128]{1,0:T(8,128)(2,1)}, f32[2,768,128]{2,1,0:T(8,128)}, f32[2,768,128]{2,1,0:T(8,128)}, f32[2,768,128]{2,1,0:T(8,128)}) custom-call(s32[3]{0:T(128)} %pad_add_fusion.own, f32[1]{0:T(128)} %dynamic_slice.3.lam, bf16[768,128]{1,0:T(8,128)(2,1)} %get-tuple-element.29.ql_ref, bf16[768,128]{1,0:T(8,128)(2,1)} %get-tuple-element.30.qh_ref, ...), custom_call_target="tpu_custom_call" | custom-call | flops 24000000000 | bytes 4194304 | tf_op jit(solution)/shard_map/pallas_call | solution.py:362
  96.0 5.4 %all-gather.11.cloned.1.call-done = bf16[6144,256]{1,0:T(8,128)(2,1)} async-done(((bf16[768,256]{1,0:T(8,128)(2,1)}), bf16[6144,256]{1,0:T(8,128)(2,1)}) %all-gather.11.cloned.1.call-update) | async-done | bytes 3145744 | tf_op jit(solution)/shard_map/all_gather | solution.py:598
  101.3 6.7 %shard_map.164 = (bf16[768,128]{1,0:T(8,128)(2,1)}, bf16[768,128]{1,0:T(8,128)(2,1)}) custom-call(s32[3]{0:T(128)} %pad_add_fusion.own, f32[1]{0:T(128)} %dynamic_slice.3.lam, bf16[768,128]{1,0:T(8,128)(2,1)} %get-tuple-element.30.qh_ref, bf16[1,128]{1,0:T(2,128)(2,1)} %bitcast.16, bf16[768,128]{1,0:T(8,128)(2,1)} %get-tuple-element.19.low_ref, ...), custom_call_target="tpu_custom_call" | custom-call | flops 12000000000 | bytes 4194304 | tf_op jit(solution)/shard_map/pallas_call | solution.py:362
  108.0 10.9 %collective-permute-start.5 = (bf16[768,128]{1,0:T(8,128)(2,1)}, bf16[768,128]{1,0:T(8,128)(2,1)S(1)}, u32[]{:S(2)}, u32[]{:S(2)}) collective-permute-start(bf16[768,128]{1,0:T(8,128)(2,1)} %get-tuple-element.24), channel_id=1, source_target_pairs={{32,0},{96,1},{33,32},{97,33},{1,64},{65,65},{0,96},{64,97},{34,2}... | collective-permute-start | bytes 589832 | tf_op jit(solution)/shard_map/ppermute | solution.py:621
  118.9 1.9 collective-permute-start.4
  120.9 1.8 collective-permute-done.5
  122.7 5.0 %collective-permute-done.4 = bf16[768,128]{1,0:T(8,128)(2,1)S(1)} collective-permute-done((bf16[768,128]{1,0:T(8,128)(2,1)}, bf16[768,128]{1,0:T(8,128)(2,1)S(1)}, u32[]{:S(2)}, u32[]{:S(2)}) %collective-permute-start.4) | collective-permute-done | bytes 196640 | tf_op jit(solution)/shard_map/ppermute | solution.py:620
  127.7 0.8 pad_maximum_fusion
  128.5 0.0 all-gather.13.cloned.1.call-update
  128.5 3.9 %column_blocks.1 = bf16[8,2,256,512]{3,2,1,0:T(8,128)(2,1)} custom-call(bf16[256,4096]{1,0:T(8,128)(2,1)} %wc_ref.3, bf16[256,4096]{1,0:T(8,128)(2,1)} %wa_ref.1), custom_call_target="tpu_custom_call" | custom-call | flops 3000000000 | bytes 9437184 | tf_op jit(solution)/shard_map/column_blocks/pallas_call | solution.py:406
  132.4 65.7 %all_to_all.10.w_ref = bf16[8,2,256,512]{3,2,1,0:T(8,128)(2,1)} all-to-all(bf16[8,2,256,512]{3,2,1,0:T(8,128)(2,1)} %column_blocks.1), channel_id=1, replica_groups=mesh['z'=4,'x'=4,'y'=4,'c'=2] {'y','c'}, dimensions={0} | all-to-all | bytes 8388608 | tf_op jit(solution)/shard_map/all_to_all | solution.py:590
  198.1 5.5 %whole_conv.1.before_ref = f32[768,512]{1,0:T(8,128)} custom-call(bf16[8,768,256]{2,1,0:T(8,128)(2,1)} %bitcast.11, bf16[8,2,256,512]{3,2,1,0:T(8,128)(2,1)} %all_to_all.10.w_ref), custom_call_target="tpu_custom_call" | custom-call | flops 1610612736 | bytes 7340032 | tf_op jit(solution)/shard_map/whole_conv/pallas_call | solution.py:468
  203.6 5.3 %whole_last.1 = (bf16[768,512]{1,0:T(8,128)(2,1)}, f32[8,2,768]{2,1,0:T(2,128)}) custom-call(s32[1]{0:T(128)} %bitcast.1.first, bf16[8,768,256]{2,1,0:T(8,128)(2,1)} %bitcast.12, bf16[8,2,256,512]{3,2,1,0:T(8,128)(2,1)} %all_to_all.10.w_ref, f32[768,512]{1,0:T(8,128)} %whole_conv.1.before_ref), custom_call_target="tpu_custom_call" | custom-call | flops 1610612736 | bytes 7340032 | tf_op jit(solution)/shard_map/whole_last/pallas_call | solution.py:487
  208.9 4.3 %all-to-all-start.1 = ((f32[8,2,768]{2,1,0:T(2,128)}), f32[8,2,768]{2,1,0:T(2,128)S(1)}, u32[]{:S(2)}, u32[]{:S(2)}) async-start(f32[8,2,768]{2,1,0:T(2,128)} %get-tuple-element.26), calls=%async_computation.1 | async-start | bytes 98304 | tf_op jit(solution)/shard_map/all_to_all | solution.py:625
  213.2 0.0 copy-done.1
  213.2 0.6 reshape.15.gain_ref
  213.8 4.2 %all-to-all-done.1.sums_ref = f32[8,2,768]{2,1,0:T(2,128)S(1)} async-done(((f32[8,2,768]{2,1,0:T(2,128)}), f32[8,2,768]{2,1,0:T(2,128)S(1)}, u32[]{:S(2)}, u32[]{:S(2)}) %all-to-all-start.1) | async-done | bytes 49184 | tf_op jit(solution)/shard_map/all_to_all | solution.py:625
  218.0 0.6 copy-done
  218.6 3.2 %norm.1 = bf16[768,512]{1,0:T(8,128)(2,1)} custom-call(s32[1]{0:T(128)} %bitcast.own, bf16[768,512]{1,0:T(8,128)(2,1)} %get-tuple-element.25.mix_ref, f32[8,2,768]{2,1,0:T(2,128)} %copy-done, bf16[1,4096]{1,0:T(2,128)(2,1)} %reshape.15.gain_ref), custom_call_target="tpu_custom_call" | custom-call | tf_op jit(solution)/shard_map/norm/pallas_call | solution.py:542
  (5 shorter events, 0.0 us)
Async XLA Ops:
  6.5 65.4 %all-gather.9.cloned.1.call-start = ((), (), s32[]{:S(2)}) async-start(), calls=%async_computation.2 | async-start | bytes 3538944 | tf_op jit(solution)/shard_map/all_gather | solution.py:597
  18.1 24.8 %copy-start.3 = (bf16[16,4096]{1,0:T(8,128)(2,1)S(1)}, bf16[16,4096]{1,0:T(8,128)(2,1)}, u32[]{:S(2)}) copy-start(bf16[16,4096]{1,0:T(8,128)(2,1)} %get-tuple-element.18) | copy-start | bytes 393220
  18.1 19.9 %collective-permute-start.2 = (bf16[768,384]{1,0:T(8,128)(2,1)}, bf16[768,384]{1,0:T(8,128)(2,1)S(1)}, u32[]{:S(2)}, u32[]{:S(2)}) collective-permute-start(bf16[768,384]{1,0:T(8,128)(2,1)} %get-tuple-element.17), channel_id=1, source_target_pairs={{0,0},{1,64},{32,1},{33,65},{64,33},{65,97},{96,32},{97,96},{2,2},... | collective-permute-start | bytes 1769480 | tf_op jit(solution)/shard_map/ppermute | solution.py:587
  25.1 16.0 %collective-permute-start.1 = (bf16[768,384]{1,0:T(8,128)(2,1)}, bf16[768,384]{1,0:T(8,128)(2,1)S(1)}, u32[]{:S(2)}, u32[]{:S(2)}) collective-permute-start(bf16[768,384]{1,0:T(8,128)(2,1)} %get-tuple-element.16), channel_id=1, source_target_pairs={{0,32},{1,96},{32,33},{33,97},{64,1},{65,65},{96,0},{97,64},{2,34}... | collective-permute-start | bytes 1769480 | tf_op jit(solution)/shard_map/ppermute | solution.py:588
  42.1 59.2 %all-gather.11.cloned.1.call-start = ((), (), s32[]{:S(2)}) async-start(), calls=%async_computation.3 | async-start | bytes 3538944 | tf_op jit(solution)/shard_map/all_gather | solution.py:598
  42.8 155.2 %all-gather.15.cloned.1.call-start = ((), (), s32[]{:S(2)}) async-start(), calls=%async_computation.5 | async-start | bytes 3538944 | tf_op jit(solution)/shard_map/all_gather | solution.py:601
  42.9 16.4 %copy-start.2 = (f32[2]{0:T(128)S(1)}, f32[2]{0:T(128)}, u32[]{:S(2)}) copy-start(f32[2]{0:T(128)} %param.25) | copy-start | bytes 28
  42.9 5.1 %collective-permute-start.3 = (bf16[16,4096]{1,0:T(8,128)(2,1)S(1)}, bf16[16,4096]{1,0:T(8,128)(2,1)S(1)}, u32[]{:S(2)}, u32[]{:S(2)}) collective-permute-start(bf16[16,4096]{1,0:T(8,128)(2,1)S(1)} %copy-done.3), channel_id=1, source_target_pairs={{0,8},{8,16},{16,24},{24,32},{32,40},{40,48},{48,56},{56,64},{64,7... | collective-permute-start | bytes 393224 | tf_op jit(solution)/shard_map/ppermute | solution.py:586
  48.0 0.7 copy-start.4
  59.3 144.3 %all-gather.13.cloned.1.call-start = ((), (), s32[]{:S(2)}) async-start(), calls=%async_computation.4 | async-start | bytes 3538944 | tf_op jit(solution)/shard_map/all_gather | solution.py:622
  59.3 3.4 %collective-permute-start = (f32[2]{0:T(128)S(1)}, f32[2]{0:T(128)S(1)}, u32[]{:S(2)}, u32[]{:S(2)}) collective-permute-start(f32[2]{0:T(128)S(1)} %copy-done.2), channel_id=1, source_target_pairs={{0,1},{1,0},{2,3},{3,2},{4,5},{5,4},{6,7},{7,6},{8,9},{9,8},{10,11... | collective-permute-start | bytes 32 | tf_op jit(solution)/shard_map/ppermute | solution.py:580
  108.0 14.7 %collective-permute-start.5 = (bf16[768,128]{1,0:T(8,128)(2,1)}, bf16[768,128]{1,0:T(8,128)(2,1)S(1)}, u32[]{:S(2)}, u32[]{:S(2)}) collective-permute-start(bf16[768,128]{1,0:T(8,128)(2,1)} %get-tuple-element.24), channel_id=1, source_target_pairs={{32,0},{96,1},{33,32},{97,33},{1,64},{65,65},{0,96},{64,97},{34,2}... | collective-permute-start | bytes 589832 | tf_op jit(solution)/shard_map/ppermute | solution.py:621
  118.9 8.8 %collective-permute-start.4 = (bf16[768,128]{1,0:T(8,128)(2,1)}, bf16[768,128]{1,0:T(8,128)(2,1)S(1)}, u32[]{:S(2)}, u32[]{:S(2)}) collective-permute-start(bf16[768,128]{1,0:T(8,128)(2,1)} %get-tuple-element.23), channel_id=1, source_target_pairs={{0,0},{64,1},{1,32},{65,33},{33,64},{97,65},{32,96},{96,97},{2,2},... | collective-permute-start | bytes 589832 | tf_op jit(solution)/shard_map/ppermute | solution.py:620
  203.6 9.6 %copy-start.1 = (bf16[4096]{0:T(1024)(128)(2,1)S(1)}, bf16[4096]{0:T(1024)(128)(2,1)}, u32[]{:S(2)}) copy-start(bf16[4096]{0:T(1024)(128)(2,1)} %param.29) | copy-start | bytes 24580
  208.9 9.1 %all-to-all-start.1 = ((f32[8,2,768]{2,1,0:T(2,128)}), f32[8,2,768]{2,1,0:T(2,128)S(1)}, u32[]{:S(2)}, u32[]{:S(2)}) async-start(f32[8,2,768]{2,1,0:T(2,128)} %get-tuple-element.26), calls=%async_computation.1 | async-start | bytes 98304 | tf_op jit(solution)/shard_map/all_to_all | solution.py:625
  218.0 0.6 copy-start
Sparse Core Ops, SparseCore 0:
  42.2 29.6 all-gather.8
  73.6 27.6 all-gather.10
  103.0 27.6 all-gather.14
  132.2 52.8 all-gather.12

commit v4 on v3

--- a/solution.py
+++ b/solution.py
@@ -101,7 +101,7 @@
 
 
 def qkv_kernel(
-    where, h_ref, wk_ref, wv_ref, wq_ref, cr, sr, cs, ss, a_ref, b_ref, rim_ref, acc, hb, kb, vb, qb, sem
+    where, h_ref, wk_ref, wv_ref, wq_ref, cr, sr, cs, ss, kva_ref, kvb_ref, qa_ref, qb_ref, rim_ref, acc, hb, kb, vb, qb, sem
 ):
     streamed_products(
         ((h_ref, hb, True), (wk_ref, kb, False), (wv_ref, vb, False), (wq_ref, qb, False)),
@@ -117,11 +117,13 @@
         query = rotated(acc[2, :, cols]) * (LOG2E / 8)
         parts = (rotated(acc[0, :, cols]), acc[1, :, cols], query)
         heads.append([part.astype(jnp.bfloat16) for part in parts])
-    for flip, o_ref in ((0, a_ref), (1, b_ref)):
-        for i in range(3):
-            o_ref[:, i * 128 : i * 128 + 128] = jnp.where(
-                where[1] == flip, heads[0][i], heads[1][i]
-            )
+    for flip, kv_ref, q_ref in ((0, kva_ref, qa_ref), (1, kvb_ref, qb_ref)):
+        key, value, query = (
+            jnp.where(where[1] == flip, heads[0][i], heads[1][i]) for i in range(3)
+        )
+        kv_ref[:, 0:128] = key
+        kv_ref[:, 128:256] = value
+        q_ref[...] = query
 
 
 def in_hbm():
@@ -143,7 +145,7 @@
     row_cos, row_sin, start_cos, start_sin = rotary_tables()
     table = pl.BlockSpec((GROUP, 128), lambda k, *_: (0, 0))
     starts = pl.BlockSpec((ROWS // GROUP, 128), lambda k, where: (where[0], 0))
-    shapes = ((ROWS, 384), (ROWS, 384), (HALO, D))
+    shapes = ((ROWS, 256), (ROWS, 256), (ROWS, 128), (ROWS, 128), (HALO, D))
     return pl.pallas_call(
         qkv_kernel,
         out_shape=tuple(jax.ShapeDtypeStruct(shape, jnp.bfloat16) for shape in shapes),
@@ -163,7 +165,7 @@
 
 
 def conv_kernel(
-    h_ref, rim_ref, wb_ref, wc_ref, wh_ref, taps_ref, o_ref, acc, rim_acc, padded, hb, rb, b, c, h, sem
+    h_ref, rim_ref, wb_ref, wc_ref, wh_ref, taps_ref, _, o_ref, acc, rim_acc, padded, hb, rb, b, c, h, sem
 ):
     streamed_products(
         (
@@ -189,7 +191,7 @@
     o_ref[...] = (once(acc[0]) * conv).astype(jnp.bfloat16)
 
 
-def gated_conv(hidden, rim, w_b, w_c, w_h, taps):
+def gated_conv(hidden, rim, w_b, w_c, w_h, taps, before):
     return pl.pallas_call(
         conv_kernel,
         out_shape=jax.ShapeDtypeStruct((ROWS, 256), jnp.bfloat16),
@@ -201,6 +203,7 @@
             in_hbm(),
             in_hbm(),
             pl.BlockSpec((3, 256), lambda k: (0, 0)),
+            in_hbm(),
         ],
         out_specs=pl.BlockSpec((ROWS, 256), lambda k: (0, 0)),
         scratch_shapes=[
@@ -214,7 +217,7 @@
             flops=2 * ROWS * D * 768, bytes_accessed=13 * 2**20, transcendentals=0
         ),
         name="gated_conv",
-    )(hidden, rim, w_b, w_c, w_h, taps)
+    )(hidden, rim, w_b, w_c, w_h, taps, before)
 
 
 KEYS_AT_ONCE = 256
@@ -380,7 +383,7 @@
     )(*args, *unread)
 
 
-def column_kernel(wc_ref, wa_ref, o_ref, buf, sem):
+def column_kernel(wc_ref, wa_ref, _, o_ref, buf, sem):
     width = o_ref.shape[3]
     loads = [
         pltpu.make_async_copy(w_ref, buf.at[i], sem.at[i, 8])
@@ -402,11 +405,11 @@
         store.wait()
 
 
-def column_blocks(w_conv, w_attn):
+def column_blocks(w_conv, w_attn, before):
     return pl.pallas_call(
         column_kernel,
         out_shape=jax.ShapeDtypeStruct((8, 2, 256, D // 8), jnp.bfloat16),
-        in_specs=[in_hbm(), in_hbm()],
+        in_specs=[in_hbm(), in_hbm(), in_hbm()],
         out_specs=in_hbm(),
         scratch_shapes=[pltpu.VMEM((2, 256, D), jnp.bfloat16), pltpu.SemaphoreType.DMA((2, 9))],
         compiler_params=pltpu.CompilerParams(vmem_limit_bytes=60 * 2**20),
@@ -414,7 +417,7 @@
             flops=3 * 10**9, bytes_accessed=9 * 2**20, transcendentals=0
         ),
         name="column_blocks",
-    )(w_conv, w_attn)
+    )(w_conv, w_attn, before)
 
 
 def whole_conv_kernel(x_ref, w_ref, o_ref):
@@ -582,22 +585,25 @@
     first = jnp.where(z < 2, 0, 1).astype(jnp.int32).reshape(1)
     where = jnp.stack([sp, jnp.where(z < 2, 0, 1)]).astype(jnp.int32)
     route_a, route_b = forward_route(0), forward_route(1)
-    head_a, head_b, last_rows = project(where, hidden_states, w_key, w_value, w_query)
+    head_a, head_b, q_a, q_b, last_rows = project(where, hidden_states, w_key, w_value, w_query)
     rim = lax.ppermute(last_rows, ("z", "x"), [(i, i + 1) for i in range(15)])
     head_a = lax.ppermute(head_a, z_core, route_a)
     head_b = lax.ppermute(head_b, z_core, route_b)
-    blocks = column_blocks(w_out_conv, w_out_attn)
+    q_a = lax.ppermute(q_a, z_core, route_a)
+    q_b = lax.ppermute(q_b, z_core, route_b)
+    even = (z % 2) == 0
+    own_low = jnp.where(even, head_a, head_b)
+    own_high = jnp.where(even, head_b, head_a)
+    q_low = jnp.where(even, q_a, q_b)
+    q_high = jnp.where(even, q_b, q_a)
+    kv_low = lax.all_gather(own_low, ("x", "c"), axis=0)
+    kv_high = lax.all_gather(own_high, ("x", "c"), axis=0)
+
+    blocks = column_blocks(w_out_conv, w_out_attn, own_low)
     w_out = lax.all_to_all(blocks, ("y", "c"), split_axis=0, concat_axis=0, tiled=True)
-    even = (z % 2) == 0
-    kv, q = slice(0, 256), slice(256, 384)
-    kv_low = jnp.where(even, head_a[:, kv], head_b[:, kv])
-    kv_high = jnp.where(even, head_b[:, kv], head_a[:, kv])
-    q_low = jnp.where(even, head_a[:, q], head_b[:, q])
-    q_high = jnp.where(even, head_b[:, q], head_a[:, q])
-    kv_low = lax.all_gather(kv_low, ("x", "c"), axis=0)
-    kv_high = lax.all_gather(kv_high, ("x", "c"), axis=0)
-
-    conv_out = gated_conv(hidden_states, rim, w_conv_b, w_conv_c, w_conv_h, conv_taps)
+    conv_out = gated_conv(
+        hidden_states, rim, w_conv_b, w_conv_c, w_conv_h, conv_taps, own_low
+    )
     conv_all = lax.all_gather(conv_out, ("y", "c"), axis=0)
 
     plane_lambdas = jnp.where(

time: 232 us -> 226 us (0.974)
  waiting for transfers between devices: 40.4 us -> 26.3 us
  starting transfers between devices: 32.6 us -> 40.5 us
    all_gather x2, waiting for transfers between devices: 13.1 us -> 0.02 us  [the longest x1 0.02 us: per_device(): kv_high = lax.all_gather(own_high, ('x', 'c'), axis=0)]
    ppermute x0 -> x2, starting transfers between devices: none -> 11.5 us  [the longest x1 8.64 us: per_device(): q_a = lax.ppermute(q_a, z_core, route_a)]
    ppermute x1, waiting for transfers between devices: 10.3 us -> 0.96 us  [per_device(): head_a = lax.ppermute(head_a, z_core, route_a)]
    ppermute x1, starting transfers between devices: 7.01 us -> 1.92 us  [per_device(): head_a = lax.ppermute(head_a, z_core, route_a)]
    ppermute x1, starting transfers between devices: 2.62 us -> 7.17 us  [per_device(): head_b = lax.ppermute(head_b, z_core, route_b)]
    ppermute x0 -> x2, waiting for transfers between devices: none -> 4.18 us  [the longest x1 4.18 us: per_device(): q_b = lax.ppermute(q_b, z_core, route_b)]
    ppermute x1, waiting for transfers between devices: 3.1 us -> 7.02 us  [per_device(): head_b = lax.ppermute(head_b, z_core, route_b)]
  transfers between devices with their start and end apart: 11 -> 13, of which waited for: 9 -> 7; matrix products, arithmetic and copies ran while one was open for 2% -> 2% of each run, Pallas kernels for 22% -> 23%
where the time goes in v4:
time: 226 us; the launch traced here: 222 us
  Pallas kernels  70 us (31%)
  blocking collectives  65.7 us (29%)
  starting transfers between devices  40.5 us (18%)
  waiting for transfers between devices  26.3 us (12%)
  between operations  13.3 us (6%)
  other arithmetic  3.97 us (2%)
  local copies, waits for them, and re-layouts  2.55 us (1%)
    all_to_all x1, blocking collectives, per_device(): lax.all_to_all(blocks, ('y', 'c'), split_axis=0, concat_axis=0, tiled=True)  65.7 us
    pallas_call x2, Pallas kernels, attention_call(): pl.pallas_call(kernel, out_shape=outs, grid_spec=pltpu.PrefetchScalarGrid...  30.8 us
    pallas_call x1, Pallas kernels, project(): pl.pallas_call(qkv_kernel, out_shape=tuple((jax.ShapeDtypeStruct(shape, j...  10.8 us
    pallas_call x1, Pallas kernels, gated_conv(): pl.pallas_call(conv_kernel, out_shape=jax.ShapeDtypeStruct((ROWS, 256), j...  10.6 us
    ppermute x1, starting transfers between devices, per_device(): back_b = lax.ppermute(o_b, z_core, reverse(route_b))  8.82 us
    ppermute x1, starting transfers between devices, per_device(): q_a = lax.ppermute(q_a, z_core, route_a)  8.64 us
    ppermute x1, starting transfers between devices, per_device(): head_b = lax.ppermute(head_b, z_core, route_b)  7.17 us
    ppermute x1, waiting for transfers between devices, per_device(): head_b = lax.ppermute(head_b, z_core, route_b)  7.02 us
  transfers between devices with their start and end apart: 13, of which 7 were waited for; matrix products, arithmetic and copies ran while one was open for 2% of the time, Pallas kernels for 23%

profile of v4, /device:TPU:1, one launch (start us, length us, event | category | flops | bytes accessed | tf_op | source)
XLA Modules:
  0.0 222.3 jit_solution(5059458237749919803)
XLA Ops:
  6.5 0.0 all-gather.9.cloned.1.call-start
  6.5 0.6 pad_add_fusion.1.where
  7.2 10.8 %qkv.1 = (bf16[768,256]{1,0:T(8,128)(2,1)}, bf16[768,256]{1,0:T(8,128)(2,1)}, bf16[768,128]{1,0:T(8,128)(2,1)}, bf16[768,128]{1,0:T(8,128)(2,1)}, bf16[16,4096]{1,0:T(8,128)(2,1)}) custom-call(s32[2]{0:T(128)} %pad_add_fusion.1.where, bf16[768,4096]{1,0:T(8,128)(2,1)} %h_ref.3, bf16[4096,256]{1,0:T(8,128)(2,1)} %wk_ref.1, bf16[4096,256]{1,0:T(8,128)(2,1)} %wv_ref.1, ...), custom_call_target="tpu_custom_call" | custom-call | flops 4831838208 | bytes 13631488 | tf_op jit(solution)/shard_map/qkv/pallas_call | solution.py:149
  18.0 0.0 copy-start.5
  18.0 7.2 %collective-permute-start.4 = (bf16[768,256]{1,0:T(8,128)(2,1)}, bf16[768,256]{1,0:T(8,128)(2,1)S(1)}, u32[]{:S(2)}, u32[]{:S(2)}) collective-permute-start(bf16[768,256]{1,0:T(8,128)(2,1)} %get-tuple-element.21), channel_id=1, source_target_pairs={{0,32},{1,96},{32,33},{33,97},{64,1},{65,65},{96,0},{97,64},{2,34}... | collective-permute-start | bytes 1179656 | tf_op jit(solution)/shard_map/ppermute | solution.py:591
  25.1 1.9 collective-permute-start.3
  27.1 7.0 %collective-permute-done.4 = bf16[768,256]{1,0:T(8,128)(2,1)S(1)} collective-permute-done((bf16[768,256]{1,0:T(8,128)(2,1)}, bf16[768,256]{1,0:T(8,128)(2,1)S(1)}, u32[]{:S(2)}, u32[]{:S(2)}) %collective-permute-start.4) | collective-permute-done | bytes 393248 | tf_op jit(solution)/shard_map/ppermute | solution.py:591
  34.1 1.0 collective-permute-done.3
  35.1 1.0 broadcast_select_fusion
  36.1 0.0 all-gather.9.cloned.1.call-update
  36.1 0.0 all-gather.11.cloned.1.call-start
  36.2 0.7 all-gather.11.cloned.1.call-update
  36.9 0.0 all-gather.15.cloned.1.call-start
  36.9 0.0 copy-start.2
  37.0 3.3 %collective-permute-start.5 = (bf16[16,4096]{1,0:T(8,128)(2,1)S(1)}, bf16[16,4096]{1,0:T(8,128)(2,1)S(1)}, u32[]{:S(2)}, u32[]{:S(2)}) collective-permute-start(bf16[16,4096]{1,0:T(8,128)(2,1)S(1)} %copy-done.5), channel_id=1, source_target_pairs={{0,8},{8,16},{16,24},{24,32},{32,40},{40,48},{48,56},{56,64},{64,7... | collective-permute-start | bytes 393224 | tf_op jit(solution)/shard_map/ppermute | solution.py:589
  40.2 2.3 %collective-permute-done.5.rim_ref = bf16[16,4096]{1,0:T(8,128)(2,1)S(1)} collective-permute-done((bf16[16,4096]{1,0:T(8,128)(2,1)S(1)}, bf16[16,4096]{1,0:T(8,128)(2,1)S(1)}, u32[]{:S(2)}, u32[]{:S(2)}) %collective-permute-start.5) | collective-permute-done | bytes 131104 | tf_op jit(solution)/shard_map/ppermute | solution.py:589
  42.6 0.7 copy-done.6
  43.2 10.6 %gated_conv.1._ = bf16[768,256]{1,0:T(8,128)(2,1)} custom-call(bf16[768,4096]{1,0:T(8,128)(2,1)} %h_ref.3, bf16[16,4096]{1,0:T(8,128)(2,1)} %copy-done.6, bf16[4096,256]{1,0:T(8,128)(2,1)} %wb_ref.1, bf16[4096,256]{1,0:T(8,128)(2,1)} %wc_ref.2, bf16[4096,256]{1,0:T(8,128)(2,1)} %wh_ref.1, bf16[3,256]{1,0:T(4,128)(2,1)} %taps_ref.1, ...), custom_call_target="tpu_custom_call" | custom-call | flops 4831838208 | bytes 13631488 | tf_op jit(solution)/shard_map/gated_conv/pallas_call | solution.py:195
  53.9 0.0 all-gather.15.cloned.1.call-update
  53.9 0.0 all-gather.13.cloned.1.call-start
  54.0 1.4 collective-permute-start
  55.4 8.6 %collective-permute-start.2 = (bf16[768,128]{1,0:T(8,128)(2,1)S(1)}, bf16[768,128]{1,0:T(8,128)(2,1)S(1)}, u32[]{:S(2)}, u32[]{:S(2)}) collective-permute-start(bf16[768,128]{1,0:T(8,128)(2,1)S(1)} %copy-done.4), channel_id=1, source_target_pairs={{0,0},{1,64},{32,1},{33,65},{64,33},{65,97},{96,32},{97,96},{2,2},... | collective-permute-start | bytes 589832 | tf_op jit(solution)/shard_map/ppermute | solution.py:592
  64.0 2.9 %collective-permute-start.1 = (bf16[768,128]{1,0:T(8,128)(2,1)S(1)}, bf16[768,128]{1,0:T(8,128)(2,1)S(1)}, u32[]{:S(2)}, u32[]{:S(2)}) collective-permute-start(bf16[768,128]{1,0:T(8,128)(2,1)S(1)} %copy-done.3), channel_id=1, source_target_pairs={{0,32},{1,96},{32,33},{33,97},{64,1},{65,65},{96,0},{97,64},{2,34}... | collective-permute-start | bytes 589832 | tf_op jit(solution)/shard_map/ppermute | solution.py:593
  66.9 0.7 pad_add_fusion.own
  67.6 0.0 collective-permute-done
  67.6 0.1 broadcast_select_fusion.4
  67.7 0.7 dynamic_slice.3.lam
  68.4 0.0 collective-permute-done.2
  68.4 4.2 %collective-permute-done.1 = bf16[768,128]{1,0:T(8,128)(2,1)S(1)} collective-permute-done((bf16[768,128]{1,0:T(8,128)(2,1)S(1)}, bf16[768,128]{1,0:T(8,128)(2,1)S(1)}, u32[]{:S(2)}, u32[]{:S(2)}) %collective-permute-start.1) | collective-permute-done | bytes 196640 | tf_op jit(solution)/shard_map/ppermute | solution.py:593
  72.5 0.8 broadcast_select_fusion.2
  73.3 24.1 %shard_map.163 = (bf16[768,128]{1,0:T(8,128)(2,1)}, f32[2,768,128]{2,1,0:T(8,128)}, f32[2,768,128]{2,1,0:T(8,128)}, f32[2,768,128]{2,1,0:T(8,128)}) custom-call(s32[3]{0:T(128)} %pad_add_fusion.own, f32[1]{0:T(128)} %dynamic_slice.3.lam, bf16[768,128]{1,0:T(8,128)(2,1)} %get-tuple-element.33.ql_ref, bf16[768,128]{1,0:T(8,128)(2,1)} %get-tuple-element.34.qh_ref, ...), custom_call_target="tpu_custom_call" | custom-call | flops 24000000000 | bytes 4194304 | tf_op jit(solution)/shard_map/pallas_call | solution.py:365
  97.4 0.0 all-gather.11.cloned.1.call-done
  97.4 6.7 %shard_map.164 = (bf16[768,128]{1,0:T(8,128)(2,1)}, bf16[768,128]{1,0:T(8,128)(2,1)}) custom-call(s32[3]{0:T(128)} %pad_add_fusion.own, f32[1]{0:T(128)} %dynamic_slice.3.lam, bf16[768,128]{1,0:T(8,128)(2,1)} %get-tuple-element.34.qh_ref, bf16[1,128]{1,0:T(2,128)(2,1)} %bitcast.16, bf16[768,128]{1,0:T(8,128)(2,1)} %get-tuple-element.23.low_ref, ...), custom_call_target="tpu_custom_call" | custom-call | flops 12000000000 | bytes 4194304 | tf_op jit(solution)/shard_map/pallas_call | solution.py:365
  104.1 8.8 %collective-permute-start.7 = (bf16[768,128]{1,0:T(8,128)(2,1)}, bf16[768,128]{1,0:T(8,128)(2,1)S(1)}, u32[]{:S(2)}, u32[]{:S(2)}) collective-permute-start(bf16[768,128]{1,0:T(8,128)(2,1)} %get-tuple-element.28), channel_id=1, source_target_pairs={{32,0},{96,1},{33,32},{97,33},{1,64},{65,65},{0,96},{64,97},{34,2}... | collective-permute-start | bytes 589832 | tf_op jit(solution)/shard_map/ppermute | solution.py:627
  113.0 1.9 collective-permute-start.6
  114.9 1.8 collective-permute-done.7
  116.7 5.0 %collective-permute-done.6 = bf16[768,128]{1,0:T(8,128)(2,1)S(1)} collective-permute-done((bf16[768,128]{1,0:T(8,128)(2,1)}, bf16[768,128]{1,0:T(8,128)(2,1)S(1)}, u32[]{:S(2)}, u32[]{:S(2)}) %collective-permute-start.6) | collective-permute-done | bytes 196640 | tf_op jit(solution)/shard_map/ppermute | solution.py:626
  121.7 0.8 pad_maximum_fusion
  122.5 0.0 all-gather.13.cloned.1.call-update
  122.5 3.8 %column_blocks.1 = bf16[8,2,256,512]{3,2,1,0:T(8,128)(2,1)} custom-call(bf16[256,4096]{1,0:T(8,128)(2,1)} %wc_ref.3, bf16[256,4096]{1,0:T(8,128)(2,1)} %wa_ref.1, bf16[768,256]{1,0:T(8,128)(2,1)} %get-tuple-element.32._), custom_call_target="tpu_custom_call" | custom-call | flops 3000000000 | bytes 9437184 | tf_op jit(solution)/shard_map/column_blocks/pallas_call | solution.py:409
  126.3 65.7 %all_to_all.10.w_ref = bf16[8,2,256,512]{3,2,1,0:T(8,128)(2,1)} all-to-all(bf16[8,2,256,512]{3,2,1,0:T(8,128)(2,1)} %column_blocks.1), channel_id=1, replica_groups=mesh['z'=4,'x'=4,'y'=4,'c'=2] {'y','c'}, dimensions={0} | all-to-all | bytes 8388608 | tf_op jit(solution)/shard_map/all_to_all | solution.py:603
  192.1 5.5 %whole_conv.1.before_ref = f32[768,512]{1,0:T(8,128)} custom-call(bf16[8,768,256]{2,1,0:T(8,128)(2,1)} %bitcast.11, bf16[8,2,256,512]{3,2,1,0:T(8,128)(2,1)} %all_to_all.10.w_ref), custom_call_target="tpu_custom_call" | custom-call | flops 1610612736 | bytes 7340032 | tf_op jit(solution)/shard_map/whole_conv/pallas_call | solution.py:471
  197.5 5.3 %whole_last.1 = (bf16[768,512]{1,0:T(8,128)(2,1)}, f32[8,2,768]{2,1,0:T(2,128)}) custom-call(s32[1]{0:T(128)} %bitcast.1.first, bf16[8,768,256]{2,1,0:T(8,128)(2,1)} %bitcast.12, bf16[8,2,256,512]{3,2,1,0:T(8,128)(2,1)} %all_to_all.10.w_ref, f32[768,512]{1,0:T(8,128)} %whole_conv.1.before_ref), custom_call_target="tpu_custom_call" | custom-call | flops 1610612736 | bytes 7340032 | tf_op jit(solution)/shard_map/whole_last/pallas_call | solution.py:490
  202.8 4.3 %all-to-all-start.1 = ((f32[8,2,768]{2,1,0:T(2,128)}), f32[8,2,768]{2,1,0:T(2,128)S(1)}, u32[]{:S(2)}, u32[]{:S(2)}) async-start(f32[8,2,768]{2,1,0:T(2,128)} %get-tuple-element.30), calls=%async_computation.1 | async-start | bytes 98304 | tf_op jit(solution)/shard_map/all_to_all | solution.py:631
  207.2 0.6 reshape.15.gain_ref
  207.8 4.2 %all-to-all-done.1.sums_ref = f32[8,2,768]{2,1,0:T(2,128)S(1)} async-done(((f32[8,2,768]{2,1,0:T(2,128)}), f32[8,2,768]{2,1,0:T(2,128)S(1)}, u32[]{:S(2)}, u32[]{:S(2)}) %all-to-all-start.1) | async-done | bytes 49184 | tf_op jit(solution)/shard_map/all_to_all | solution.py:631
  212.0 0.6 copy-done
  212.6 3.2 %norm.1 = bf16[768,512]{1,0:T(8,128)(2,1)} custom-call(s32[1]{0:T(128)} %bitcast.own, bf16[768,512]{1,0:T(8,128)(2,1)} %get-tuple-element.29.mix_ref, f32[8,2,768]{2,1,0:T(2,128)} %copy-done, bf16[1,4096]{1,0:T(2,128)(2,1)} %reshape.15.gain_ref), custom_call_target="tpu_custom_call" | custom-call | tf_op jit(solution)/shard_map/norm/pallas_call | solution.py:545
  (13 shorter events, 0.0 us)
Async XLA Ops:
  6.5 66.8 %all-gather.9.cloned.1.call-start = ((), (), s32[]{:S(2)}) async-start(), calls=%async_computation.2 | async-start | bytes 3538944 | tf_op jit(solution)/shard_map/all_gather | solution.py:599
  18.0 19.0 %copy-start.5 = (bf16[16,4096]{1,0:T(8,128)(2,1)S(1)}, bf16[16,4096]{1,0:T(8,128)(2,1)}, u32[]{:S(2)}) copy-start(bf16[16,4096]{1,0:T(8,128)(2,1)} %get-tuple-element.22) | copy-start | bytes 393220
  18.0 16.1 %collective-permute-start.4 = (bf16[768,256]{1,0:T(8,128)(2,1)}, bf16[768,256]{1,0:T(8,128)(2,1)S(1)}, u32[]{:S(2)}, u32[]{:S(2)}) collective-permute-start(bf16[768,256]{1,0:T(8,128)(2,1)} %get-tuple-element.21), channel_id=1, source_target_pairs={{0,32},{1,96},{32,33},{33,97},{64,1},{65,65},{96,0},{97,64},{2,34}... | collective-permute-start | bytes 1179656 | tf_op jit(solution)/shard_map/ppermute | solution.py:591
  25.1 9.9 %collective-permute-start.3 = (bf16[768,256]{1,0:T(8,128)(2,1)}, bf16[768,256]{1,0:T(8,128)(2,1)S(1)}, u32[]{:S(2)}, u32[]{:S(2)}) collective-permute-start(bf16[768,256]{1,0:T(8,128)(2,1)} %get-tuple-element.20), channel_id=1, source_target_pairs={{0,0},{1,64},{32,1},{33,65},{64,33},{65,97},{96,32},{97,96},{2,2},... | collective-permute-start | bytes 1179656 | tf_op jit(solution)/shard_map/ppermute | solution.py:590
  36.1 61.3 %all-gather.11.cloned.1.call-start = ((), (), s32[]{:S(2)}) async-start(), calls=%async_computation.3 | async-start | bytes 3538944 | tf_op jit(solution)/shard_map/all_gather | solution.py:600
  36.9 155.2 %all-gather.15.cloned.1.call-start = ((), (), s32[]{:S(2)}) async-start(), calls=%async_computation.5 | async-start | bytes 3538944 | tf_op jit(solution)/shard_map/all_gather | solution.py:607
  36.9 17.0 %copy-start.2 = (f32[2]{0:T(128)S(1)}, f32[2]{0:T(128)}, u32[]{:S(2)}) copy-start(f32[2]{0:T(128)} %param.25) | copy-start | bytes 28
  36.9 18.4 %copy-start.4 = (bf16[768,128]{1,0:T(8,128)(2,1)S(1)}, bf16[768,128]{1,0:T(8,128)(2,1)}, u32[]{:S(2)}) copy-start(bf16[768,128]{1,0:T(8,128)(2,1)} %get-tuple-element.19) | copy-start | bytes 589828
  37.0 27.1 %copy-start.3 = (bf16[768,128]{1,0:T(8,128)(2,1)S(1)}, bf16[768,128]{1,0:T(8,128)(2,1)}, u32[]{:S(2)}) copy-start(bf16[768,128]{1,0:T(8,128)(2,1)} %get-tuple-element.18) | copy-start | bytes 589828
  37.0 5.6 %collective-permute-start.5 = (bf16[16,4096]{1,0:T(8,128)(2,1)S(1)}, bf16[16,4096]{1,0:T(8,128)(2,1)S(1)}, u32[]{:S(2)}, u32[]{:S(2)}) collective-permute-start(bf16[16,4096]{1,0:T(8,128)(2,1)S(1)} %copy-done.5), channel_id=1, source_target_pairs={{0,8},{8,16},{16,24},{24,32},{32,40},{40,48},{48,56},{56,64},{64,7... | collective-permute-start | bytes 393224 | tf_op jit(solution)/shard_map/ppermute | solution.py:589
  42.6 0.7 copy-start.6
  53.9 143.6 %all-gather.13.cloned.1.call-start = ((), (), s32[]{:S(2)}) async-start(), calls=%async_computation.4 | async-start | bytes 3538944 | tf_op jit(solution)/shard_map/all_gather | solution.py:628
  54.0 13.7 %collective-permute-start = (f32[2]{0:T(128)S(1)}, f32[2]{0:T(128)S(1)}, u32[]{:S(2)}, u32[]{:S(2)}) collective-permute-start(f32[2]{0:T(128)S(1)} %copy-done.2), channel_id=1, source_target_pairs={{0,1},{1,0},{2,3},{3,2},{4,5},{5,4},{6,7},{7,6},{8,9},{9,8},{10,11... | collective-permute-start | bytes 32 | tf_op jit(solution)/shard_map/ppermute | solution.py:583
  55.4 13.0 %collective-permute-start.2 = (bf16[768,128]{1,0:T(8,128)(2,1)S(1)}, bf16[768,128]{1,0:T(8,128)(2,1)S(1)}, u32[]{:S(2)}, u32[]{:S(2)}) collective-permute-start(bf16[768,128]{1,0:T(8,128)(2,1)S(1)} %copy-done.4), channel_id=1, source_target_pairs={{0,0},{1,64},{32,1},{33,65},{64,33},{65,97},{96,32},{97,96},{2,2},... | collective-permute-start | bytes 589832 | tf_op jit(solution)/shard_map/ppermute | solution.py:592
  64.0 8.5 %collective-permute-start.1 = (bf16[768,128]{1,0:T(8,128)(2,1)S(1)}, bf16[768,128]{1,0:T(8,128)(2,1)S(1)}, u32[]{:S(2)}, u32[]{:S(2)}) collective-permute-start(bf16[768,128]{1,0:T(8,128)(2,1)S(1)} %copy-done.3), channel_id=1, source_target_pairs={{0,32},{1,96},{32,33},{33,97},{64,1},{65,65},{96,0},{97,64},{2,34}... | collective-permute-start | bytes 589832 | tf_op jit(solution)/shard_map/ppermute | solution.py:593
  104.1 12.6 %collective-permute-start.7 = (bf16[768,128]{1,0:T(8,128)(2,1)}, bf16[768,128]{1,0:T(8,128)(2,1)S(1)}, u32[]{:S(2)}, u32[]{:S(2)}) collective-permute-start(bf16[768,128]{1,0:T(8,128)(2,1)} %get-tuple-element.28), channel_id=1, source_target_pairs={{32,0},{96,1},{33,32},{97,33},{1,64},{65,65},{0,96},{64,97},{34,2}... | collective-permute-start | bytes 589832 | tf_op jit(solution)/shard_map/ppermute | solution.py:627
  113.0 8.8 %collective-permute-start.6 = (bf16[768,128]{1,0:T(8,128)(2,1)}, bf16[768,128]{1,0:T(8,128)(2,1)S(1)}, u32[]{:S(2)}, u32[]{:S(2)}) collective-permute-start(bf16[768,128]{1,0:T(8,128)(2,1)} %get-tuple-element.27), channel_id=1, source_target_pairs={{0,0},{64,1},{1,32},{65,33},{33,64},{97,65},{32,96},{96,97},{2,2},... | collective-permute-start | bytes 589832 | tf_op jit(solution)/shard_map/ppermute | solution.py:626
  197.5 9.6 %copy-start.1 = (bf16[4096]{0:T(1024)(128)(2,1)S(1)}, bf16[4096]{0:T(1024)(128)(2,1)}, u32[]{:S(2)}) copy-start(bf16[4096]{0:T(1024)(128)(2,1)} %param.29) | copy-start | bytes 24580
  202.8 9.1 %all-to-all-start.1 = ((f32[8,2,768]{2,1,0:T(2,128)}), f32[8,2,768]{2,1,0:T(2,128)S(1)}, u32[]{:S(2)}, u32[]{:S(2)}) async-start(f32[8,2,768]{2,1,0:T(2,128)} %get-tuple-element.30), calls=%async_computation.1 | async-start | bytes 98304 | tf_op jit(solution)/shard_map/all_to_all | solution.py:631
  212.0 0.6 copy-start
Sparse Core Ops, SparseCore 0:
  36.2 29.6 all-gather.8
  67.7 27.5 all-gather.10
  97.0 27.6 all-gather.14
  126.2 52.8 all-gather.12

commit v5 on v4

--- a/solution.py
+++ b/solution.py
@@ -420,10 +420,14 @@
     )(w_conv, w_attn, before)
 
 
-def whole_conv_kernel(x_ref, w_ref, o_ref):
-    left = jnp.concatenate([x_ref[t] for t in range(8)], axis=1)
-    right = jnp.concatenate([w_ref[t, 0] for t in range(8)], axis=0)
-    o_ref[...] = jnp.dot(left, right, preferred_element_type=jnp.float32)
+def whole_conv_kernel(core, own_ref, other_ref, w_ref, o_ref):
+    left = [ref[y] for ref in (own_ref, other_ref) for y in range(4)]
+    right = [w_ref[2 * y + c, 0] for c in (core[0], 1 - core[0]) for y in range(4)]
+    o_ref[...] = jnp.dot(
+        jnp.concatenate(left, axis=1),
+        jnp.concatenate(right, axis=0),
+        preferred_element_type=jnp.float32,
+    )
 
 
 def whole_last_kernel(first, x_ref, w_ref, before_ref, mix_ref, sums_ref, xb, wb, acc, sem):
@@ -466,23 +470,28 @@
         sums_ref[copy] = sums
 
 
-def whole_conv(gathered, weights):
+def whole_conv(core, own, other, weights):
     width = weights.shape[3]
+    half = pl.BlockSpec(own.shape, lambda i, *_: (0, 0, 0))
     return pl.pallas_call(
         whole_conv_kernel,
         out_shape=jax.ShapeDtypeStruct((ROWS, width), jnp.float32),
-        grid=(1,),
-        in_specs=[
-            pl.BlockSpec(gathered.shape, lambda i: (0, 0, 0)),
-            pl.BlockSpec((8, 1, 256, width), lambda i: (0, 0, 0, 0)),
-        ],
-        out_specs=pl.BlockSpec((ROWS, width), lambda i: (0, 0)),
+        grid_spec=pltpu.PrefetchScalarGridSpec(
+            num_scalar_prefetch=1,
+            grid=(1,),
+            in_specs=[
+                half,
+                half,
+                pl.BlockSpec((8, 1, 256, width), lambda i, *_: (0, 0, 0, 0)),
+            ],
+            out_specs=pl.BlockSpec((ROWS, width), lambda i, *_: (0, 0)),
+        ),
         compiler_params=pltpu.CompilerParams(vmem_limit_bytes=60 * 2**20),
         cost_estimate=pl.CostEstimate(
             flops=2 * ROWS * 2048 * width, bytes_accessed=7 * 2**20, transcendentals=0
         ),
         name="whole_conv",
-    )(gathered, weights)
+    )(core, own, other, weights)
 
 
 def whole_last(first, gathered, weights, before):
@@ -604,7 +613,7 @@
     conv_out = gated_conv(
         hidden_states, rim, w_conv_b, w_conv_c, w_conv_h, conv_taps, own_low
     )
-    conv_all = lax.all_gather(conv_out, ("y", "c"), axis=0)
+    conv_own = lax.all_gather(conv_out, "y", axis=0)
 
     plane_lambdas = jnp.where(
         core == 0,
@@ -626,7 +635,10 @@
     back_a = lax.ppermute(o_a, z_core, reverse(route_a))
     back_b = lax.ppermute(o_b, z_core, reverse(route_b))
     attn_all = lax.all_gather(jnp.concatenate([back_a, back_b], axis=1), ("y", "c"), axis=0)
-    conv_part = whole_conv(conv_all, w_out)
+    conv_other = lax.ppermute(conv_own, "c", [(0, 1), (1, 0)])
+    conv_part = whole_conv(
+        core.astype(jnp.int32).reshape(1), conv_own, conv_other, w_out
+    )
     mix, sums = whole_last(first, attn_all, w_out, conv_part)
     everything = lax.all_to_all(sums, ("y", "c"), split_axis=0, concat_axis=0, tiled=True)
     tp = (lax.axis_index("y") * 2 + core).astype(jnp.int32).reshape(1)

time: 226 us -> 228 us (level)
  blocking collectives: 65.7 us -> 0 us
  waiting for transfers between devices: 26.3 us -> 89.5 us
  starting transfers between devices: 40.5 us -> 44.5 us
    all_to_all x1 -> x0, blocking collectives: 65.7 us -> none  [per_device(): lax.all_to_all(blocks, ('y', 'c'), split_axis=0, concat_axis=0, tiled=True)]
    all_to_all x0 -> x1, waiting for transfers between devices: none -> 61.1 us  [per_device(): lax.all_to_all(blocks, ('y', 'c'), split_axis=0, concat_axis=0, tiled=True)]
    all_gather x1, waiting for transfers between devices: 0.02 us -> 4.75 us  [per_device(): kv_high = lax.all_gather(own_high, ('x', 'c'), axis=0)]
    all_to_all x0 -> x1, starting transfers between devices: none -> 4.52 us  [per_device(): lax.all_to_all(blocks, ('y', 'c'), split_axis=0, concat_axis=0, tiled=True)]
    ppermute x1, waiting for transfers between devices: 4.18 us -> 0.01 us  [per_device(): q_b = lax.ppermute(q_b, z_core, route_b)]
    ppermute x1, starting transfers between devices: 8.64 us -> 5.18 us  [per_device(): q_a = lax.ppermute(q_a, z_core, route_a)]
  transfers between devices with their start and end apart: 13 -> 15, of which waited for: 7 -> 9; matrix products, arithmetic and copies ran while one was open for 2% -> 2% of each run, Pallas kernels for 23% -> 23%
where the time goes in v5:
time: 228 us; the launch traced here: 225 us
  waiting for transfers between devices  89.5 us (39%)
  Pallas kernels  70 us (31%)
  starting transfers between devices  44.5 us (20%)
  between operations  13.4 us (6%)
  other arithmetic  3.95 us (2%)
  local copies, waits for them, and re-layouts  3.68 us (2%)
    all_to_all x1, waiting for transfers between devices, per_device(): lax.all_to_all(blocks, ('y', 'c'), split_axis=0, concat_axis=0, tiled=True)  61.1 us
    pallas_call x2, Pallas kernels, attention_call(): pl.pallas_call(kernel, out_shape=outs, grid_spec=pltpu.PrefetchScalarGrid...  30.7 us
    ppermute x1, starting transfers between devices, per_device(): back_b = lax.ppermute(o_b, z_core, reverse(route_b))  10.9 us
    pallas_call x1, Pallas kernels, project(): pl.pallas_call(qkv_kernel, out_shape=tuple((jax.ShapeDtypeStruct(shape, j...  10.8 us
    pallas_call x1, Pallas kernels, gated_conv(): pl.pallas_call(conv_kernel, out_shape=jax.ShapeDtypeStruct((ROWS, 256), j...  10.6 us
    ppermute x1, starting transfers between devices, per_device(): head_b = lax.ppermute(head_b, z_core, route_b)  7.18 us
    ppermute x1, waiting for transfers between devices, per_device(): head_b = lax.ppermute(head_b, z_core, route_b)  7.02 us
    pallas_call x1, Pallas kernels, whole_conv(): pl.pallas_call(whole_conv_kernel, out_shape=jax.ShapeDtypeStruct((ROWS, w...  5.49 us
  transfers between devices with their start and end apart: 15, of which 9 were waited for; matrix products, arithmetic and copies ran while one was open for 2% of the time, Pallas kernels for 23%

profile of v5, /device:TPU:1, one launch (start us, length us, event | category | flops | bytes accessed | tf_op | source)
XLA Modules:
  0.0 224.9 jit_solution(4048208750135761469)
XLA Ops:
  6.5 0.7 pad_add_fusion.1.where
  7.2 10.8 %qkv.1 = (bf16[768,256]{1,0:T(8,128)(2,1)}, bf16[768,256]{1,0:T(8,128)(2,1)}, bf16[768,128]{1,0:T(8,128)(2,1)}, bf16[768,128]{1,0:T(8,128)(2,1)}, bf16[16,4096]{1,0:T(8,128)(2,1)}) custom-call(s32[2]{0:T(128)} %pad_add_fusion.1.where, bf16[768,4096]{1,0:T(8,128)(2,1)} %h_ref.3, bf16[4096,256]{1,0:T(8,128)(2,1)} %wk_ref.1, bf16[4096,256]{1,0:T(8,128)(2,1)} %wv_ref.1, ...), custom_call_target="tpu_custom_call" | custom-call | flops 4831838208 | bytes 13631488 | tf_op jit(solution)/shard_map/qkv/pallas_call | solution.py:149
  18.0 0.0 copy-start.3
  18.0 7.2 %collective-permute-start.4 = (bf16[768,256]{1,0:T(8,128)(2,1)}, bf16[768,256]{1,0:T(8,128)(2,1)S(1)}, u32[]{:S(2)}, u32[]{:S(2)}) collective-permute-start(bf16[768,256]{1,0:T(8,128)(2,1)} %get-tuple-element.21), channel_id=1, source_target_pairs={{0,32},{1,96},{32,33},{33,97},{64,1},{65,65},{96,0},{97,64},{2,34}... | collective-permute-start | bytes 1179656 | tf_op jit(solution)/shard_map/ppermute | solution.py:600
  25.2 1.9 collective-permute-start.3
  27.2 7.0 %collective-permute-done.4 = bf16[768,256]{1,0:T(8,128)(2,1)S(1)} collective-permute-done((bf16[768,256]{1,0:T(8,128)(2,1)}, bf16[768,256]{1,0:T(8,128)(2,1)S(1)}, u32[]{:S(2)}, u32[]{:S(2)}) %collective-permute-start.4) | collective-permute-done | bytes 393248 | tf_op jit(solution)/shard_map/ppermute | solution.py:600
  34.2 1.0 collective-permute-done.3
  35.2 1.0 broadcast_select_fusion
  36.1 0.0 all-gather.9.cloned.1.call-update
  36.1 0.0 all-gather.11.cloned.1.call-start
  36.2 0.7 all-gather.11.cloned.1.call-update
  36.9 0.0 all-gather.15.cloned.1.call-start
  36.9 0.6 collective-permute-start
  37.5 5.2 %collective-permute-start.2 = (bf16[768,128]{1,0:T(8,128)(2,1)S(1)}, bf16[768,128]{1,0:T(8,128)(2,1)S(1)}, u32[]{:S(2)}, u32[]{:S(2)}) collective-permute-start(bf16[768,128]{1,0:T(8,128)(2,1)S(1)} %copy-done.5), channel_id=1, source_target_pairs={{0,0},{1,64},{32,1},{33,65},{64,33},{65,97},{96,32},{97,96},{2,2},... | collective-permute-start | bytes 589832 | tf_op jit(solution)/shard_map/ppermute | solution.py:601
  42.7 4.5 %collective-permute-start.1 = (bf16[768,128]{1,0:T(8,128)(2,1)S(1)}, bf16[768,128]{1,0:T(8,128)(2,1)S(1)}, u32[]{:S(2)}, u32[]{:S(2)}) collective-permute-start(bf16[768,128]{1,0:T(8,128)(2,1)S(1)} %copy-done.4), channel_id=1, source_target_pairs={{0,32},{1,96},{32,33},{33,97},{64,1},{65,65},{96,0},{97,64},{2,34}... | collective-permute-start | bytes 589832 | tf_op jit(solution)/shard_map/ppermute | solution.py:602
  47.2 3.1 %collective-permute-start.5 = (bf16[16,4096]{1,0:T(8,128)(2,1)S(1)}, bf16[16,4096]{1,0:T(8,128)(2,1)S(1)}, u32[]{:S(2)}, u32[]{:S(2)}) collective-permute-start(bf16[16,4096]{1,0:T(8,128)(2,1)S(1)} %copy-done.6), channel_id=1, source_target_pairs={{0,8},{8,16},{16,24},{24,32},{32,40},{40,48},{48,56},{56,64},{64,7... | collective-permute-start | bytes 393224 | tf_op jit(solution)/shard_map/ppermute | solution.py:598
  50.4 0.7 pad_add_fusion.own
  51.0 0.1 broadcast_select_fusion.4
  51.1 0.6 dynamic_slice.3.lam
  51.8 0.8 broadcast_select_fusion.2
  52.6 3.2 %collective-permute-done.5.rim_ref = bf16[16,4096]{1,0:T(8,128)(2,1)S(1)} collective-permute-done((bf16[16,4096]{1,0:T(8,128)(2,1)S(1)}, bf16[16,4096]{1,0:T(8,128)(2,1)S(1)}, u32[]{:S(2)}, u32[]{:S(2)}) %collective-permute-start.5) | collective-permute-done | bytes 131104 | tf_op jit(solution)/shard_map/ppermute | solution.py:598
  55.8 0.7 copy-done.7
  56.4 10.6 %gated_conv.1._ = bf16[768,256]{1,0:T(8,128)(2,1)} custom-call(bf16[768,4096]{1,0:T(8,128)(2,1)} %h_ref.3, bf16[16,4096]{1,0:T(8,128)(2,1)} %copy-done.7, bf16[4096,256]{1,0:T(8,128)(2,1)} %wb_ref.1, bf16[4096,256]{1,0:T(8,128)(2,1)} %wc_ref.2, bf16[4096,256]{1,0:T(8,128)(2,1)} %wh_ref.1, bf16[3,256]{1,0:T(4,128)(2,1)} %taps_ref.1, ...), custom_call_target="tpu_custom_call" | custom-call | flops 4831838208 | bytes 13631488 | tf_op jit(solution)/shard_map/gated_conv/pallas_call | solution.py:195
  67.1 0.0 all-gather.15.cloned.1.call-update
  67.1 0.2 all-gather.13.cloned.1.call-start
  67.3 0.6 all-gather.9.cloned.1.call-done
  68.0 24.0 %shard_map.163 = (bf16[768,128]{1,0:T(8,128)(2,1)}, f32[2,768,128]{2,1,0:T(8,128)}, f32[2,768,128]{2,1,0:T(8,128)}, f32[2,768,128]{2,1,0:T(8,128)}) custom-call(s32[3]{0:T(128)} %pad_add_fusion.own, f32[1]{0:T(128)} %dynamic_slice.3.lam, bf16[768,128]{1,0:T(8,128)(2,1)} %get-tuple-element.33.ql_ref, bf16[768,128]{1,0:T(8,128)(2,1)} %get-tuple-element.34.qh_ref, ...), custom_call_target="tpu_custom_call" | custom-call | flops 24000000000 | bytes 4194304 | tf_op jit(solution)/shard_map/pallas_call | solution.py:365
  92.0 4.7 %all-gather.11.cloned.1.call-done = bf16[6144,256]{1,0:T(8,128)(2,1)} async-done(((bf16[768,256]{1,0:T(8,128)(2,1)}), bf16[6144,256]{1,0:T(8,128)(2,1)}) %all-gather.11.cloned.1.call-update) | async-done | bytes 3145744 | tf_op jit(solution)/shard_map/all_gather | solution.py:609
  96.8 6.7 %shard_map.164 = (bf16[768,128]{1,0:T(8,128)(2,1)}, bf16[768,128]{1,0:T(8,128)(2,1)}) custom-call(s32[3]{0:T(128)} %pad_add_fusion.own, f32[1]{0:T(128)} %dynamic_slice.3.lam, bf16[768,128]{1,0:T(8,128)(2,1)} %get-tuple-element.34.qh_ref, bf16[1,128]{1,0:T(2,128)(2,1)} %bitcast.18, bf16[768,128]{1,0:T(8,128)(2,1)} %get-tuple-element.23.low_ref, ...), custom_call_target="tpu_custom_call" | custom-call | flops 12000000000 | bytes 4194304 | tf_op jit(solution)/shard_map/pallas_call | solution.py:365
  103.5 10.9 %collective-permute-start.7 = (bf16[768,128]{1,0:T(8,128)(2,1)}, bf16[768,128]{1,0:T(8,128)(2,1)S(1)}, u32[]{:S(2)}, u32[]{:S(2)}) collective-permute-start(bf16[768,128]{1,0:T(8,128)(2,1)} %get-tuple-element.28), channel_id=1, source_target_pairs={{32,0},{96,1},{33,32},{97,33},{1,64},{65,65},{0,96},{64,97},{34,2}... | collective-permute-start | bytes 589832 | tf_op jit(solution)/shard_map/ppermute | solution.py:636
  114.4 1.9 collective-permute-start.6
  116.3 1.8 collective-permute-done.7
  118.2 5.0 %collective-permute-done.6 = bf16[768,128]{1,0:T(8,128)(2,1)S(1)} collective-permute-done((bf16[768,128]{1,0:T(8,128)(2,1)}, bf16[768,128]{1,0:T(8,128)(2,1)S(1)}, u32[]{:S(2)}, u32[]{:S(2)}) %collective-permute-start.6) | collective-permute-done | bytes 196640 | tf_op jit(solution)/shard_map/ppermute | solution.py:635
  123.2 0.8 pad_maximum_fusion
  124.0 0.0 all-gather.13.cloned.1.call-update
  124.0 3.8 %column_blocks.1 = bf16[8,2,256,512]{3,2,1,0:T(8,128)(2,1)} custom-call(bf16[256,4096]{1,0:T(8,128)(2,1)} %wc_ref.3, bf16[256,4096]{1,0:T(8,128)(2,1)} %wa_ref.1, bf16[768,256]{1,0:T(8,128)(2,1)} %get-tuple-element.32._), custom_call_target="tpu_custom_call" | custom-call | flops 3000000000 | bytes 9437184 | tf_op jit(solution)/shard_map/column_blocks/pallas_call | solution.py:409
  127.8 4.5 %all-to-all-start = ((bf16[8,2,256,512]{3,2,1,0:T(8,128)(2,1)}), bf16[8,2,256,512]{3,2,1,0:T(8,128)(2,1)}, u32[]{:S(2)}, u32[]{:S(2)}) async-start(bf16[8,2,256,512]{3,2,1,0:T(8,128)(2,1)} %column_blocks.1), calls=%async_computation | async-start | bytes 8388608 | tf_op jit(solution)/shard_map/all_to_all | solution.py:612
  132.3 0.0 all-gather.15.cloned.1.call-done
  132.3 0.1 collective-permute-start.8
  132.4 61.1 %all-to-all-done.w_ref = bf16[8,2,256,512]{3,2,1,0:T(8,128)(2,1)} async-done(((bf16[8,2,256,512]{3,2,1,0:T(8,128)(2,1)}), bf16[8,2,256,512]{3,2,1,0:T(8,128)(2,1)}, u32[]{:S(2)}, u32[]{:S(2)}) %all-to-all-start) | async-done | bytes 4194336 | tf_op jit(solution)/shard_map/all_to_all | solution.py:612
  193.6 1.1 copy-done
  194.7 5.5 %whole_conv.1.before_ref = f32[768,512]{1,0:T(8,128)} custom-call(s32[1]{0:T(128)} %bitcast.10.core, bf16[4,768,256]{2,1,0:T(8,128)(2,1)} %bitcast.14, bf16[4,768,256]{2,1,0:T(8,128)(2,1)} %copy-done, bf16[8,2,256,512]{3,2,1,0:T(8,128)(2,1)} %all-to-all-done.w_ref), custom_call_target="tpu_custom_call" | custom-call | flops 1610612736 | bytes 7340032 | tf_op jit(solution)/shard_map/whole_conv/pallas_call | solution.py:476
  200.2 5.3 %whole_last.1 = (bf16[768,512]{1,0:T(8,128)(2,1)}, f32[8,2,768]{2,1,0:T(2,128)}) custom-call(s32[1]{0:T(128)} %bitcast.1.first, bf16[8,768,256]{2,1,0:T(8,128)(2,1)} %bitcast.12, bf16[8,2,256,512]{3,2,1,0:T(8,128)(2,1)} %all-to-all-done.w_ref, f32[768,512]{1,0:T(8,128)} %whole_conv.1.before_ref), custom_call_target="tpu_custom_call" | custom-call | flops 1610612736 | bytes 7340032 | tf_op jit(solution)/shard_map/whole_last/pallas_call | solution.py:499
  205.5 4.2 %all-to-all-start.1 = ((f32[8,2,768]{2,1,0:T(2,128)}), f32[8,2,768]{2,1,0:T(2,128)S(1)}, u32[]{:S(2)}, u32[]{:S(2)}) async-start(f32[8,2,768]{2,1,0:T(2,128)} %get-tuple-element.30), calls=%async_computation.1 | async-start | bytes 98304 | tf_op jit(solution)/shard_map/all_to_all | solution.py:643
  209.7 0.6 reshape.19.gain_ref
  210.3 4.2 %all-to-all-done.1.sums_ref = f32[8,2,768]{2,1,0:T(2,128)S(1)} async-done(((f32[8,2,768]{2,1,0:T(2,128)}), f32[8,2,768]{2,1,0:T(2,128)S(1)}, u32[]{:S(2)}, u32[]{:S(2)}) %all-to-all-start.1) | async-done | bytes 49184 | tf_op jit(solution)/shard_map/all_to_all | solution.py:643
  214.5 0.6 copy-done.1
  215.1 3.2 %norm.1 = bf16[768,512]{1,0:T(8,128)(2,1)} custom-call(s32[1]{0:T(128)} %bitcast.own, bf16[768,512]{1,0:T(8,128)(2,1)} %get-tuple-element.29.mix_ref, f32[8,2,768]{2,1,0:T(2,128)} %copy-done.1, bf16[1,4096]{1,0:T(2,128)(2,1)} %reshape.19.gain_ref), custom_call_target="tpu_custom_call" | custom-call | tf_op jit(solution)/shard_map/norm/pallas_call | solution.py:554
  (18 shorter events, 0.0 us)
Async XLA Ops:
  6.5 61.5 %all-gather.9.cloned.1.call-start = ((), (), s32[]{:S(2)}) async-start(), calls=%async_computation.2 | async-start | bytes 3538944 | tf_op jit(solution)/shard_map/all_gather | solution.py:608
  18.0 18.9 %copy-start.3 = (f32[2]{0:T(128)S(1)}, f32[2]{0:T(128)}, u32[]{:S(2)}) copy-start(f32[2]{0:T(128)} %param.25) | copy-start | bytes 28
  18.0 19.5 %copy-start.5 = (bf16[768,128]{1,0:T(8,128)(2,1)S(1)}, bf16[768,128]{1,0:T(8,128)(2,1)}, u32[]{:S(2)}) copy-start(bf16[768,128]{1,0:T(8,128)(2,1)} %get-tuple-element.19) | copy-start | bytes 589828
  18.0 24.7 %copy-start.4 = (bf16[768,128]{1,0:T(8,128)(2,1)S(1)}, bf16[768,128]{1,0:T(8,128)(2,1)}, u32[]{:S(2)}) copy-start(bf16[768,128]{1,0:T(8,128)(2,1)} %get-tuple-element.18) | copy-start | bytes 589828
  18.0 29.2 %copy-start.6 = (bf16[16,4096]{1,0:T(8,128)(2,1)S(1)}, bf16[16,4096]{1,0:T(8,128)(2,1)}, u32[]{:S(2)}) copy-start(bf16[16,4096]{1,0:T(8,128)(2,1)} %get-tuple-element.22) | copy-start | bytes 393220
  18.0 16.1 %collective-permute-start.4 = (bf16[768,256]{1,0:T(8,128)(2,1)}, bf16[768,256]{1,0:T(8,128)(2,1)S(1)}, u32[]{:S(2)}, u32[]{:S(2)}) collective-permute-start(bf16[768,256]{1,0:T(8,128)(2,1)} %get-tuple-element.21), channel_id=1, source_target_pairs={{0,32},{1,96},{32,33},{33,97},{64,1},{65,65},{96,0},{97,64},{2,34}... | collective-permute-start | bytes 1179656 | tf_op jit(solution)/shard_map/ppermute | solution.py:600
  25.2 9.9 %collective-permute-start.3 = (bf16[768,256]{1,0:T(8,128)(2,1)}, bf16[768,256]{1,0:T(8,128)(2,1)S(1)}, u32[]{:S(2)}, u32[]{:S(2)}) collective-permute-start(bf16[768,256]{1,0:T(8,128)(2,1)} %get-tuple-element.20), channel_id=1, source_target_pairs={{0,0},{1,64},{32,1},{33,65},{64,33},{65,97},{96,32},{97,96},{2,2},... | collective-permute-start | bytes 1179656 | tf_op jit(solution)/shard_map/ppermute | solution.py:599
  36.1 60.6 %all-gather.11.cloned.1.call-start = ((), (), s32[]{:S(2)}) async-start(), calls=%async_computation.3 | async-start | bytes 3538944 | tf_op jit(solution)/shard_map/all_gather | solution.py:609
  36.9 95.4 %all-gather.15.cloned.1.call-start = ((), (), s32[]{:S(2)}) async-start(), calls=%async_computation.5 | async-start | bytes 1966080 | tf_op jit(solution)/shard_map/all_gather | solution.py:616
  36.9 14.1 %collective-permute-start = (f32[2]{0:T(128)S(1)}, f32[2]{0:T(128)S(1)}, u32[]{:S(2)}, u32[]{:S(2)}) collective-permute-start(f32[2]{0:T(128)S(1)} %copy-done.3), channel_id=1, source_target_pairs={{0,1},{1,0},{2,3},{3,2},{4,5},{5,4},{6,7},{7,6},{8,9},{9,8},{10,11... | collective-permute-start | bytes 32 | tf_op jit(solution)/shard_map/ppermute | solution.py:592
  37.5 14.3 %collective-permute-start.2 = (bf16[768,128]{1,0:T(8,128)(2,1)S(1)}, bf16[768,128]{1,0:T(8,128)(2,1)S(1)}, u32[]{:S(2)}, u32[]{:S(2)}) collective-permute-start(bf16[768,128]{1,0:T(8,128)(2,1)S(1)} %copy-done.5), channel_id=1, source_target_pairs={{0,0},{1,64},{32,1},{33,65},{64,33},{65,97},{96,32},{97,96},{2,2},... | collective-permute-start | bytes 589832 | tf_op jit(solution)/shard_map/ppermute | solution.py:601
  42.7 9.1 %collective-permute-start.1 = (bf16[768,128]{1,0:T(8,128)(2,1)S(1)}, bf16[768,128]{1,0:T(8,128)(2,1)S(1)}, u32[]{:S(2)}, u32[]{:S(2)}) collective-permute-start(bf16[768,128]{1,0:T(8,128)(2,1)S(1)} %copy-done.4), channel_id=1, source_target_pairs={{0,32},{1,96},{32,33},{33,97},{64,1},{65,65},{96,0},{97,64},{2,34}... | collective-permute-start | bytes 589832 | tf_op jit(solution)/shard_map/ppermute | solution.py:602
  47.2 8.5 %collective-permute-start.5 = (bf16[16,4096]{1,0:T(8,128)(2,1)S(1)}, bf16[16,4096]{1,0:T(8,128)(2,1)S(1)}, u32[]{:S(2)}, u32[]{:S(2)}) collective-permute-start(bf16[16,4096]{1,0:T(8,128)(2,1)S(1)} %copy-done.6), channel_id=1, source_target_pairs={{0,8},{8,16},{16,24},{24,32},{32,40},{40,48},{48,56},{56,64},{64,7... | collective-permute-start | bytes 393224 | tf_op jit(solution)/shard_map/ppermute | solution.py:598
  55.8 0.7 copy-start.7
  67.1 133.1 %all-gather.13.cloned.1.call-start = ((), (), s32[]{:S(2)}) async-start(), calls=%async_computation.4 | async-start | bytes 3538944 | tf_op jit(solution)/shard_map/all_gather | solution.py:637
  103.5 14.7 %collective-permute-start.7 = (bf16[768,128]{1,0:T(8,128)(2,1)}, bf16[768,128]{1,0:T(8,128)(2,1)S(1)}, u32[]{:S(2)}, u32[]{:S(2)}) collective-permute-start(bf16[768,128]{1,0:T(8,128)(2,1)} %get-tuple-element.28), channel_id=1, source_target_pairs={{32,0},{96,1},{33,32},{97,33},{1,64},{65,65},{0,96},{64,97},{34,2}... | collective-permute-start | bytes 589832 | tf_op jit(solution)/shard_map/ppermute | solution.py:636
  114.4 8.8 %collective-permute-start.6 = (bf16[768,128]{1,0:T(8,128)(2,1)}, bf16[768,128]{1,0:T(8,128)(2,1)S(1)}, u32[]{:S(2)}, u32[]{:S(2)}) collective-permute-start(bf16[768,128]{1,0:T(8,128)(2,1)} %get-tuple-element.27), channel_id=1, source_target_pairs={{0,0},{64,1},{1,32},{65,33},{33,64},{97,65},{32,96},{96,97},{2,2},... | collective-permute-start | bytes 589832 | tf_op jit(solution)/shard_map/ppermute | solution.py:635
  127.8 65.8 %all-to-all-start = ((bf16[8,2,256,512]{3,2,1,0:T(8,128)(2,1)}), bf16[8,2,256,512]{3,2,1,0:T(8,128)(2,1)}, u32[]{:S(2)}, u32[]{:S(2)}) async-start(bf16[8,2,256,512]{3,2,1,0:T(8,128)(2,1)} %column_blocks.1), calls=%async_computation | async-start | bytes 8388608 | tf_op jit(solution)/shard_map/all_to_all | solution.py:612
  132.3 61.2 %collective-permute-start.8 = (bf16[4,768,256]{2,1,0:T(8,128)(2,1)}, bf16[4,768,256]{2,1,0:T(8,128)(2,1)S(1)}, u32[]{:S(2)}, u32[]{:S(2)}) collective-permute-start(bf16[4,768,256]{2,1,0:T(8,128)(2,1)} %bitcast.13), channel_id=1, source_target_pairs={{0,1},{1,0},{2,3},{3,2},{4,5},{5,4},{6,7},{7,6},{8,9},{9,8},{10,11... | collective-permute-start | bytes 4718600 | tf_op jit(solution)/shard_map/ppermute | solution.py:638
  193.6 1.1 copy-start
  200.2 9.5 %copy-start.2 = (bf16[4096]{0:T(1024)(128)(2,1)S(1)}, bf16[4096]{0:T(1024)(128)(2,1)}, u32[]{:S(2)}) copy-start(bf16[4096]{0:T(1024)(128)(2,1)} %param.29) | copy-start | bytes 24580
  205.5 9.0 %all-to-all-start.1 = ((f32[8,2,768]{2,1,0:T(2,128)}), f32[8,2,768]{2,1,0:T(2,128)S(1)}, u32[]{:S(2)}, u32[]{:S(2)}) async-start(f32[8,2,768]{2,1,0:T(2,128)} %get-tuple-element.30), calls=%async_computation.1 | async-start | bytes 98304 | tf_op jit(solution)/shard_map/all_to_all | solution.py:643
  214.5 0.6 copy-start.1
Sparse Core Ops, SparseCore 0:
  36.2 31.6 all-gather.8
  69.7 27.0 all-gather.10
  98.4 25.8 all-gather.14
  125.9 44.5 all-gather.12

commit v6 on v5

--- a/solution.py
+++ b/solution.py
@@ -306,7 +306,9 @@
     return (kb % 4) * 2 + 3 - kb // 4
 
 
-def low_kernel(own, lam, ql_ref, qh_ref, gain_ref, kv_hbm, _, o_ref, m_o, l_o, a_o, qz, kv_ref, sem):
+def low_kernel(
+    own, lam, ql_ref, qh_ref, gain_ref, high_ref, kv_hbm, _, o_ref, m_o, l_o, a_o, qz, kv_ref, sem
+):
     step = pl.program_id(0)
 
     def load(kb):
@@ -332,6 +334,10 @@
         load(own[0]).wait()
         attend_diagonal(own[0], refs)
         o_ref[...] = finish(lam, gain_ref, l_o, a_o)
+
+    @pl.when(step == 1)
+    def _():
+        attend_diagonal(0, (qz, high_ref, m_o, l_o, a_o))
 
 
 def high_kernel(
@@ -343,15 +349,13 @@
 
     for kb in range(8, 16):
 
-        @pl.when(kb <= own[1])
+        @pl.when(kb < own[1])
         def _(kb=kb):
             load(kb).start()
 
     split_maps(qh_ref[...], qz)
     refs = (qz, kv_ref, m_i, l_i, a_i)
     attend_blocks(8, own[1] - 8, lambda kb: kb - 8, lambda kb: load(kb).wait(), refs)
-    load(own[1]).wait()
-    attend_diagonal(own[1] - 8, refs)
     high = finish(lam, gain_ref, l_i, a_i)
     low_first = own[2] == 0
     oa_ref[...] = jnp.where(low_first, low_ref[...], high)
@@ -627,7 +631,12 @@
     rows = jax.ShapeDtypeStruct((ROWS, VD), jnp.bfloat16)
     state = (jax.ShapeDtypeStruct((2, ROWS, VD), jnp.float32),) * 3
     o_low, *carried = attention_call(
-        low_kernel, 2, (own, lam, q_low, q_high, gain), (rows, *state), (kv_low, conv_out), 12
+        low_kernel,
+        2,
+        (own, lam, q_low, q_high, gain, own_high[None]),
+        (rows, *state),
+        (kv_low, conv_out),
+        12,
     )
     o_a, o_b = attention_call(
         high_kernel, 1, (own, lam, q_high, gain, o_low, *carried), (rows, rows), (kv_high,), 6

time: 228 us -> 227 us (level)
    ppermute x1, starting transfers between devices: 1.92 us -> 7.02 us  [per_device(): head_a = lax.ppermute(head_a, z_core, route_a)]
    ppermute x1, waiting for transfers between devices: 0.96 us -> 6.05 us  [per_device(): head_a = lax.ppermute(head_a, z_core, route_a)]
    ppermute x1, starting transfers between devices: 7.18 us -> 2.62 us  [per_device(): head_b = lax.ppermute(head_b, z_core, route_b)]
    ppermute x1, waiting for transfers between devices: 7.02 us -> 3.02 us  [per_device(): head_b = lax.ppermute(head_b, z_core, route_b)]
    ppermute x1, starting transfers between devices: 5.18 us -> 1.91 us  [per_device(): q_a = lax.ppermute(q_a, z_core, route_a)]
    all_gather x1, waiting for transfers between devices: 4.75 us -> 2.02 us  [per_device(): kv_high = lax.all_gather(own_high, ('x', 'c'), axis=0)]
  transfers between devices with their start and end apart: 15 -> 15, of which waited for: 9 -> 10; matrix products, arithmetic and copies ran while one was open for 2% -> 2% of each run, Pallas kernels for 23% -> 23%
where the time goes in v6:
time: 227 us; the launch traced here: 224 us
  waiting for transfers between devices  90.1 us (40%)
  Pallas kernels  69.7 us (31%)
  starting transfers between devices  43 us (19%)
  between operations  13.4 us (6%)
  other arithmetic  3.98 us (2%)
  local copies, waits for them, and re-layouts  3.68 us (2%)
    all_to_all x1, waiting for transfers between devices, per_device(): lax.all_to_all(blocks, ('y', 'c'), split_axis=0, concat_axis=0, tiled=True)  61.1 us
    pallas_call x2, Pallas kernels, attention_call(): pl.pallas_call(kernel, out_shape=outs, grid_spec=pltpu.PrefetchScalarGrid...  30.4 us
    ppermute x1, starting transfers between devices, per_device(): back_b = lax.ppermute(o_b, z_core, reverse(route_b))  11.6 us
    pallas_call x1, Pallas kernels, project(): pl.pallas_call(qkv_kernel, out_shape=tuple((jax.ShapeDtypeStruct(shape, j...  10.8 us
    pallas_call x1, Pallas kernels, gated_conv(): pl.pallas_call(conv_kernel, out_shape=jax.ShapeDtypeStruct((ROWS, 256), j...  10.6 us
    ppermute x1, starting transfers between devices, per_device(): head_a = lax.ppermute(head_a, z_core, route_a)  7.02 us
    ppermute x1, waiting for transfers between devices, per_device(): head_a = lax.ppermute(head_a, z_core, route_a)  6.05 us
    pallas_call x1, Pallas kernels, whole_conv(): pl.pallas_call(whole_conv_kernel, out_shape=jax.ShapeDtypeStruct((ROWS, w...  5.49 us
  transfers between devices with their start and end apart: 15, of which 10 were waited for; matrix products, arithmetic and copies ran while one was open for 2% of the time, Pallas kernels for 23%

profile of v6, /device:TPU:1, one launch (start us, length us, event | category | flops | bytes accessed | tf_op | source)
XLA Modules:
  0.0 223.7 jit_solution(13294565471478039460)
XLA Ops:
  6.5 0.7 pad_add_fusion.1.where
  7.2 10.8 %qkv.1 = (bf16[768,256]{1,0:T(8,128)(2,1)}, bf16[768,256]{1,0:T(8,128)(2,1)}, bf16[768,128]{1,0:T(8,128)(2,1)}, bf16[768,128]{1,0:T(8,128)(2,1)}, bf16[16,4096]{1,0:T(8,128)(2,1)}) custom-call(s32[2]{0:T(128)} %pad_add_fusion.1.where, bf16[768,4096]{1,0:T(8,128)(2,1)} %h_ref.3, bf16[4096,256]{1,0:T(8,128)(2,1)} %wk_ref.1, bf16[4096,256]{1,0:T(8,128)(2,1)} %wv_ref.1, ...), custom_call_target="tpu_custom_call" | custom-call | flops 4831838208 | bytes 13631488 | tf_op jit(solution)/shard_map/qkv/pallas_call | solution.py:149
  18.0 7.0 %collective-permute-start.4 = (bf16[768,256]{1,0:T(8,128)(2,1)}, bf16[768,256]{1,0:T(8,128)(2,1)S(1)}, u32[]{:S(2)}, u32[]{:S(2)}) collective-permute-start(bf16[768,256]{1,0:T(8,128)(2,1)} %get-tuple-element.21), channel_id=1, source_target_pairs={{0,0},{1,64},{32,1},{33,65},{64,33},{65,97},{96,32},{97,96},{2,2},... | collective-permute-start | bytes 1179656 | tf_op jit(solution)/shard_map/ppermute | solution.py:603
  25.1 2.6 %collective-permute-start.3 = (bf16[768,256]{1,0:T(8,128)(2,1)}, bf16[768,256]{1,0:T(8,128)(2,1)S(1)}, u32[]{:S(2)}, u32[]{:S(2)}) collective-permute-start(bf16[768,256]{1,0:T(8,128)(2,1)} %get-tuple-element.20), channel_id=1, source_target_pairs={{0,32},{1,96},{32,33},{33,97},{64,1},{65,65},{96,0},{97,64},{2,34}... | collective-permute-start | bytes 1179656 | tf_op jit(solution)/shard_map/ppermute | solution.py:604
  27.7 6.0 %collective-permute-done.4 = bf16[768,256]{1,0:T(8,128)(2,1)S(1)} collective-permute-done((bf16[768,256]{1,0:T(8,128)(2,1)}, bf16[768,256]{1,0:T(8,128)(2,1)S(1)}, u32[]{:S(2)}, u32[]{:S(2)}) %collective-permute-start.4) | collective-permute-done | bytes 393248 | tf_op jit(solution)/shard_map/ppermute | solution.py:603
  33.8 3.0 %collective-permute-done.3 = bf16[768,256]{1,0:T(8,128)(2,1)S(1)} collective-permute-done((bf16[768,256]{1,0:T(8,128)(2,1)}, bf16[768,256]{1,0:T(8,128)(2,1)S(1)}, u32[]{:S(2)}, u32[]{:S(2)}) %collective-permute-start.3) | collective-permute-done | bytes 393248 | tf_op jit(solution)/shard_map/ppermute | solution.py:604
  36.8 1.0 broadcast_select_fusion
  37.8 0.0 all-gather.9.cloned.1.call-update
  37.8 0.0 all-gather.11.cloned.1.call-start
  37.8 0.7 all-gather.11.cloned.1.call-update
  38.5 0.0 all-gather.15.cloned.1.call-start
  38.6 1.6 collective-permute-start
  40.2 1.9 collective-permute-start.2
  42.1 4.1 %collective-permute-start.1 = (bf16[768,128]{1,0:T(8,128)(2,1)S(1)}, bf16[768,128]{1,0:T(8,128)(2,1)S(1)}, u32[]{:S(2)}, u32[]{:S(2)}) collective-permute-start(bf16[768,128]{1,0:T(8,128)(2,1)S(1)} %copy-done.4), channel_id=1, source_target_pairs={{0,32},{1,96},{32,33},{33,97},{64,1},{65,65},{96,0},{97,64},{2,34}... | collective-permute-start | bytes 589832 | tf_op jit(solution)/shard_map/ppermute | solution.py:606
  46.2 3.1 %collective-permute-start.5 = (bf16[16,4096]{1,0:T(8,128)(2,1)S(1)}, bf16[16,4096]{1,0:T(8,128)(2,1)S(1)}, u32[]{:S(2)}, u32[]{:S(2)}) collective-permute-start(bf16[16,4096]{1,0:T(8,128)(2,1)S(1)} %copy-done.6), channel_id=1, source_target_pairs={{0,8},{8,16},{16,24},{24,32},{32,40},{40,48},{48,56},{56,64},{64,7... | collective-permute-start | bytes 393224 | tf_op jit(solution)/shard_map/ppermute | solution.py:602
  49.3 0.7 pad_add_fusion.own
  50.0 0.1 broadcast_select_fusion.4
  50.0 0.6 dynamic_slice.3.lam
  50.7 0.2 collective-permute-done.1
  50.8 0.8 broadcast_select_fusion.2
  51.7 3.0 %collective-permute-done.5.rim_ref = bf16[16,4096]{1,0:T(8,128)(2,1)S(1)} collective-permute-done((bf16[16,4096]{1,0:T(8,128)(2,1)S(1)}, bf16[16,4096]{1,0:T(8,128)(2,1)S(1)}, u32[]{:S(2)}, u32[]{:S(2)}) %collective-permute-start.5) | collective-permute-done | bytes 131104 | tf_op jit(solution)/shard_map/ppermute | solution.py:602
  54.7 0.7 copy-done.7
  55.3 10.6 %gated_conv.1._ = bf16[768,256]{1,0:T(8,128)(2,1)} custom-call(bf16[768,4096]{1,0:T(8,128)(2,1)} %h_ref.3, bf16[16,4096]{1,0:T(8,128)(2,1)} %copy-done.7, bf16[4096,256]{1,0:T(8,128)(2,1)} %wb_ref.1, bf16[4096,256]{1,0:T(8,128)(2,1)} %wc_ref.2, bf16[4096,256]{1,0:T(8,128)(2,1)} %wh_ref.1, bf16[3,256]{1,0:T(4,128)(2,1)} %taps_ref.1, ...), custom_call_target="tpu_custom_call" | custom-call | flops 4831838208 | bytes 13631488 | tf_op jit(solution)/shard_map/gated_conv/pallas_call | solution.py:195
  66.0 0.0 all-gather.15.cloned.1.call-update
  66.0 0.2 all-gather.13.cloned.1.call-start
  66.2 2.9 %all-gather.9.cloned.1.call-done = bf16[6144,256]{1,0:T(8,128)(2,1)} async-done(((bf16[768,256]{1,0:T(8,128)(2,1)}), bf16[6144,256]{1,0:T(8,128)(2,1)}) %all-gather.9.cloned.1.call-update) | async-done | bytes 3145744 | tf_op jit(solution)/shard_map/all_gather | solution.py:612
  69.1 25.8 %shard_map.163 = (bf16[768,128]{1,0:T(8,128)(2,1)}, f32[2,768,128]{2,1,0:T(8,128)}, f32[2,768,128]{2,1,0:T(8,128)}, f32[2,768,128]{2,1,0:T(8,128)}) custom-call(s32[3]{0:T(128)} %pad_add_fusion.own, f32[1]{0:T(128)} %dynamic_slice.3.lam, bf16[768,128]{1,0:T(8,128)(2,1)} %get-tuple-element.33.ql_ref, bf16[768,128]{1,0:T(8,128)(2,1)} %get-tuple-element.34.qh_ref, ...), custom_call_target="tpu_custom_call" | custom-call | flops 24000000000 | bytes 4194304 | tf_op jit(solution)/shard_map/pallas_call | solution.py:369
  94.9 2.0 all-gather.11.cloned.1.call-done
  97.0 4.6 %shard_map.164 = (bf16[768,128]{1,0:T(8,128)(2,1)}, bf16[768,128]{1,0:T(8,128)(2,1)}) custom-call(s32[3]{0:T(128)} %pad_add_fusion.own, f32[1]{0:T(128)} %dynamic_slice.3.lam, bf16[768,128]{1,0:T(8,128)(2,1)} %get-tuple-element.34.qh_ref, bf16[1,128]{1,0:T(2,128)(2,1)} %bitcast.20, bf16[768,128]{1,0:T(8,128)(2,1)} %get-tuple-element.23.low_ref, ...), custom_call_target="tpu_custom_call" | custom-call | flops 12000000000 | bytes 4194304 | tf_op jit(solution)/shard_map/pallas_call | solution.py:369
  101.6 11.6 %collective-permute-start.7 = (bf16[768,128]{1,0:T(8,128)(2,1)}, bf16[768,128]{1,0:T(8,128)(2,1)S(1)}, u32[]{:S(2)}, u32[]{:S(2)}) collective-permute-start(bf16[768,128]{1,0:T(8,128)(2,1)} %get-tuple-element.28), channel_id=1, source_target_pairs={{32,0},{96,1},{33,32},{97,33},{1,64},{65,65},{0,96},{64,97},{34,2}... | collective-permute-start | bytes 589832 | tf_op jit(solution)/shard_map/ppermute | solution.py:645
  113.2 1.9 collective-permute-start.6
  115.2 1.8 collective-permute-done.7
  117.0 5.0 %collective-permute-done.6 = bf16[768,128]{1,0:T(8,128)(2,1)S(1)} collective-permute-done((bf16[768,128]{1,0:T(8,128)(2,1)}, bf16[768,128]{1,0:T(8,128)(2,1)S(1)}, u32[]{:S(2)}, u32[]{:S(2)}) %collective-permute-start.6) | collective-permute-done | bytes 196640 | tf_op jit(solution)/shard_map/ppermute | solution.py:644
  122.0 0.8 pad_maximum_fusion
  122.8 0.0 all-gather.13.cloned.1.call-update
  122.8 3.8 %column_blocks.1 = bf16[8,2,256,512]{3,2,1,0:T(8,128)(2,1)} custom-call(bf16[256,4096]{1,0:T(8,128)(2,1)} %wc_ref.3, bf16[256,4096]{1,0:T(8,128)(2,1)} %wa_ref.1, bf16[768,256]{1,0:T(8,128)(2,1)} %get-tuple-element.31._), custom_call_target="tpu_custom_call" | custom-call | flops 3000000000 | bytes 9437184 | tf_op jit(solution)/shard_map/column_blocks/pallas_call | solution.py:413
  126.6 4.5 %all-to-all-start = ((bf16[8,2,256,512]{3,2,1,0:T(8,128)(2,1)}), bf16[8,2,256,512]{3,2,1,0:T(8,128)(2,1)}, u32[]{:S(2)}, u32[]{:S(2)}) async-start(bf16[8,2,256,512]{3,2,1,0:T(8,128)(2,1)} %column_blocks.1), calls=%async_computation | async-start | bytes 8388608 | tf_op jit(solution)/shard_map/all_to_all | solution.py:616
  131.1 0.0 all-gather.15.cloned.1.call-done
  131.2 0.1 collective-permute-start.8
  131.3 61.1 %all-to-all-done.w_ref = bf16[8,2,256,512]{3,2,1,0:T(8,128)(2,1)} async-done(((bf16[8,2,256,512]{3,2,1,0:T(8,128)(2,1)}), bf16[8,2,256,512]{3,2,1,0:T(8,128)(2,1)}, u32[]{:S(2)}, u32[]{:S(2)}) %all-to-all-start) | async-done | bytes 4194336 | tf_op jit(solution)/shard_map/all_to_all | solution.py:616
  192.4 1.1 copy-done
  193.5 5.5 %whole_conv.1.before_ref = f32[768,512]{1,0:T(8,128)} custom-call(s32[1]{0:T(128)} %bitcast.11.core, bf16[4,768,256]{2,1,0:T(8,128)(2,1)} %bitcast.15, bf16[4,768,256]{2,1,0:T(8,128)(2,1)} %copy-done, bf16[8,2,256,512]{3,2,1,0:T(8,128)(2,1)} %all-to-all-done.w_ref), custom_call_target="tpu_custom_call" | custom-call | flops 1610612736 | bytes 7340032 | tf_op jit(solution)/shard_map/whole_conv/pallas_call | solution.py:480
  199.0 5.3 %whole_last.1 = (bf16[768,512]{1,0:T(8,128)(2,1)}, f32[8,2,768]{2,1,0:T(2,128)}) custom-call(s32[1]{0:T(128)} %bitcast.1.first, bf16[8,768,256]{2,1,0:T(8,128)(2,1)} %bitcast.13, bf16[8,2,256,512]{3,2,1,0:T(8,128)(2,1)} %all-to-all-done.w_ref, f32[768,512]{1,0:T(8,128)} %whole_conv.1.before_ref), custom_call_target="tpu_custom_call" | custom-call | flops 1610612736 | bytes 7340032 | tf_op jit(solution)/shard_map/whole_last/pallas_call | solution.py:503
  204.3 4.2 %all-to-all-start.1 = ((f32[8,2,768]{2,1,0:T(2,128)}), f32[8,2,768]{2,1,0:T(2,128)S(1)}, u32[]{:S(2)}, u32[]{:S(2)}) async-start(f32[8,2,768]{2,1,0:T(2,128)} %get-tuple-element.30), calls=%async_computation.1 | async-start | bytes 98304 | tf_op jit(solution)/shard_map/all_to_all | solution.py:652
  208.6 0.6 reshape.19.gain_ref
  209.2 4.2 %all-to-all-done.1.sums_ref = f32[8,2,768]{2,1,0:T(2,128)S(1)} async-done(((f32[8,2,768]{2,1,0:T(2,128)}), f32[8,2,768]{2,1,0:T(2,128)S(1)}, u32[]{:S(2)}, u32[]{:S(2)}) %all-to-all-start.1) | async-done | bytes 49184 | tf_op jit(solution)/shard_map/all_to_all | solution.py:652
  213.4 0.6 copy-done.1
  214.0 3.2 %norm.1 = bf16[768,512]{1,0:T(8,128)(2,1)} custom-call(s32[1]{0:T(128)} %bitcast.own, bf16[768,512]{1,0:T(8,128)(2,1)} %get-tuple-element.29.mix_ref, f32[8,2,768]{2,1,0:T(2,128)} %copy-done.1, bf16[1,4096]{1,0:T(2,128)(2,1)} %reshape.19.gain_ref), custom_call_target="tpu_custom_call" | custom-call | tf_op jit(solution)/shard_map/norm/pallas_call | solution.py:558
  (18 shorter events, 0.0 us)
Async XLA Ops:
  6.5 62.6 %all-gather.9.cloned.1.call-start = ((), (), s32[]{:S(2)}) async-start(), calls=%async_computation.2 | async-start | bytes 3538944 | tf_op jit(solution)/shard_map/all_gather | solution.py:612
  18.0 20.6 %copy-start.3 = (f32[2]{0:T(128)S(1)}, f32[2]{0:T(128)}, u32[]{:S(2)}) copy-start(f32[2]{0:T(128)} %param.25) | copy-start | bytes 28
  18.0 22.1 %copy-start.5 = (bf16[768,128]{1,0:T(8,128)(2,1)S(1)}, bf16[768,128]{1,0:T(8,128)(2,1)}, u32[]{:S(2)}) copy-start(bf16[768,128]{1,0:T(8,128)(2,1)} %get-tuple-element.19) | copy-start | bytes 589828
  18.0 24.0 %copy-start.4 = (bf16[768,128]{1,0:T(8,128)(2,1)S(1)}, bf16[768,128]{1,0:T(8,128)(2,1)}, u32[]{:S(2)}) copy-start(bf16[768,128]{1,0:T(8,128)(2,1)} %get-tuple-element.18) | copy-start | bytes 589828
  18.0 28.1 %copy-start.6 = (bf16[16,4096]{1,0:T(8,128)(2,1)S(1)}, bf16[16,4096]{1,0:T(8,128)(2,1)}, u32[]{:S(2)}) copy-start(bf16[16,4096]{1,0:T(8,128)(2,1)} %get-tuple-element.22) | copy-start | bytes 393220
  18.0 15.7 %collective-permute-start.4 = (bf16[768,256]{1,0:T(8,128)(2,1)}, bf16[768,256]{1,0:T(8,128)(2,1)S(1)}, u32[]{:S(2)}, u32[]{:S(2)}) collective-permute-start(bf16[768,256]{1,0:T(8,128)(2,1)} %get-tuple-element.21), channel_id=1, source_target_pairs={{0,0},{1,64},{32,1},{33,65},{64,33},{65,97},{96,32},{97,96},{2,2},... | collective-permute-start | bytes 1179656 | tf_op jit(solution)/shard_map/ppermute | solution.py:603
  25.1 11.7 %collective-permute-start.3 = (bf16[768,256]{1,0:T(8,128)(2,1)}, bf16[768,256]{1,0:T(8,128)(2,1)S(1)}, u32[]{:S(2)}, u32[]{:S(2)}) collective-permute-start(bf16[768,256]{1,0:T(8,128)(2,1)} %get-tuple-element.20), channel_id=1, source_target_pairs={{0,32},{1,96},{32,33},{33,97},{64,1},{65,65},{96,0},{97,64},{2,34}... | collective-permute-start | bytes 1179656 | tf_op jit(solution)/shard_map/ppermute | solution.py:604
  37.8 59.2 %all-gather.11.cloned.1.call-start = ((), (), s32[]{:S(2)}) async-start(), calls=%async_computation.3 | async-start | bytes 3538944 | tf_op jit(solution)/shard_map/all_gather | solution.py:613
  38.5 92.6 %all-gather.15.cloned.1.call-start = ((), (), s32[]{:S(2)}) async-start(), calls=%async_computation.5 | async-start | bytes 1966080 | tf_op jit(solution)/shard_map/all_gather | solution.py:620
  38.6 11.4 %collective-permute-start = (f32[2]{0:T(128)S(1)}, f32[2]{0:T(128)S(1)}, u32[]{:S(2)}, u32[]{:S(2)}) collective-permute-start(f32[2]{0:T(128)S(1)} %copy-done.3), channel_id=1, source_target_pairs={{0,1},{1,0},{2,3},{3,2},{4,5},{5,4},{6,7},{7,6},{8,9},{9,8},{10,11... | collective-permute-start | bytes 32 | tf_op jit(solution)/shard_map/ppermute | solution.py:596
  40.2 10.5 %collective-permute-start.2 = (bf16[768,128]{1,0:T(8,128)(2,1)S(1)}, bf16[768,128]{1,0:T(8,128)(2,1)S(1)}, u32[]{:S(2)}, u32[]{:S(2)}) collective-permute-start(bf16[768,128]{1,0:T(8,128)(2,1)S(1)} %copy-done.5), channel_id=1, source_target_pairs={{0,0},{1,64},{32,1},{33,65},{64,33},{65,97},{96,32},{97,96},{2,2},... | collective-permute-start | bytes 589832 | tf_op jit(solution)/shard_map/ppermute | solution.py:605
  42.1 8.8 %collective-permute-start.1 = (bf16[768,128]{1,0:T(8,128)(2,1)S(1)}, bf16[768,128]{1,0:T(8,128)(2,1)S(1)}, u32[]{:S(2)}, u32[]{:S(2)}) collective-permute-start(bf16[768,128]{1,0:T(8,128)(2,1)S(1)} %copy-done.4), channel_id=1, source_target_pairs={{0,32},{1,96},{32,33},{33,97},{64,1},{65,65},{96,0},{97,64},{2,34}... | collective-permute-start | bytes 589832 | tf_op jit(solution)/shard_map/ppermute | solution.py:606
  46.2 8.5 %collective-permute-start.5 = (bf16[16,4096]{1,0:T(8,128)(2,1)S(1)}, bf16[16,4096]{1,0:T(8,128)(2,1)S(1)}, u32[]{:S(2)}, u32[]{:S(2)}) collective-permute-start(bf16[16,4096]{1,0:T(8,128)(2,1)S(1)} %copy-done.6), channel_id=1, source_target_pairs={{0,8},{8,16},{16,24},{24,32},{32,40},{40,48},{48,56},{56,64},{64,7... | collective-permute-start | bytes 393224 | tf_op jit(solution)/shard_map/ppermute | solution.py:602
  54.7 0.7 copy-start.7
  66.0 133.0 %all-gather.13.cloned.1.call-start = ((), (), s32[]{:S(2)}) async-start(), calls=%async_computation.4 | async-start | bytes 3538944 | tf_op jit(solution)/shard_map/all_gather | solution.py:646
  101.6 15.4 %collective-permute-start.7 = (bf16[768,128]{1,0:T(8,128)(2,1)}, bf16[768,128]{1,0:T(8,128)(2,1)S(1)}, u32[]{:S(2)}, u32[]{:S(2)}) collective-permute-start(bf16[768,128]{1,0:T(8,128)(2,1)} %get-tuple-element.28), channel_id=1, source_target_pairs={{32,0},{96,1},{33,32},{97,33},{1,64},{65,65},{0,96},{64,97},{34,2}... | collective-permute-start | bytes 589832 | tf_op jit(solution)/shard_map/ppermute | solution.py:645
  113.2 8.8 %collective-permute-start.6 = (bf16[768,128]{1,0:T(8,128)(2,1)}, bf16[768,128]{1,0:T(8,128)(2,1)S(1)}, u32[]{:S(2)}, u32[]{:S(2)}) collective-permute-start(bf16[768,128]{1,0:T(8,128)(2,1)} %get-tuple-element.27), channel_id=1, source_target_pairs={{0,0},{64,1},{1,32},{65,33},{33,64},{97,65},{32,96},{96,97},{2,2},... | collective-permute-start | bytes 589832 | tf_op jit(solution)/shard_map/ppermute | solution.py:644
  126.6 65.8 %all-to-all-start = ((bf16[8,2,256,512]{3,2,1,0:T(8,128)(2,1)}), bf16[8,2,256,512]{3,2,1,0:T(8,128)(2,1)}, u32[]{:S(2)}, u32[]{:S(2)}) async-start(bf16[8,2,256,512]{3,2,1,0:T(8,128)(2,1)} %column_blocks.1), calls=%async_computation | async-start | bytes 8388608 | tf_op jit(solution)/shard_map/all_to_all | solution.py:616
  131.2 61.2 %collective-permute-start.8 = (bf16[4,768,256]{2,1,0:T(8,128)(2,1)}, bf16[4,768,256]{2,1,0:T(8,128)(2,1)S(1)}, u32[]{:S(2)}, u32[]{:S(2)}) collective-permute-start(bf16[4,768,256]{2,1,0:T(8,128)(2,1)} %bitcast.14), channel_id=1, source_target_pairs={{0,1},{1,0},{2,3},{3,2},{4,5},{5,4},{6,7},{7,6},{8,9},{9,8},{10,11... | collective-permute-start | bytes 4718600 | tf_op jit(solution)/shard_map/ppermute | solution.py:647
  192.4 1.1 copy-start
  199.0 9.5 %copy-start.2 = (bf16[4096]{0:T(1024)(128)(2,1)S(1)}, bf16[4096]{0:T(1024)(128)(2,1)}, u32[]{:S(2)}) copy-start(bf16[4096]{0:T(1024)(128)(2,1)} %param.29) | copy-start | bytes 24580
  204.3 9.0 %all-to-all-start.1 = ((f32[8,2,768]{2,1,0:T(2,128)}), f32[8,2,768]{2,1,0:T(2,128)S(1)}, u32[]{:S(2)}, u32[]{:S(2)}) async-start(f32[8,2,768]{2,1,0:T(2,128)} %get-tuple-element.30), calls=%async_computation.1 | async-start | bytes 98304 | tf_op jit(solution)/shard_map/all_to_all | solution.py:652
  213.4 0.6 copy-start.1
Sparse Core Ops, SparseCore 0:
  37.9 31.1 all-gather.8
  70.8 26.1 all-gather.10
  98.6 25.8 all-gather.14
  126.1 43.8 all-gather.12
